TPU v7x, 32 devices: a whole 2x2x4 slice. The times are simulated.
32 devices in a mesh: ep: 4 (over z), tp: 8 (over y, x, core).
Axes of the slice: x: 2, y: 2, z: 4, core: 2. Of those that a mesh axis runs over, the one named last changes fastest.
Arguments:
- tokens: bfloat16 [4096, 2048], P(('ep', 'tp')), may hold values from -40 to 40
- norm_gain: float32 [2048], replicated, may hold values from 0.1 to 1.9
- routes: int32 [4096, 2], P(('ep', 'tp')), may hold values from 0 to 7, all different within a row; in each aligned block of 128 rows (0 to 127, 128 to 255, ...) at most 64 rows name the same one
- gates: float32 [4096, 2], P(('ep', 'tp')), may hold values from 0.25 to 2
- expert_gate: bfloat16 [8, 2048, 512], P('tp'), may hold values from -0.125 to 0.125
- expert_up: bfloat16 [8, 2048, 512], P('tp'), may hold values from -0.125 to 0.125
- expert_down: bfloat16 [8, 512, 2048], P('tp'), may hold values from -0.25 to 0.25
- shared_gate: bfloat16 [2048, 256], replicated, may hold values from -0.125 to 0.125
- shared_up: bfloat16 [2048, 256], replicated, may hold values from -0.125 to 0.125
- shared_down: bfloat16 [256, 2048], replicated, may hold values from -0.375 to 0.375
Outputs:
- mixed: bfloat16 [4096, 2048], P(('ep', 'tp'))
- load: float32 [8], replicated
Inputs may be any that keep to these rules, and one draw needn't show every extreme that they name: `routes`: each row names 2 different experts. Among the rows of one device no expert is named by more than 64 rows, and in every draw some expert is named by exactly 64 rows of some device.
All inputs are finite; a program needn't handle non-finite values.
Results may differ from a plain program's by a relative error of at most 0.002.
The roundings to bfloat16 on the way count: a program that leaves them out, or rounds other values in their place, can miss the bound.
Values may be sent and summed in bfloat16 or wider, within the bound.
No kernel may reach another device: no remote copies, remote signals or barrier semaphores. Data moves between devices by JAX's collectives and lax.ppermute only.
A program may use at most 64 MiB of HBM per device.

v0:
```python
import jax
import jax.numpy as jnp
from jax import lax
from jax.sharding import PartitionSpec as P


def layer_normed(token_block, norm_gain):
    values = token_block.astype(jnp.float32)
    center = jnp.mean(values, axis=-1, keepdims=True)
    spread = jnp.mean(jnp.square(values - center), axis=-1, keepdims=True)
    return ((values - center) * lax.rsqrt(spread + 1e-05) * norm_gain).astype(jnp.bfloat16)


def gated_mlp(row_block, w_gate, w_up, w_down):
    gate_part = jnp.dot(row_block, w_gate, preferred_element_type=jnp.float32)
    up_part = jnp.dot(row_block, w_up, preferred_element_type=jnp.float32)
    hidden = (jax.nn.silu(gate_part) * up_part).astype(jnp.bfloat16)
    return jnp.dot(hidden, w_down, preferred_element_type=jnp.float32)


def per_device(
    tokens,
    norm_gain,
    routes,
    gates,
    expert_gate,
    expert_up,
    expert_down,
    shared_gate,
    shared_up,
    shared_down,
):
    normed = layer_normed(tokens, norm_gain)
    count_rows, feature_count = normed.shape
    top_count = routes.shape[1]
    groups = lax.axis_size("tp")
    devices = lax.axis_size("ep") * groups
    capacity = 2 * count_rows * top_count // groups
    flat_expert = routes.reshape(-1)
    onehot = (flat_expert[:, None] == jnp.arange(groups, dtype=jnp.int32)[None, :]).astype(
        jnp.int32
    )
    earlier = jnp.cumsum(onehot, axis=0) - onehot
    slot_index = jnp.sum(earlier * onehot, axis=1)
    destination = flat_expert * capacity + slot_index
    local_counts = jnp.sum(onehot, axis=0).astype(jnp.float32)
    copies = jnp.repeat(normed, top_count, axis=0)
    outgoing = (
        jnp.zeros((groups * capacity, feature_count), jnp.bfloat16).at[destination].set(copies)
    )
    outgoing = outgoing.reshape(groups, capacity, feature_count)
    arrived = lax.all_to_all(outgoing, "tp", split_axis=0, concat_axis=0, tiled=True)
    sources, slot_count, _ = arrived.shape
    result = gated_mlp(
        arrived.reshape(sources * slot_count, feature_count),
        expert_gate[0],
        expert_up[0],
        expert_down[0],
    )
    result = result.astype(jnp.bfloat16).reshape(sources, slot_count, feature_count)
    returned = lax.all_to_all(result, "tp", split_axis=0, concat_axis=0, tiled=True)
    flat_returned = returned.reshape(groups * capacity, feature_count)
    per_copy = flat_returned[destination].reshape(count_rows, top_count, feature_count)
    routed = jnp.sum(gates[:, :, None] * per_copy.astype(jnp.float32), axis=1)
    shared_out = gated_mlp(normed, shared_gate, shared_up, shared_down)
    mixed = (routed + shared_out).astype(jnp.bfloat16)
    total_counts = lax.psum(local_counts, ("ep", "tp"))
    load = total_counts * (groups / (count_rows * top_count * devices))
    return (mixed, load)


def solution(mesh):
    placed = (
        P(("ep", "tp"), None),
        P(),
        P(("ep", "tp"), None),
        P(("ep", "tp"), None),
        P("tp", None, None),
        P("tp", None, None),
        P("tp", None, None),
        P(),
        P(),
        P(),
    )
    return jax.shard_map(
        per_device,
        mesh=mesh,
        in_specs=placed,
        out_specs=(P(("ep", "tp"), None), P()),
        check_vma=False,
    )
```

profile of v0, /device:TPU:0, one launch (start us, length us, event | category | flops | bytes accessed | tf_op | source)
XLA Modules:
  0.0 142.1 jit_solution(17562173664722931788)
XLA Ops:
  0.6 0.0 copy-start
  0.6 0.9 copy.15
  1.6 0.1 eq.29
  1.7 0.1 eq.25
  1.9 0.7 broadcast_multiply_fusion
  2.6 0.6 reduce-window.6
  3.1 0.2 slice_reduce_fusion
  3.4 0.1 copy.14
  3.5 0.1 mul.63
  3.6 1.2 convert_reduce_fusion
  4.8 1.3 fusion.15
  6.2 1.4 fusion.17
  7.6 1.6 %broadcast_in_dim.5 = bf16[128,2,2048]{2,1,0:T(2,128)(2,1)} broadcast(bf16[128,2048]{1,0:T(8,128)(2,1)S(1)} %fusion.17), dimensions={0,2} | broadcast | bytes 1572864 | tf_op jit(solution)/shard_map/broadcast_in_dim | solution.py:47
  9.2 2.3 %reshape.101 = bf16[256,2048]{1,0:T(8,128)(2,1)} reshape(bf16[128,2,2048]{2,1,0:T(2,128)(2,1)} %broadcast_in_dim.5) | data formatting | bytes 2097152 | tf_op jit(solution)/shard_map/reshape | solution.py:47
  11.5 0.1 convert_reduce_fusion.1
  11.6 4.4 %scatter_custom_fusion = bf16[512,2048]{1,0:T(8,128)(2,1)} fusion(s32[256]{0:T(256)S(1)} %bitcast.36, bf16[256,2048]{1,0:T(8,128)(2,1)} %reshape.101, bf16[]{:T(256)} %constant.9.clone.1), kind=kCustom, calls=%fused_computation.22 | custom fusion | bytes 2097664 | tf_op jit(solution)/shard_map/scatter | solution.py:49
  16.1 0.0 copy-start.3
  16.1 31.9 %all_to_all.10 = bf16[8,64,2048]{2,1,0:T(8,128)(2,1)S(1)} all-to-all(bf16[8,64,2048]{2,1,0:T(8,128)(2,1)} %bitcast.32), channel_id=1, replica_groups=mesh['ep'=4,'tp'=8] {'tp'}, dimensions={0} | all-to-all | bytes 4194304 | tf_op jit(solution)/shard_map/all_to_all | solution.py:52
  48.0 0.0 copy-start.1
  48.0 1.3 copy-done.1
  49.3 0.0 copy-done.3
  49.3 2.2 %fusion.4 = f32[512,512]{1,0:T(8,128)} fusion(bf16[512,2048]{1,0:T(8,128)(2,1)S(1)} %bitcast.34, bf16[1,2048,512]{2,1,0:T(8,128)(2,1)S(1)} %copy-done.3), kind=kOutput, calls=%fused_computation.8 | convolution fusion | flops 1073741824 | bytes 5242880 | tf_op jit(solution)/shard_map/dot_general | solution.py:15
  51.5 0.0 copy-done
  51.5 6.3 %convolution_convert_fusion = bf16[512,2048]{1,0:T(8,128)(2,1)} fusion(bf16[1,512,2048]{2,1,0:T(8,128)(2,1)S(1)} %copy-done, bf16[512,2048]{1,0:T(8,128)(2,1)} %bitcast.35, bf16[1,2048,512]{2,1,0:T(8,128)(2,1)} %param.15, f32[512,512]{1,0:T(8,128)} %fusion.4), kind=kOutput, calls=%fused_computation.2 | convolution fusion | flops 2150105088 | bytes 9437184 | tf_op jit(solution)/shard_map/dot_general | solution.py:18
  57.8 0.0 copy-start.2
  57.8 4.5 %all-to-all-start.1 = ((bf16[8,64,2048]{2,1,0:T(8,128)(2,1)}), bf16[8,64,2048]{2,1,0:T(8,128)(2,1)}, u32[]{:S(2)}, u32[]{:S(2)}) async-start(bf16[8,64,2048]{2,1,0:T(8,128)(2,1)} %bitcast.33), calls=%async_computation.1 | async-start | bytes 4194304 | tf_op jit(solution)/shard_map/all_to_all | solution.py:61
  62.3 59.9 %psum.7 = f32[8]{0:T(128)S(1)} all-reduce(f32[8]{0:T(128)S(1)} %convert_element_type.44), channel_id=1, replica_groups=mesh['ep'=4,'tp'=8] {'ep','tp'}, use_global_device_ids=true, to_apply=%region_8.9 | all-reduce | flops 8 | bytes 64 | tf_op jit(solution)/shard_map/psum | solution.py:67
  122.2 0.0 copy-done.2
  122.2 0.1 copy.13
  122.3 0.5 broadcast_multiply_fusion.1
  122.8 1.5 %fusion.34 = f32[128,256]{1,0:T(8,128)S(1)} fusion(bf16[128,2048]{1,0:T(8,128)(2,1)S(1)} %fusion.17, bf16[2048,256]{1,0:T(8,128)(2,1)} %param.17), kind=kOutput, calls=%fused_computation.47 | convolution fusion | flops 134217728 | bytes 1703936 | tf_op jit(solution)/shard_map/dot_general | solution.py:15
  124.4 0.0 all-to-all-done.1
  124.4 5.2 %gather_fusion = bf16[256,2048]{1,0:T(8,128)(2,1)} fusion(bf16[512,2048]{1,0:T(8,128)(2,1)} %bitcast.10, s32[1024]{0:T(1024)S(1)} %pad_clamp_fusion), kind=kCustom, calls=%fused_computation | custom fusion | bytes 2098176 | tf_op jit(solution)/shard_map/gather | solution.py:63
  129.6 3.4 %reshape.88 = f32[128,2,2048]{2,1,0:T(2,128)} reshape(bf16[256,2048]{1,0:T(8,128)(2,1)} %gather_fusion) | data formatting | bytes 3145728 | tf_op jit(solution)/shard_map/convert_element_type | solution.py:64
  133.0 5.7 %multiply_reduce_fusion = f32[128,2048]{1,0:T(8,128)} fusion(f32[128,2,2048]{2,1,0:T(2,128)} %reshape.88, f32[128,2]{1,0:T(8,128)S(1)} %copy.13), kind=kLoop, calls=%fused_computation.10 | loop fusion | flops 786432 | bytes 3146752 | tf_op jit(solution)/shard_map/reduce_sum | solution.py:64
  138.7 3.4 %fusion = bf16[128,2048]{1,0:T(8,128)(2,1)} fusion(f32[128,2048]{1,0:T(8,128)} %multiply_reduce_fusion, bf16[256,2048]{1,0:T(8,128)(2,1)} %param.19, bf16[128,2048]{1,0:T(8,128)(2,1)S(1)} %fusion.17, bf16[2048,256]{1,0:T(8,128)(2,1)} %param.18, f32[128,256]{1,0:T(8,128)S(1)} %fusion.34), kind=kOutput, calls=%fused_computation.4 | convolution fusion | flops 269156352 | bytes 4325376 | tf_op jit(solution)/shard_map/dot_general | solution.py:18
  (8 shorter events, 0.1 us)
Async XLA Ops:
  0.6 50.9 %copy-start = (bf16[1,512,2048]{2,1,0:T(8,128)(2,1)S(1)}, bf16[1,512,2048]{2,1,0:T(8,128)(2,1)}, u32[]{:S(2)}) copy-start(bf16[1,512,2048]{2,1,0:T(8,128)(2,1)} %param.16) | copy-start | bytes 6291460
  16.1 33.2 %copy-start.3 = (bf16[1,2048,512]{2,1,0:T(8,128)(2,1)S(1)}, bf16[1,2048,512]{2,1,0:T(8,128)(2,1)}, u32[]{:S(2)}) copy-start(bf16[1,2048,512]{2,1,0:T(8,128)(2,1)} %param.14) | copy-start | bytes 6291460
  48.0 1.3 copy-start.1
  57.8 64.4 %copy-start.2 = (f32[128,2]{0,1:T(2,128)S(1)}, f32[128,2]{0,1:T(2,128)}, u32[]{:S(2)}) copy-start(f32[128,2]{0,1:T(2,128)} %param.13) | copy-start | bytes 3076
  57.8 66.6 %all-to-all-start.1 = ((bf16[8,64,2048]{2,1,0:T(8,128)(2,1)}), bf16[8,64,2048]{2,1,0:T(8,128)(2,1)}, u32[]{:S(2)}, u32[]{:S(2)}) async-start(bf16[8,64,2048]{2,1,0:T(8,128)(2,1)} %bitcast.33), calls=%async_computation.1 | async-start | bytes 4194304 | tf_op jit(solution)/shard_map/all_to_all | solution.py:61
where the time goes:
time: 143 us; the launch traced here: 142 us
  blocking collectives  91.8 us (64%)
  local copies, waits for them, and re-layouts  20 us (14%)
  matrix products  13.5 us (9%)
  other arithmetic  11.6 us (8%)
  starting transfers between devices  4.5 us (3%)
    psum x1, blocking collectives, per_device(): total_counts = lax.psum(local_counts, ('ep', 'tp'))  59.9 us
    all_to_all x1, blocking collectives, per_device(): lax.all_to_all(outgoing, 'tp', split_axis=0, concat_axis=0, tiled=True)  31.9 us
    dot_general x2, matrix products, gated_mlp(): return jnp.dot(hidden, w_down, preferred_element_type=jnp.float32)  9.71 us
    reduce_sum x1, other arithmetic, per_device(): routed = jnp.sum(gates[:, :, None] * per_copy.astype(jnp.float32), axis=1)  5.72 us
    gather x1, local copies, waits for them, and re-layouts, per_device(): flat_returned[destination].reshape(count_rows, top_count, feature_count)  5.2 us
    all_to_all x1, starting transfers between devices, per_device(): lax.all_to_all(result, 'tp', split_axis=0, concat_axis=0, tiled=True)  4.5 us
    scatter x1, local copies, waits for them, and re-layouts, per_device(): jnp.zeros((groups * capacity, feature_count), jnp.bfloat16).at[destination]  4.44 us
    dot_general x2, matrix products, gated_mlp(): gate_part = jnp.dot(row_block, w_gate, preferred_element_type=jnp.float32)  3.76 us
  transfers between devices with their start and end apart: 1, of which 0 were waited for; matrix products, arithmetic and copies ran while one was open for 2% of the time, Pallas kernels for 0%

commit v1 on v0

v1 whole, which is shorter than its diff:
```python
import functools

import jax
import jax.numpy as jnp
import numpy as np
from jax import lax
from jax.experimental import pallas as pl
from jax.experimental.pallas import tpu as pltpu
from jax.sharding import PartitionSpec as P

LANES = 128
HBM = pl.BlockSpec(memory_space=pl.ANY)
VMEM = pl.BlockSpec(memory_space=pltpu.VMEM)
SMEM = pl.BlockSpec(memory_space=pltpu.SMEM)
F32 = jnp.float32
BF16 = jnp.bfloat16


def dot(a, b, contract=((1,), (0,))):
    return lax.dot_general(a, b, (contract, ((), ())), preferred_element_type=F32)


def layer_normed(values, gain):
    center = jnp.mean(values, axis=-1, keepdims=True)
    moved = values - center
    spread = jnp.mean(moved * moved, axis=-1, keepdims=True)
    return (moved * lax.rsqrt(spread + 1e-05) * gain).astype(BF16)


def silu(v):
    return v / (1.0 + jnp.exp(-v))


def places(meta, expert, slots):
    rows = meta.shape[0]
    named = ((meta[:, 0:1] == expert) | (meta[:, 1:2] == expert)).astype(F32)
    row = lax.broadcasted_iota(jnp.int32, (rows, rows), 0)
    col = lax.broadcasted_iota(jnp.int32, (rows, rows), 1)
    before = (col < row).astype(F32).astype(BF16)
    rank = dot(before, jnp.broadcast_to(named, (rows, LANES)).astype(BF16))[:, :slots]
    slot = lax.broadcasted_iota(jnp.int32, (rows, slots), 1).astype(F32)
    return jnp.where(rank == slot, named, 0.0).astype(BF16)


def expert_kernel(count, slots, me_ref, gain_ref, *refs):
    blocks = refs[:count]
    wg_hbm, wu_hbm, wd_hbm = refs[count : count + 3]
    outs = refs[count + 3 : 2 * count + 3]
    tally_ref = refs[2 * count + 3]
    normed, wg, wu, wd, sems = refs[2 * count + 4 :]
    width = gain_ref.shape[1]
    loads = [
        pltpu.make_async_copy(src.at[0], dst, sems.at[i])
        for i, (src, dst) in enumerate(((wg_hbm, wg), (wu_hbm, wu), (wd_hbm, wd)))
    ]
    for load in loads:
        load.start()
    expert = me_ref[0].astype(F32)
    tally = jnp.zeros(tally_ref.shape, F32)
    for i, block in enumerate(blocks):
        meta = block[:, width:].astype(F32)
        tally = tally + meta[0:8]
        chosen = dot(places(meta, expert, slots), block[:, :width], ((0,), (0,)))
        normed[i * slots : (i + 1) * slots, :] = layer_normed(chosen, gain_ref[...])
    tally_ref[...] = tally
    loads[0].wait()
    gate = dot(normed[...], wg[...])
    loads[1].wait()
    up = dot(normed[...], wu[...])
    hidden = (silu(gate) * up).astype(BF16)
    loads[2].wait()
    result = dot(hidden, wd[...]).astype(BF16)
    for i, out in enumerate(outs):
        out[...] = result[i * slots : (i + 1) * slots]


def expert_call(me, gain, blocks, slots, wg, wu, wd):
    count = len(blocks)
    width, units = wg.shape[1:]
    return pl.pallas_call(
        functools.partial(expert_kernel, count, slots),
        out_shape=[jax.ShapeDtypeStruct((slots, width), BF16)] * count
        + [jax.ShapeDtypeStruct((8, LANES), F32)],
        in_specs=[SMEM, VMEM] + [VMEM] * count + [HBM] * 3,
        out_specs=[VMEM] * (count + 1),
        scratch_shapes=[
            pltpu.VMEM((count * slots, width), BF16),
            pltpu.VMEM((width, units), BF16),
            pltpu.VMEM((width, units), BF16),
            pltpu.VMEM((units, width), BF16),
            pltpu.SemaphoreType.DMA((3,)),
        ],
        compiler_params=pltpu.CompilerParams(vmem_limit_bytes=40 * 2**20),
        cost_estimate=pl.CostEstimate(
            flops=6 * count * slots * width * units, bytes_accessed=6 * width * units, transcendentals=0
        ),
        name="expert_rows",
    )(me, gain, *blocks, wg, wu, wd)


def shared_kernel(tokens_ref, gain_ref, wg_ref, wu_ref, wd_ref, out_ref):
    normed = layer_normed(tokens_ref[...].astype(F32), gain_ref[...])
    hidden = (silu(dot(normed, wg_ref[...])) * dot(normed, wu_ref[...])).astype(BF16)
    out_ref[...] = dot(hidden, wd_ref[...])


def combine_kernel(count, experts_ref, meta_ref, gates_ref, base_ref, *refs):
    blocks, out_ref = refs[:count], refs[count]
    meta = meta_ref[...].astype(F32)
    total = base_ref[...]
    for i, block in enumerate(blocks):
        expert = experts_ref[i].astype(F32)
        gate = jnp.where(meta[:, 0:1] == expert, gates_ref[:, 0:1], gates_ref[:, 1:2])
        total = total + gate * dot(places(meta, expert, block.shape[0]), block[...])
    out_ref[...] = total.astype(out_ref.dtype)


def combine_call(experts, meta, gates, base, blocks, kind):
    return pl.pallas_call(
        functools.partial(combine_kernel, len(blocks)),
        out_shape=jax.ShapeDtypeStruct(base.shape, kind),
        in_specs=[SMEM] + [VMEM] * (3 + len(blocks)),
        out_specs=VMEM,
        compiler_params=pltpu.CompilerParams(vmem_limit_bytes=24 * 2**20),
        name="combine_rows",
    )(experts, meta, gates, base, *blocks)


def per_device(
    tokens,
    norm_gain,
    routes,
    gates,
    expert_gate,
    expert_up,
    expert_down,
    shared_gate,
    shared_up,
    shared_down,
):
    rows, width = tokens.shape
    top = routes.shape[1]
    groups, planes = lax.axis_size("tp"), lax.axis_size("ep")
    slots = 2 * rows * top // groups
    me = lax.axis_index("tp")
    ids = np.arange(groups)

    def send(value, perm):
        return lax.ppermute(value, "tp", [(int(i), int(perm[i])) for i in ids])

    onehot = (routes.reshape(-1)[:, None] == jnp.arange(groups)[None, :]).astype(F32)
    counts = jnp.sum(onehot, axis=0)
    meta = jnp.concatenate(
        [routes.astype(F32), jnp.broadcast_to(counts[None, :], (rows, groups))], axis=1
    )
    meta = jnp.pad(meta, ((0, 0), (0, LANES - meta.shape[1]))).astype(BF16)
    packed = jnp.concatenate([tokens, meta], axis=1)
    gain = norm_gain.reshape(1, width)

    masks = [1 << b for b in range(1, groups.bit_length() - 1)]
    stages = [[(packed, ids)]]
    known = [(packed, ids)]
    for step in range(len(masks)):
        hop = np.where(ids % 2 == 0, ids ^ masks[step], ids ^ masks[-1 - step])
        fresh = [(send(block, hop), origin[hop]) for block, origin in known]
        known = known + fresh
        if step == 0:
            stages.append(fresh)
        else:
            stages[-1].append(fresh[0])
            stages.append(fresh[1:])
    partner = ids ^ 1
    stages = [
        stage + [(send(block, partner), origin[partner]) for block, origin in stage]
        for stage in stages
    ]

    base = pl.pallas_call(
        shared_kernel,
        out_shape=jax.ShapeDtypeStruct((rows, width), F32),
        in_specs=[VMEM] * 5,
        out_specs=VMEM,
        compiler_params=pltpu.CompilerParams(vmem_limit_bytes=24 * 2**20),
        name="shared_rows",
    )(tokens, gain, shared_gate, shared_up, shared_down)

    mine = me.reshape(1).astype(jnp.int32)
    tally = jnp.zeros((8, LANES), F32)
    returned = []
    for stage in stages:
        *results, part = expert_call(
            mine, gain, [b for b, _ in stage], slots, expert_gate, expert_up, expert_down
        )
        tally = tally + part
        back = []
        for (_, origin), result in zip(stage, results):
            if np.array_equal(origin, ids):
                back.append((result, ids))
            else:
                back.append((send(result, origin), np.argsort(origin)))
        returned.append(back)

    early = [item for back in returned[:-1] for item in back]
    for blocks, kind in ((early, F32), (returned[-1], BF16)):
        experts = jnp.stack([jnp.asarray(origin, jnp.int32)[me] for _, origin in blocks])
        base = combine_call(experts, meta, gates, base, [b for b, _ in blocks], kind)

    total = tally[0:1]
    if planes & (planes - 1):
        total = lax.psum(total, "ep")
    else:
        for bit in range(planes.bit_length() - 1):
            total = total + lax.ppermute(total, "ep", [(i, i ^ (1 << bit)) for i in range(planes)])
    load = total[0, top : top + groups] * (groups / (rows * top * planes * groups))
    return base, load


def solution(mesh):
    placed = (
        P(("ep", "tp"), None),
        P(),
        P(("ep", "tp"), None),
        P(("ep", "tp"), None),
        P("tp", None, None),
        P("tp", None, None),
        P("tp", None, None),
        P(),
        P(),
        P(),
    )
    return jax.shard_map(
        per_device,
        mesh=mesh,
        in_specs=placed,
        out_specs=(P(("ep", "tp"), None), P()),
        check_vma=False,
    )
```

time: 143 us -> 88.9 us (0.62)
  blocking collectives: 91.8 us -> 0 us
  Pallas kernels: 0 us -> 20.9 us
  waiting for transfers between devices: 0.01 us -> 18.9 us
  matrix products: 13.5 us -> 0 us
  starting transfers between devices: 4.5 us -> 18 us
  other arithmetic: 11.6 us -> 3.83 us
  local copies, waits for them, and re-layouts: 20 us -> 25.1 us
    psum x1 -> x0, blocking collectives: 59.9 us -> none  [per_device(): total_counts = lax.psum(local_counts, ('ep', 'tp'))]
    all_to_all x1 -> x0, blocking collectives: 31.9 us -> none  [per_device(): lax.all_to_all(outgoing, 'tp', split_axis=0, concat_axis=0, tiled=True)]
    pallas_call x0 -> x6, Pallas kernels: none -> 20.9 us  [the longest x3 14.2 us: expert_call(): pl.pallas_call(functools.partial(expert_kernel, count, slots), out_shape=...]
    ppermute x0 -> x16, waiting for transfers between devices: none -> 18.9 us  [the longest x14 18.9 us: send(): return lax.ppermute(value, 'tp', [(int(i), int(perm[i])) for i in ids])]
    ppermute x0 -> x16, starting transfers between devices: none -> 18 us  [the longest x14 13.9 us: send(): return lax.ppermute(value, 'tp', [(int(i), int(perm[i])) for i in ids])]
    dot_general x4 -> x0, matrix products: 13.5 us -> none  [the longest x2 9.71 us: gated_mlp(): return jnp.dot(hidden, w_down, preferred_element_type=jnp.float32)]
    unnamed x10 -> x50, local copies, waits for them, and re-layouts: 2.36 us -> 14.7 us
    reduce_sum x4 -> x1, other arithmetic: 8.39 us -> 0.12 us  [per_device(): counts = jnp.sum(onehot, axis=0)]
  transfers between devices with their start and end apart: 1 -> 16, of which waited for: 0 -> 2; matrix products, arithmetic and copies ran while one was open for 2% -> 14% of each run, Pallas kernels for 0% -> 21%
where the time goes in v1:
time: 88.9 us; the launch traced here: 87.6 us
  local copies, waits for them, and re-layouts  25.1 us (28%)
  Pallas kernels  20.9 us (24%)
  waiting for transfers between devices  18.9 us (21%)
  starting transfers between devices  18 us (20%)
  other arithmetic  3.83 us (4%)
    ppermute x14, waiting for transfers between devices, send(): return lax.ppermute(value, 'tp', [(int(i), int(perm[i])) for i in ids])  18.9 us
    unnamed x50, local copies, waits for them, and re-layouts  14.7 us
    pallas_call x3, Pallas kernels, expert_call(): pl.pallas_call(functools.partial(expert_kernel, count, slots), out_shape=...  14.2 us
    ppermute x14, starting transfers between devices, send(): return lax.ppermute(value, 'tp', [(int(i), int(perm[i])) for i in ids])  13.9 us
    dynamic_slice x7, local copies, waits for them, and re-layouts, per_device(): jnp.asarray(origin, jnp.int32)[me]  6.81 us
    pallas_call x2, Pallas kernels, combine_call(): pl.pallas_call(functools.partial(combine_kernel, len(blocks)), out_shape=...  5.71 us
    ppermute x2, starting transfers between devices, per_device(): lax.ppermute(total, 'ep', [(i, i ^ 1 << bit) for i in range(planes)])  4.17 us
    another operation x1, local copies, waits for them, and re-layouts, per_device(): jnp.stack([jnp.asarray(origin, jnp.int32)[me] for _, origin in blocks])  3.2 us
  transfers between devices with their start and end apart: 16, of which 2 were waited for; matrix products, arithmetic and copies ran while one was open for 14% of the time, Pallas kernels for 21%

profile of v1, /device:TPU:0, one launch (start us, length us, event | category | flops | bytes accessed | tf_op | source)
XLA Modules:
  0.0 87.6 jit_solution(5173989060739557125)
XLA Ops:
  0.6 0.8 copy.31
  1.4 0.7 convert_convert_fusion
  2.5 0.1 copy.32
  2.7 1.1 %pad_maximum_fusion.refs_0_ = bf16[128,2176]{1,0:T(8,128)(2,1)S(1)} fusion(bf16[128,128]{1,0:T(8,128)(2,1)S(1)} %pad.5.meta_ref, bf16[128,2048]{1,0:T(8,128)(2,1)} %tokens_ref.1), kind=kLoop, calls=%fused_computation | loop fusion | flops 1114112 | bytes 1114112 | tf_op jit(solution)/shard_map/concatenate | solution.py:157
  3.8 3.0 %collective-permute-start.2 = (bf16[128,2176]{1,0:T(8,128)(2,1)S(1)}, bf16[128,2176]{1,0:T(8,128)(2,1)S(1)}, u32[]{:S(2)}, u32[]{:S(2)}) collective-permute-start(bf16[128,2176]{1,0:T(8,128)(2,1)S(1)} %pad_maximum_fusion.refs_0_), channel_id=1, source_target_pairs={{0,2},{1,5},{2,0},{3,7},{4,6},{5,1},{6,4},{7,3},{8,10},{9,13},{10,... | collective-permute-start | bytes 1671176 | tf_op jit(solution)/shard_map/ppermute | solution.py:149
  6.8 1.5 %collective-permute-start.3 = (bf16[128,2176]{1,0:T(8,128)(2,1)S(1)}, bf16[128,2176]{1,0:T(8,128)(2,1)S(1)}, u32[]{:S(2)}, u32[]{:S(2)}) collective-permute-start(bf16[128,2176]{1,0:T(8,128)(2,1)S(1)} %pad_maximum_fusion.refs_0_), channel_id=1, source_target_pairs={{0,4},{1,3},{2,6},{3,1},{4,0},{5,7},{6,2},{7,5},{8,12},{9,11},{10,... | collective-permute-start | bytes 1671176 | tf_op jit(solution)/shard_map/ppermute | solution.py:149
  8.3 11.4 %collective-permute-done.2.refs_0_ = bf16[128,2176]{1,0:T(8,128)(2,1)S(1)} collective-permute-done((bf16[128,2176]{1,0:T(8,128)(2,1)S(1)}, bf16[128,2176]{1,0:T(8,128)(2,1)S(1)}, u32[]{:S(2)}, u32[]{:S(2)}) %collective-permute-start.2) | collective-permute-done | bytes 557088 | tf_op jit(solution)/shard_map/ppermute | solution.py:149
  19.7 1.6 %collective-permute-start.10 = (bf16[128,2176]{1,0:T(8,128)(2,1)S(1)}, bf16[128,2176]{1,0:T(8,128)(2,1)S(1)}, u32[]{:S(2)}, u32[]{:S(2)}) collective-permute-start(bf16[128,2176]{1,0:T(8,128)(2,1)S(1)} %collective-permute-done.2.refs_0_), channel_id=1, source_target_pairs={{0,4},{1,3},{2,6},{3,1},{4,0},{5,7},{6,2},{7,5},{8,12},{9,11},{10,... | collective-permute-start | bytes 1671176 | tf_op jit(solution)/shard_map/ppermute | solution.py:149
  21.3 0.5 collective-permute-start.4
  21.8 7.5 %collective-permute-done.10.refs_0_ = bf16[128,2176]{1,0:T(8,128)(2,1)S(1)} collective-permute-done((bf16[128,2176]{1,0:T(8,128)(2,1)S(1)}, bf16[128,2176]{1,0:T(8,128)(2,1)S(1)}, u32[]{:S(2)}, u32[]{:S(2)}) %collective-permute-start.10) | collective-permute-done | bytes 557088 | tf_op jit(solution)/shard_map/ppermute | solution.py:149
  29.2 1.3 %dynamic_slice.27 = s32[1]{0:T(128)} dynamic-slice(s32[8]{0:T(128)} %constant.31.clone, s32[]{:T(128)S(6)} %select_n.2), dynamic_slice_sizes={1} | dynamic-slice | bytes 12 | tf_op jit(solution)/shard_map/dynamic_slice | solution.py:205
  30.5 1.2 %dynamic_slice.28 = s32[1]{0:T(128)} dynamic-slice(s32[8]{0:T(128)} %constant.32.clone, s32[]{:T(128)S(6)} %select_n.2), dynamic_slice_sizes={1} | dynamic-slice | bytes 12 | tf_op jit(solution)/shard_map/dynamic_slice | solution.py:205
  31.8 1.2 %dynamic_slice.24 = s32[1]{0:T(128)} dynamic-slice(s32[8]{0:T(128)} %constant.36.clone, s32[]{:T(128)S(6)} %select_n.2), dynamic_slice_sizes={1} | dynamic-slice | bytes 12 | tf_op jit(solution)/shard_map/dynamic_slice | solution.py:205
  33.0 1.2 %dynamic_slice.25 = s32[1]{0:T(128)} dynamic-slice(s32[8]{0:T(128)} %constant.37.clone, s32[]{:T(128)S(6)} %select_n.2), dynamic_slice_sizes={1} | dynamic-slice | bytes 12 | tf_op jit(solution)/shard_map/dynamic_slice | solution.py:205
  34.2 1.3 %pad_add_fusion.experts_ref = s32[2]{0:T(128)S(1)} fusion(s32[1]{0:T(128)} %dynamic_slice.25, s32[1]{0:T(128)} %dynamic_slice.24), kind=kLoop, calls=%fused_computation.6 | loop fusion | flops 2 | bytes 16 | tf_op jit(solution)/shard_map/stack | solution.py:205
  35.5 1.6 %copy-done = bf16[1,2048,512]{2,1,0:T(8,128)(2,1)S(1)} copy-done((bf16[1,2048,512]{2,1,0:T(8,128)(2,1)S(1)}, bf16[1,2048,512]{2,1,0:T(8,128)(2,1)}, u32[]{:S(2)}) %copy-start) | copy-done | bytes 2097176
  37.1 1.6 %copy-done.2 = bf16[1,2048,512]{2,1,0:T(8,128)(2,1)S(1)} copy-done((bf16[1,2048,512]{2,1,0:T(8,128)(2,1)S(1)}, bf16[1,2048,512]{2,1,0:T(8,128)(2,1)}, u32[]{:S(2)}) %copy-start.2) | copy-done | bytes 2097176
  38.7 1.6 %copy-done.4 = bf16[1,512,2048]{2,1,0:T(8,128)(2,1)S(1)} copy-done((bf16[1,512,2048]{2,1,0:T(8,128)(2,1)S(1)}, bf16[1,512,2048]{2,1,0:T(8,128)(2,1)}, u32[]{:S(2)}) %copy-start.4) | copy-done | bytes 2097176
  40.3 0.7 copy-done.18
  41.0 4.1 %expert_rows.3 = (bf16[64,2048]{1,0:T(8,128)(2,1)S(1)}, bf16[64,2048]{1,0:T(8,128)(2,1)S(1)}, f32[8,128]{1,0:T(8,128)S(1)}) custom-call(s32[1]{0:T(128)} %bitcast.2.me_ref, f32[1,2048]{1,0:T(1,128)S(1)} %bitcast.5, bf16[128,2176]{1,0:T(8,128)(2,1)S(1)} %pad_maximum_fusion.refs_0_, bf16[128,2176]{1,0:T(8,128)(2,1)} %collective-permute-done.refs_1_, ...), custom_call_target="tpu_custom_call" | custom-call | flops 805306368 | bytes 6291456 | tf_op jit(solution)/shard_map/expert_rows/pallas_call | solution.py:80
  45.1 0.6 collective-permute-start.1
  45.7 6.4 %expert_rows.4 = (bf16[64,2048]{1,0:T(8,128)(2,1)}, bf16[64,2048]{1,0:T(8,128)(2,1)}, bf16[64,2048]{1,0:T(8,128)(2,1)}, bf16[64,2048]{1,0:T(8,128)(2,1)}, f32[8,128]{1,0:T(8,128)S(1)}) custom-call(s32[1]{0:T(128)} %bitcast.2.me_ref, f32[1,2048]{1,0:T(1,128)S(1)} %bitcast.6, bf16[128,2176]{1,0:T(8,128)(2,1)S(1)} %collective-permute-done.2.refs_0_, ...), custom_call_target="tpu_custom_call" | custom-call | flops 1610612736 | bytes 6291456 | tf_op jit(solution)/shard_map/expert_rows/pallas_call | solution.py:80
  52.1 2.5 %collective-permute-start.6 = (bf16[64,2048]{1,0:T(8,128)(2,1)}, bf16[64,2048]{1,0:T(8,128)(2,1)S(1)}, u32[]{:S(2)}, u32[]{:S(2)}) collective-permute-start(bf16[64,2048]{1,0:T(8,128)(2,1)} %get-tuple-element.15), channel_id=1, source_target_pairs={{0,2},{1,5},{2,0},{3,7},{4,6},{5,1},{6,4},{7,3},{8,10},{9,13},{10,... | collective-permute-start | bytes 786440 | tf_op jit(solution)/shard_map/ppermute | solution.py:149
  54.7 0.7 collective-permute-start.7
  55.4 0.4 collective-permute-start.8
  55.8 0.8 copy-done.10
  56.6 1.4 %collective-permute-start.9 = (bf16[64,2048]{1,0:T(8,128)(2,1)}, bf16[64,2048]{1,0:T(8,128)(2,1)}, u32[]{:S(2)}, u32[]{:S(2)}) collective-permute-start(bf16[64,2048]{1,0:T(8,128)(2,1)} %get-tuple-element.18), channel_id=1, source_target_pairs={{0,3},{1,4},{2,1},{3,6},{4,7},{5,0},{6,5},{7,2},{8,11},{9,12},{10,... | collective-permute-start | bytes 786440 | tf_op jit(solution)/shard_map/ppermute | solution.py:149
  58.0 1.1 %copy-done.11 = bf16[128,2176]{1,0:T(8,128)(2,1)S(1)} copy-done((bf16[128,2176]{1,0:T(8,128)(2,1)S(1)}, bf16[128,2176]{1,0:T(8,128)(2,1)}, u32[]{:S(2)}) %copy-start.11) | copy-done | bytes 557080
  59.0 3.7 %expert_rows.5 = (bf16[64,2048]{1,0:T(8,128)(2,1)}, bf16[64,2048]{1,0:T(8,128)(2,1)}, f32[8,128]{1,0:T(8,128)S(1)}) custom-call(s32[1]{0:T(128)} %bitcast.2.me_ref, f32[1,2048]{1,0:T(1,128)S(1)} %bitcast.7, bf16[128,2176]{1,0:T(8,128)(2,1)S(1)} %collective-permute-done.10.refs_0_, bf16[128,2176]{1,0:T(8,128)(2,1)S(1)} %copy-done.11, ...), custom_call_target="tpu_custom_call" | custom-call | flops 805306368 | bytes 6291456 | tf_op jit(solution)/shard_map/expert_rows/pallas_call | solution.py:80
  62.7 0.7 copy-done.12
  63.4 1.6 %collective-permute-start.14 = (f32[1,128]{1,0:T(1,128)S(1)}, f32[1,128]{1,0:T(1,128)S(1)}, u32[]{:S(2)}, u32[]{:S(2)}) collective-permute-start(f32[1,128]{1,0:T(1,128)S(1)} %slice.6), channel_id=1, source_target_pairs={{0,8},{8,0},{16,24},{24,16},{1,9},{9,1},{17,25},{25,17},{2,10},{10... | collective-permute-start | bytes 1544 | tf_op jit(solution)/shard_map/ppermute | solution.py:213
  65.0 0.6 dynamic_slice.29
  65.6 0.6 dynamic_slice.30
  66.2 0.6 dynamic_slice.31
  67.0 0.7 copy-done.14
  67.7 1.3 %collective-permute-start.12 = (bf16[64,2048]{1,0:T(8,128)(2,1)}, bf16[64,2048]{1,0:T(8,128)(2,1)}, u32[]{:S(2)}, u32[]{:S(2)}) collective-permute-start(bf16[64,2048]{1,0:T(8,128)(2,1)} %get-tuple-element.19), channel_id=1, source_target_pairs={{0,6},{1,7},{2,4},{3,5},{4,2},{5,3},{6,0},{7,1},{8,14},{9,15},{10,... | collective-permute-start | bytes 786440 | tf_op jit(solution)/shard_map/ppermute | solution.py:149
  69.0 0.4 collective-permute-start.13
  69.4 0.7 copy-done.16
  70.1 2.6 %collective-permute-start.15 = (f32[1,128]{1,0:T(1,128)S(1)}, f32[1,128]{1,0:T(1,128)S(1)}, u32[]{:S(2)}, u32[]{:S(2)}) collective-permute-start(f32[1,128]{1,0:T(1,128)S(1)} %slice_add_fusion), channel_id=1, source_target_pairs={{0,16},{8,24},{16,0},{24,8},{1,17},{9,25},{17,1},{25,9},{2,18},{10... | collective-permute-start | bytes 1544 | tf_op jit(solution)/shard_map/ppermute | solution.py:213
  72.7 1.2 %copy-done.8 = bf16[2048,256]{1,0:T(8,128)(2,1)S(1)} copy-done((bf16[2048,256]{1,0:T(8,128)(2,1)S(1)}, bf16[2048,256]{1,0:T(8,128)(2,1)}, u32[]{:S(2)}) %copy-start.8) | copy-done | bytes 1048600
  73.9 1.2 %copy-done.9 = bf16[256,2048]{1,0:T(8,128)(2,1)S(1)} copy-done((bf16[256,2048]{1,0:T(8,128)(2,1)S(1)}, bf16[256,2048]{1,0:T(8,128)(2,1)}, u32[]{:S(2)}) %copy-start.9) | copy-done | bytes 1048600
  75.1 1.0 %shared_rows.1.base_ref = f32[128,2048]{1,0:T(8,128)S(1)} custom-call(bf16[128,2048]{1,0:T(8,128)(2,1)S(1)} %copy-done.6, f32[1,2048]{1,0:T(1,128)S(1)} %bitcast.8, bf16[2048,256]{1,0:T(8,128)(2,1)S(1)} %copy-done.7, bf16[2048,256]{1,0:T(8,128)(2,1)S(1)} %copy-done.8, bf16[256,2048]{1,0:T(8,128)(2,1)S(1)} %copy-done.9), custom_call_target="tpu_custom_call" | custom-call | tf_op jit(solution)/shard_map/shared_rows/pallas_call | solution.py:178
  76.1 3.2 %stack.7.experts_ref = s32[6]{0:T(128)S(1)} concatenate(s32[1]{0:T(128)} %bitcast, s32[1]{0:T(128)} %dynamic_slice.27, s32[1]{0:T(128)} %dynamic_slice.28, s32[1]{0:T(128)} %dynamic_slice.29, s32[1]{0:T(128)} %dynamic_slice.30, s32[1]{0:T(128)} %dynamic_slice.31), dimensions={0} | concatenate | bytes 48 | tf_op jit(solution)/shard_map/stack | solution.py:205
  79.4 0.9 %copy-done.15 = bf16[64,2048]{1,0:T(8,128)(2,1)S(1)} copy-done((bf16[64,2048]{1,0:T(8,128)(2,1)S(1)}, bf16[64,2048]{1,0:T(8,128)(2,1)}, u32[]{:S(2)}) %copy-start.15) | copy-done | bytes 262168
  80.3 0.9 %copy-done.17 = bf16[64,2048]{1,0:T(8,128)(2,1)S(1)} copy-done((bf16[64,2048]{1,0:T(8,128)(2,1)S(1)}, bf16[64,2048]{1,0:T(8,128)(2,1)}, u32[]{:S(2)}) %copy-start.17) | copy-done | bytes 262168
  81.2 3.0 %combine_rows.2.base_ref = f32[128,2048]{1,0:T(8,128)S(1)} custom-call(s32[6]{0:T(128)S(1)} %stack.7.experts_ref, bf16[128,128]{1,0:T(8,128)(2,1)S(1)} %pad.5.meta_ref, f32[128,2]{1,0:T(8,128)S(1)} %copy.34.gates_ref, f32[128,2048]{1,0:T(8,128)S(1)} %shared_rows.1.base_ref, bf16[64,2048]{1,0:T(8,128)(2,1)S(1)} %get-tuple-element.13.refs_0_, ...), custom_call_target="tpu_custom_call" | custom-call | tf_op jit(solution)/shard_map/combine_rows/pallas_call | solution.py:119
  84.3 0.6 multiply_bitcast_fusion
  84.9 2.7 %combine_rows.3 = bf16[128,2048]{1,0:T(8,128)(2,1)} custom-call(s32[2]{0:T(128)S(1)} %pad_add_fusion.experts_ref, bf16[128,128]{1,0:T(8,128)(2,1)S(1)} %pad.5.meta_ref, f32[128,2]{1,0:T(8,128)S(1)} %copy.34.gates_ref, f32[128,2048]{1,0:T(8,128)S(1)} %combine_rows.2.base_ref, bf16[64,2048]{1,0:T(8,128)(2,1)} %collective-permute-done.12.refs_0_, ...), custom_call_target="tpu_custom_call" | custom-call | tf_op jit(solution)/shard_map/combine_rows/pallas_call | solution.py:119
  (62 shorter events, 0.7 us)
Async XLA Ops:
  3.8 15.9 %collective-permute-start.2 = (bf16[128,2176]{1,0:T(8,128)(2,1)S(1)}, bf16[128,2176]{1,0:T(8,128)(2,1)S(1)}, u32[]{:S(2)}, u32[]{:S(2)}) collective-permute-start(bf16[128,2176]{1,0:T(8,128)(2,1)S(1)} %pad_maximum_fusion.refs_0_), channel_id=1, source_target_pairs={{0,2},{1,5},{2,0},{3,7},{4,6},{5,1},{6,4},{7,3},{8,10},{9,13},{10,... | collective-permute-start | bytes 1671176 | tf_op jit(solution)/shard_map/ppermute | solution.py:149
  6.8 15.0 %collective-permute-start.3 = (bf16[128,2176]{1,0:T(8,128)(2,1)S(1)}, bf16[128,2176]{1,0:T(8,128)(2,1)S(1)}, u32[]{:S(2)}, u32[]{:S(2)}) collective-permute-start(bf16[128,2176]{1,0:T(8,128)(2,1)S(1)} %pad_maximum_fusion.refs_0_), channel_id=1, source_target_pairs={{0,4},{1,3},{2,6},{3,1},{4,0},{5,7},{6,2},{7,5},{8,12},{9,11},{10,... | collective-permute-start | bytes 1671176 | tf_op jit(solution)/shard_map/ppermute | solution.py:149
  19.7 9.5 %collective-permute-start.10 = (bf16[128,2176]{1,0:T(8,128)(2,1)S(1)}, bf16[128,2176]{1,0:T(8,128)(2,1)S(1)}, u32[]{:S(2)}, u32[]{:S(2)}) collective-permute-start(bf16[128,2176]{1,0:T(8,128)(2,1)S(1)} %collective-permute-done.2.refs_0_), channel_id=1, source_target_pairs={{0,4},{1,3},{2,6},{3,1},{4,0},{5,7},{6,2},{7,5},{8,12},{9,11},{10,... | collective-permute-start | bytes 1671176 | tf_op jit(solution)/shard_map/ppermute | solution.py:149
  21.3 14.2 %collective-permute-start = (bf16[128,2176]{1,0:T(8,128)(2,1)S(1)}, bf16[128,2176]{1,0:T(8,128)(2,1)}, u32[]{:S(2)}, u32[]{:S(2)}) collective-permute-start(bf16[128,2176]{1,0:T(8,128)(2,1)S(1)} %pad_maximum_fusion.refs_0_), channel_id=1, source_target_pairs={{0,1},{1,0},{2,3},{3,2},{4,5},{5,4},{6,7},{7,6},{8,9},{9,8},{10,11... | collective-permute-start | bytes 1671176 | tf_op jit(solution)/shard_map/ppermute | solution.py:149
  21.3 24.4 %collective-permute-start.4 = (bf16[128,2176]{1,0:T(8,128)(2,1)S(1)}, bf16[128,2176]{1,0:T(8,128)(2,1)}, u32[]{:S(2)}, u32[]{:S(2)}) collective-permute-start(bf16[128,2176]{1,0:T(8,128)(2,1)S(1)} %collective-permute-done.2.refs_0_), channel_id=1, source_target_pairs={{0,1},{1,0},{2,3},{3,2},{4,5},{5,4},{6,7},{7,6},{8,9},{9,8},{10,11... | collective-permute-start | bytes 1671176 | tf_op jit(solution)/shard_map/ppermute | solution.py:149
  21.8 23.9 %collective-permute-start.5 = (bf16[128,2176]{1,0:T(8,128)(2,1)S(1)}, bf16[128,2176]{1,0:T(8,128)(2,1)}, u32[]{:S(2)}, u32[]{:S(2)}) collective-permute-start(bf16[128,2176]{1,0:T(8,128)(2,1)S(1)} %collective-permute-done.3.refs_1_), channel_id=1, source_target_pairs={{0,1},{1,0},{2,3},{3,2},{4,5},{5,4},{6,7},{7,6},{8,9},{9,8},{10,11... | collective-permute-start | bytes 1671176 | tf_op jit(solution)/shard_map/ppermute | solution.py:149
  29.2 26.5 %collective-permute-start.11 = (bf16[128,2176]{1,0:T(8,128)(2,1)S(1)}, bf16[128,2176]{1,0:T(8,128)(2,1)S(1)}, u32[]{:S(2)}, u32[]{:S(2)}) collective-permute-start(bf16[128,2176]{1,0:T(8,128)(2,1)S(1)} %collective-permute-done.10.refs_0_), channel_id=1, source_target_pairs={{0,1},{1,0},{2,3},{3,2},{4,5},{5,4},{6,7},{7,6},{8,9},{9,8},{10,11... | collective-permute-start | bytes 1671176 | tf_op jit(solution)/shard_map/ppermute | solution.py:149
  35.5 1.6 %copy-start = (bf16[1,2048,512]{2,1,0:T(8,128)(2,1)S(1)}, bf16[1,2048,512]{2,1,0:T(8,128)(2,1)}, u32[]{:S(2)}) copy-start(bf16[1,2048,512]{2,1,0:T(8,128)(2,1)} %refs_2_.3) | copy-start | bytes 6291460
  37.1 1.6 %copy-start.2 = (bf16[1,2048,512]{2,1,0:T(8,128)(2,1)S(1)}, bf16[1,2048,512]{2,1,0:T(8,128)(2,1)}, u32[]{:S(2)}) copy-start(bf16[1,2048,512]{2,1,0:T(8,128)(2,1)} %refs_3_.3) | copy-start | bytes 6291460
  38.7 1.6 %copy-start.4 = (bf16[1,512,2048]{2,1,0:T(8,128)(2,1)S(1)}, bf16[1,512,2048]{2,1,0:T(8,128)(2,1)}, u32[]{:S(2)}) copy-start(bf16[1,512,2048]{2,1,0:T(8,128)(2,1)} %refs_4_.5) | copy-start | bytes 6291460
  40.3 0.7 copy-start.18
  41.0 4.7 %copy-start.1 = (bf16[1,2048,512]{2,1,0:T(8,128)(2,1)S(1)}, bf16[1,2048,512]{2,1,0:T(8,128)(2,1)}, u32[]{:S(2)}) copy-start(bf16[1,2048,512]{2,1,0:T(8,128)(2,1)} %refs_2_.3) | copy-start | bytes 6291460
  41.0 4.7 %copy-start.3 = (bf16[1,2048,512]{2,1,0:T(8,128)(2,1)S(1)}, bf16[1,2048,512]{2,1,0:T(8,128)(2,1)}, u32[]{:S(2)}) copy-start(bf16[1,2048,512]{2,1,0:T(8,128)(2,1)} %refs_3_.3) | copy-start | bytes 6291460
  41.0 4.7 %copy-start.5 = (bf16[1,512,2048]{2,1,0:T(8,128)(2,1)S(1)}, bf16[1,512,2048]{2,1,0:T(8,128)(2,1)}, u32[]{:S(2)}) copy-start(bf16[1,512,2048]{2,1,0:T(8,128)(2,1)} %refs_4_.5) | copy-start | bytes 6291460
  45.1 17.7 %collective-permute-start.1 = (bf16[64,2048]{1,0:T(8,128)(2,1)S(1)}, bf16[64,2048]{1,0:T(8,128)(2,1)S(1)}, u32[]{:S(2)}, u32[]{:S(2)}) collective-permute-start(bf16[64,2048]{1,0:T(8,128)(2,1)S(1)} %get-tuple-element.14), channel_id=1, source_target_pairs={{0,1},{1,0},{2,3},{3,2},{4,5},{5,4},{6,7},{7,6},{8,9},{9,8},{10,11... | collective-permute-start | bytes 786440 | tf_op jit(solution)/shard_map/ppermute | solution.py:149
  52.1 14.9 %collective-permute-start.6 = (bf16[64,2048]{1,0:T(8,128)(2,1)}, bf16[64,2048]{1,0:T(8,128)(2,1)S(1)}, u32[]{:S(2)}, u32[]{:S(2)}) collective-permute-start(bf16[64,2048]{1,0:T(8,128)(2,1)} %get-tuple-element.15), channel_id=1, source_target_pairs={{0,2},{1,5},{2,0},{3,7},{4,6},{5,1},{6,4},{7,3},{8,10},{9,13},{10,... | collective-permute-start | bytes 786440 | tf_op jit(solution)/shard_map/ppermute | solution.py:149
  54.7 14.7 %collective-permute-start.7 = (bf16[64,2048]{1,0:T(8,128)(2,1)}, bf16[64,2048]{1,0:T(8,128)(2,1)S(1)}, u32[]{:S(2)}, u32[]{:S(2)}) collective-permute-start(bf16[64,2048]{1,0:T(8,128)(2,1)} %get-tuple-element.16), channel_id=1, source_target_pairs={{0,4},{1,3},{2,6},{3,1},{4,0},{5,7},{6,2},{7,5},{8,12},{9,11},{10,... | collective-permute-start | bytes 786440 | tf_op jit(solution)/shard_map/ppermute | solution.py:149
  55.4 23.9 %collective-permute-start.8 = (bf16[64,2048]{1,0:T(8,128)(2,1)}, bf16[64,2048]{1,0:T(8,128)(2,1)}, u32[]{:S(2)}, u32[]{:S(2)}) collective-permute-start(bf16[64,2048]{1,0:T(8,128)(2,1)} %get-tuple-element.17), channel_id=1, source_target_pairs={{0,5},{1,2},{2,7},{3,0},{4,1},{5,6},{6,3},{7,4},{8,13},{9,10},{10,... | collective-permute-start | bytes 786440 | tf_op jit(solution)/shard_map/ppermute | solution.py:149
  55.8 0.8 copy-start.10
  56.6 16.1 %copy-start.6 = (bf16[128,2048]{1,0:T(8,128)(2,1)S(1)}, bf16[128,2048]{1,0:T(8,128)(2,1)}, u32[]{:S(2)}) copy-start(bf16[128,2048]{1,0:T(8,128)(2,1)} %tokens_ref.1) | copy-start | bytes 1572868
  56.6 16.1 %copy-start.7 = (bf16[2048,256]{1,0:T(8,128)(2,1)S(1)}, bf16[2048,256]{1,0:T(8,128)(2,1)}, u32[]{:S(2)}) copy-start(bf16[2048,256]{1,0:T(8,128)(2,1)} %wg_ref.1) | copy-start | bytes 3145732
  56.6 22.8 %collective-permute-start.9 = (bf16[64,2048]{1,0:T(8,128)(2,1)}, bf16[64,2048]{1,0:T(8,128)(2,1)}, u32[]{:S(2)}, u32[]{:S(2)}) collective-permute-start(bf16[64,2048]{1,0:T(8,128)(2,1)} %get-tuple-element.18), channel_id=1, source_target_pairs={{0,3},{1,4},{2,1},{3,6},{4,7},{5,0},{6,5},{7,2},{8,11},{9,12},{10,... | collective-permute-start | bytes 786440 | tf_op jit(solution)/shard_map/ppermute | solution.py:149
  58.0 1.1 %copy-start.11 = (bf16[128,2176]{1,0:T(8,128)(2,1)S(1)}, bf16[128,2176]{1,0:T(8,128)(2,1)}, u32[]{:S(2)}) copy-start(bf16[128,2176]{1,0:T(8,128)(2,1)} %copy-done.10) | copy-start | bytes 1671172
  59.0 6.0 %copy-start.23 = (s32[8]{0:T(128)S(1)}, s32[8]{0:T(128)}, u32[]{:S(2)}) copy-start(s32[8]{0:T(128)} %constant.33.clone) | copy-start | bytes 100
  59.0 6.6 %copy-start.22 = (s32[8]{0:T(128)S(1)}, s32[8]{0:T(128)}, u32[]{:S(2)}) copy-start(s32[8]{0:T(128)} %constant.34.clone) | copy-start | bytes 100
  59.0 7.2 %copy-start.21 = (s32[8]{0:T(128)S(1)}, s32[8]{0:T(128)}, u32[]{:S(2)}) copy-start(s32[8]{0:T(128)} %constant.35.clone) | copy-start | bytes 100
  59.0 7.8 %copy-start.20 = (f32[128,2]{0,1:T(2,128)S(1)}, f32[128,2]{0,1:T(2,128)}, u32[]{:S(2)}) copy-start(f32[128,2]{0,1:T(2,128)} %param.21) | copy-start | bytes 3076
  59.0 13.6 %copy-start.19 = (f32[2048]{0:T(1024)S(1)}, f32[2048]{0:T(1024)}, u32[]{:S(2)}) copy-start(f32[2048]{0:T(1024)} %param.19) | copy-start | bytes 24580
  62.7 0.7 copy-start.12
  63.4 5.5 %collective-permute-start.14 = (f32[1,128]{1,0:T(1,128)S(1)}, f32[1,128]{1,0:T(1,128)S(1)}, u32[]{:S(2)}, u32[]{:S(2)}) collective-permute-start(f32[1,128]{1,0:T(1,128)S(1)} %slice.6), channel_id=1, source_target_pairs={{0,8},{8,0},{16,24},{24,16},{1,9},{9,1},{17,25},{25,17},{2,10},{10... | collective-permute-start | bytes 1544 | tf_op jit(solution)/shard_map/ppermute | solution.py:213
  67.0 0.7 copy-start.14
  67.7 17.2 %collective-permute-start.12 = (bf16[64,2048]{1,0:T(8,128)(2,1)}, bf16[64,2048]{1,0:T(8,128)(2,1)}, u32[]{:S(2)}, u32[]{:S(2)}) collective-permute-start(bf16[64,2048]{1,0:T(8,128)(2,1)} %get-tuple-element.19), channel_id=1, source_target_pairs={{0,6},{1,7},{2,4},{3,5},{4,2},{5,3},{6,0},{7,1},{8,14},{9,15},{10,... | collective-permute-start | bytes 786440 | tf_op jit(solution)/shard_map/ppermute | solution.py:149
  69.0 15.9 %collective-permute-start.13 = (bf16[64,2048]{1,0:T(8,128)(2,1)}, bf16[64,2048]{1,0:T(8,128)(2,1)}, u32[]{:S(2)}, u32[]{:S(2)}) collective-permute-start(bf16[64,2048]{1,0:T(8,128)(2,1)} %get-tuple-element.20), channel_id=1, source_target_pairs={{0,7},{1,6},{2,5},{3,4},{4,3},{5,2},{6,1},{7,0},{8,15},{9,14},{10,... | collective-permute-start | bytes 786440 | tf_op jit(solution)/shard_map/ppermute | solution.py:149
  69.4 0.7 copy-start.16
  70.1 14.2 %collective-permute-start.15 = (f32[1,128]{1,0:T(1,128)S(1)}, f32[1,128]{1,0:T(1,128)S(1)}, u32[]{:S(2)}, u32[]{:S(2)}) collective-permute-start(f32[1,128]{1,0:T(1,128)S(1)} %slice_add_fusion), channel_id=1, source_target_pairs={{0,16},{8,24},{16,0},{24,8},{1,17},{9,25},{17,1},{25,9},{2,18},{10... | collective-permute-start | bytes 1544 | tf_op jit(solution)/shard_map/ppermute | solution.py:213
  72.7 1.2 %copy-start.8 = (bf16[2048,256]{1,0:T(8,128)(2,1)S(1)}, bf16[2048,256]{1,0:T(8,128)(2,1)}, u32[]{:S(2)}) copy-start(bf16[2048,256]{1,0:T(8,128)(2,1)} %wu_ref.1) | copy-start | bytes 3145732
  73.9 1.2 %copy-start.9 = (bf16[256,2048]{1,0:T(8,128)(2,1)S(1)}, bf16[256,2048]{1,0:T(8,128)(2,1)}, u32[]{:S(2)}) copy-start(bf16[256,2048]{1,0:T(8,128)(2,1)} %wd_ref.1) | copy-start | bytes 3145732
  75.1 4.2 %copy-start.13 = (bf16[64,2048]{1,0:T(8,128)(2,1)S(1)}, bf16[64,2048]{1,0:T(8,128)(2,1)}, u32[]{:S(2)}) copy-start(bf16[64,2048]{1,0:T(8,128)(2,1)} %copy-done.12) | copy-start | bytes 786436
  79.3 1.0 %copy-start.15 = (bf16[64,2048]{1,0:T(8,128)(2,1)S(1)}, bf16[64,2048]{1,0:T(8,128)(2,1)}, u32[]{:S(2)}) copy-start(bf16[64,2048]{1,0:T(8,128)(2,1)} %copy-done.14) | copy-start | bytes 786436
  80.3 0.9 %copy-start.17 = (bf16[64,2048]{1,0:T(8,128)(2,1)S(1)}, bf16[64,2048]{1,0:T(8,128)(2,1)}, u32[]{:S(2)}) copy-start(bf16[64,2048]{1,0:T(8,128)(2,1)} %copy-done.16) | copy-start | bytes 786436

commit v2 on v1

v2 whole, which is shorter than its diff:
```python
import functools

import jax
import jax.numpy as jnp
import numpy as np
from jax import lax
from jax.experimental import pallas as pl
from jax.experimental.pallas import tpu as pltpu
from jax.sharding import PartitionSpec as P

LANES = 128
VMEM = pl.BlockSpec(memory_space=pltpu.VMEM)
F32 = jnp.float32
BF16 = jnp.bfloat16


def dot(a, b, contract=((1,), (0,))):
    return lax.dot_general(a, b, (contract, ((), ())), preferred_element_type=F32)


def layer_normed(values, gain):
    center = jnp.mean(values, axis=-1, keepdims=True)
    moved = values - center
    spread = jnp.mean(moved * moved, axis=-1, keepdims=True)
    return (moved * lax.rsqrt(spread + 1e-05) * gain).astype(BF16)


def silu(v):
    return v / (1.0 + jnp.exp(-v))


def before_mask(rows):
    row = lax.broadcasted_iota(jnp.int32, (rows, rows), 0)
    col = lax.broadcasted_iota(jnp.int32, (rows, rows), 1)
    return jnp.where(row < col, 1.0, 0.0).astype(BF16)


def places(first, second, expert, slots, before):
    rows = first.shape[1]
    named = jnp.where((first == expert) | (second == expert), 1.0, 0.0)
    rank = dot(jnp.broadcast_to(named, (8, rows)).astype(BF16), before)[0:1]
    slot = lax.broadcasted_iota(jnp.int32, (slots, rows), 0).astype(F32)
    return jnp.where((rank == slot) & (named > 0.0), 1.0, 0.0)


def origin_id(masks):
    me = lax.axis_index("tp")
    return jnp.where(me % 2 == 0, me ^ masks[0], me ^ masks[1])


def expert_kernel(count, slots, gain_ref, wg_ref, wu_ref, wd_ref, tally_in, *refs):
    blocks, metas = refs[:count], refs[count : 2 * count]
    outs, tally_ref, normed = refs[2 * count : 3 * count], refs[3 * count], refs[3 * count + 1]
    rows = blocks[0].shape[0]
    me = lax.axis_index("tp")
    before = before_mask(rows)
    kinds = lax.broadcasted_iota(jnp.int32, (LANES, rows), 0)
    seen = jnp.zeros((LANES, rows), F32)
    for i, block in enumerate(blocks):
        first, second = metas[i][0:1, :], metas[i][1:2, :]
        seen = seen + jnp.where((first == kinds) | (second == kinds), 1.0, 0.0)
        pick = places(first, second, me, slots, before).astype(BF16)
        normed[i * slots : (i + 1) * slots, :] = layer_normed(dot(pick, block[...]), gain_ref[...])
    tally_ref[...] = tally_in[...] + dot(
        jnp.ones((8, rows), BF16), seen.astype(BF16), ((1,), (1,))
    )
    gate = dot(normed[...], wg_ref[...])
    up = dot(normed[...], wu_ref[...])
    hidden = (silu(gate) * up).astype(BF16)
    result = dot(hidden, wd_ref[...]).astype(BF16)
    for i, out in enumerate(outs):
        out[...] = result[i * slots : (i + 1) * slots]


def expert_call(gain, weights, tally, blocks, metas, slots):
    count = len(blocks)
    width, units = weights[0].shape
    return pl.pallas_call(
        functools.partial(expert_kernel, count, slots),
        out_shape=[jax.ShapeDtypeStruct((slots, width), BF16)] * count
        + [jax.ShapeDtypeStruct((8, LANES), F32)],
        in_specs=[VMEM] * (5 + 2 * count),
        out_specs=[VMEM] * (count + 1),
        scratch_shapes=[pltpu.VMEM((count * slots, width), BF16)],
        compiler_params=pltpu.CompilerParams(vmem_limit_bytes=24 * 2**20),
        cost_estimate=pl.CostEstimate(
            flops=6 * count * slots * width * units, bytes_accessed=6 * width * units, transcendentals=0
        ),
        name="expert_rows",
    )(gain, *weights, tally, *blocks, *metas)


def load_kernel(*refs):
    sources, targets, sems = refs[:3], refs[3:6], refs[6]
    copies = []
    for i, (source, target) in enumerate(zip(sources, targets)):
        part = target.shape[0] // 4
        for j in range(4):
            piece = pl.ds(j * part, part)
            copies.append(
                pltpu.make_async_copy(source.at[0, piece], target.at[piece], sems.at[i, j])
            )
    for copy in copies:
        copy.start()
    for copy in copies:
        copy.wait()


def load_call(*weights):
    return pl.pallas_call(
        load_kernel,
        out_shape=[jax.ShapeDtypeStruct(w.shape[1:], w.dtype) for w in weights],
        in_specs=[pl.BlockSpec(memory_space=pltpu.HBM)] * 3,
        out_specs=[VMEM] * 3,
        scratch_shapes=[pltpu.SemaphoreType.DMA((3, 4))],
        compiler_params=pltpu.CompilerParams(vmem_limit_bytes=16 * 2**20),
        name="load_weights",
    )(*[pltpu.with_memory_space_constraint(w, pltpu.HBM) for w in weights])


def shared_kernel(tokens_ref, gain_ref, wg_ref, wu_ref, wd_ref, out_ref):
    normed = layer_normed(tokens_ref[...].astype(F32), gain_ref[...])
    hidden = (silu(dot(normed, wg_ref[...])) * dot(normed, wu_ref[...])).astype(BF16)
    out_ref[...] = dot(hidden, wd_ref[...])


def combine_kernel(origins, routes_ref, gates_ref, base_ref, *refs):
    blocks, out_ref = refs[: len(origins)], refs[len(origins)]
    rows = base_ref.shape[0]
    first, second = routes_ref[0:1, :], routes_ref[1:2, :]
    before = before_mask(rows)
    lefts, rights = [], []
    for block, masks in zip(blocks, origins):
        expert = origin_id(masks)
        pick = places(first, second, expert, block.shape[0], before)
        left = jnp.where(first == expert, pick, 0.0)
        lefts.append(left.astype(BF16))
        rights.append((pick - left).astype(BF16))
    values = jnp.concatenate([block[...] for block in blocks], axis=0)
    gates = gates_ref[...].T
    total = base_ref[...]
    for k, picks in enumerate((lefts, rights)):
        chosen = dot(jnp.concatenate(picks, axis=0), values, ((0,), (0,)))
        total = total + gates[:, k : k + 1] * chosen
    out_ref[...] = total.astype(out_ref.dtype)


def combine_call(origins, routes, gates, base, blocks, kind):
    return pl.pallas_call(
        functools.partial(combine_kernel, origins),
        out_shape=jax.ShapeDtypeStruct(base.shape, kind),
        in_specs=[VMEM] * (3 + len(blocks)),
        out_specs=VMEM,
        compiler_params=pltpu.CompilerParams(vmem_limit_bytes=24 * 2**20),
        name="combine_rows",
    )(routes, gates, base, *blocks)


def per_device(
    tokens,
    norm_gain,
    routes,
    gates,
    expert_gate,
    expert_up,
    expert_down,
    shared_gate,
    shared_up,
    shared_down,
):
    rows, width = tokens.shape
    top = routes.shape[1]
    groups, planes = lax.axis_size("tp"), lax.axis_size("ep")
    slots = 2 * rows * top // groups
    ids = np.arange(groups)
    partner = ids ^ 1
    gain = norm_gain.reshape(1, width)
    routes, gates = routes.T, gates.T

    def send(value, perm):
        return lax.ppermute(value, "tp", [(int(i), int(perm[i])) for i in ids])

    def masks_of(perm):
        return int(perm[0]), int(perm[1] ^ 1)

    masks = [1 << b for b in range(1, groups.bit_length() - 1)]
    hops = [
        np.where(ids % 2 == 0, ids ^ masks[i], ids ^ masks[-1 - i]) for i in range(len(masks))
    ]
    known, metas = [(tokens, ids)], [(routes, ids)]
    for hop in hops:
        for block, origin in list(known):
            known.append((send(block, hop), origin[hop]))
            metas.append((send(routes, origin[hop]), origin[hop]))
    weights = load_call(expert_gate, expert_up, expert_down)

    tally = jnp.zeros((8, LANES), F32)
    returned = []

    def run(block, meta, origin, tally):
        across = send(block, partner)
        meta_across = send(meta, partner)
        *results, tally = expert_call(
            gain, weights, tally, [block, across], [meta, meta_across], slots
        )
        back = []
        for result, source in zip(results, (origin, origin[partner])):
            if np.array_equal(source, ids):
                back.append((result, ids))
            else:
                back.append((send(result, source), np.argsort(source)))
        returned.append(back)
        return tally

    for number in (*range(1, len(known)), 0):
        tally = run(known[number][0], *metas[number], tally)

    base = pl.pallas_call(
        shared_kernel,
        out_shape=jax.ShapeDtypeStruct((rows, width), F32),
        in_specs=[VMEM] * 5,
        out_specs=VMEM,
        compiler_params=pltpu.CompilerParams(vmem_limit_bytes=24 * 2**20),
        name="shared_rows",
    )(tokens, gain, shared_gate, shared_up, shared_down)

    late = returned.pop(-2) if len(returned) > 1 else []
    early = [item for back in returned for item in back]
    for blocks, kind in ((early, F32), (late, BF16)):
        origins = [masks_of(origin) for _, origin in blocks]
        base = combine_call(origins, routes, gates, base, [b for b, _ in blocks], kind)

    total = tally[0:1]
    if planes & (planes - 1):
        total = lax.psum(total, "ep")
    else:
        for bit in range(planes.bit_length() - 1):
            other = lax.ppermute(total, "ep", [(i, i ^ (1 << bit)) for i in range(planes)])
            total = total + other
    load = total[0, :groups] * (groups / (rows * top * planes * groups))
    return base, load


def solution(mesh):
    placed = (
        P(("ep", "tp"), None),
        P(),
        P(("ep", "tp"), None),
        P(("ep", "tp"), None),
        P("tp", None, None),
        P("tp", None, None),
        P("tp", None, None),
        P(),
        P(),
        P(),
    )

    return jax.shard_map(
        per_device,
        mesh=mesh,
        in_specs=placed,
        out_specs=(P(("ep", "tp"), None), P()),
        check_vma=False,
    )
```

time: 88.9 us -> 77.9 us (0.88); the launches traced: 87.6 us -> 77.7 us
  local copies, waits for them, and re-layouts: 25.1 us -> 0.04 us
  waiting for transfers between devices: 18.9 us -> 38.7 us
  Pallas kernels: 20.9 us -> 13.6 us
  starting transfers between devices: 18 us -> 24.1 us
  other arithmetic: 3.83 us -> 0.52 us
    ppermute x14 -> x21, waiting for transfers between devices: 18.9 us -> 36.8 us  [send(): return lax.ppermute(value, 'tp', [(int(i), int(perm[i])) for i in ids])]
    unnamed x50 -> x14, local copies, waits for them, and re-layouts: 14.7 us -> 0.03 us
    pallas_call x3 -> x4, Pallas kernels: 14.2 us -> 7.26 us  [expert_call(): pl.pallas_call(functools.partial(expert_kernel, count, slots), out_shape=...]
    dynamic_slice x7 -> x0, local copies, waits for them, and re-layouts: 6.81 us -> none  [per_device(): jnp.asarray(origin, jnp.int32)[me]]
    ppermute x14 -> x21, starting transfers between devices: 13.9 us -> 19.5 us  [send(): return lax.ppermute(value, 'tp', [(int(i), int(perm[i])) for i in ids])]
    another operation x1 -> x0, local copies, waits for them, and re-layouts: 3.2 us -> none  [per_device(): jnp.stack([jnp.asarray(origin, jnp.int32)[me] for _, origin in blocks])]
    another operation x2 -> x0, other arithmetic: 1.96 us -> none  [the longest x1 1.28 us: per_device(): jnp.stack([jnp.asarray(origin, jnp.int32)[me] for _, origin in blocks])]
    ppermute x2, waiting for transfers between devices: 0.01 us -> 1.81 us  [per_device(): lax.ppermute(total, 'ep', [(i, i ^ 1 << bit) for i in range(planes)])]
  transfers between devices with their start and end apart: 16 -> 23, of which waited for: 2 -> 10; matrix products, arithmetic and copies ran while one was open for 14% -> 1% of each run, Pallas kernels for 21% -> 16%
where the time goes in v2:
time: 77.9 us; the launch traced here: 77.7 us
  waiting for transfers between devices  38.7 us (50%)
  starting transfers between devices  24.1 us (31%)
  Pallas kernels  13.6 us (17%)
  between operations  0.79 us (1%)
    ppermute x21, waiting for transfers between devices, send(): return lax.ppermute(value, 'tp', [(int(i), int(perm[i])) for i in ids])  36.8 us
    ppermute x21, starting transfers between devices, send(): return lax.ppermute(value, 'tp', [(int(i), int(perm[i])) for i in ids])  19.5 us
    pallas_call x4, Pallas kernels, expert_call(): pl.pallas_call(functools.partial(expert_kernel, count, slots), out_shape=...  7.26 us
    ppermute x2, starting transfers between devices, per_device(): lax.ppermute(total, 'ep', [(i, i ^ 1 << bit) for i in range(planes)])  4.6 us
    pallas_call x1, Pallas kernels, load_call(): pl.pallas_call(load_kernel, out_shape=[jax.ShapeDtypeStruct(w.shape[1:],...  2.88 us
    pallas_call x2, Pallas kernels, combine_call(): pl.pallas_call(functools.partial(combine_kernel, origins), out_shape=jax....  2.41 us
    ppermute x2, waiting for transfers between devices, per_device(): lax.ppermute(total, 'ep', [(i, i ^ 1 << bit) for i in range(planes)])  1.81 us
  transfers between devices with their start and end apart: 23, of which 10 were waited for; matrix products, arithmetic and copies ran while one was open for 1% of the time, Pallas kernels for 16%

profile of v2, /device:TPU:0, one launch (start us, length us, event | category | flops | bytes accessed | tf_op | source)
XLA Modules:
  0.0 77.7 jit_solution(11101993393789879684)
XLA Ops:
  0.6 3.0 %collective-permute-start = (bf16[128,2048]{1,0:T(8,128)(2,1)}, bf16[128,2048]{1,0:T(8,128)(2,1)S(1)}, u32[]{:S(2)}, u32[]{:S(2)}) collective-permute-start(bf16[128,2048]{1,0:T(8,128)(2,1)} %refs_0_.3), channel_id=1, source_target_pairs={{0,2},{1,5},{2,0},{3,7},{4,6},{5,1},{6,4},{7,3},{8,10},{9,13},{10,... | collective-permute-start | bytes 1572872 | tf_op jit(solution)/shard_map/ppermute | solution.py:181
  3.7 1.5 %collective-permute-start.6 = (bf16[128,2048]{1,0:T(8,128)(2,1)}, bf16[128,2048]{1,0:T(8,128)(2,1)S(1)}, u32[]{:S(2)}, u32[]{:S(2)}) collective-permute-start(bf16[128,2048]{1,0:T(8,128)(2,1)} %refs_0_.3), channel_id=1, source_target_pairs={{0,4},{1,3},{2,6},{3,1},{4,0},{5,7},{6,2},{7,5},{8,12},{9,11},{10,... | collective-permute-start | bytes 1572872 | tf_op jit(solution)/shard_map/ppermute | solution.py:181
  5.2 11.0 %collective-permute-done.refs_0_ = bf16[128,2048]{1,0:T(8,128)(2,1)S(1)} collective-permute-done((bf16[128,2048]{1,0:T(8,128)(2,1)}, bf16[128,2048]{1,0:T(8,128)(2,1)S(1)}, u32[]{:S(2)}, u32[]{:S(2)}) %collective-permute-start) | collective-permute-done | bytes 524320 | tf_op jit(solution)/shard_map/ppermute | solution.py:181
  16.2 1.5 %collective-permute-start.12 = (bf16[128,2048]{1,0:T(8,128)(2,1)S(1)}, bf16[128,2048]{1,0:T(8,128)(2,1)S(1)}, u32[]{:S(2)}, u32[]{:S(2)}) collective-permute-start(bf16[128,2048]{1,0:T(8,128)(2,1)S(1)} %collective-permute-done.refs_0_), channel_id=1, source_target_pairs={{0,4},{1,3},{2,6},{3,1},{4,0},{5,7},{6,2},{7,5},{8,12},{9,11},{10,... | collective-permute-start | bytes 1572872 | tf_op jit(solution)/shard_map/ppermute | solution.py:181
  17.7 0.5 collective-permute-start.7
  18.2 7.2 %collective-permute-done.12.refs_0_ = bf16[128,2048]{1,0:T(8,128)(2,1)S(1)} collective-permute-done((bf16[128,2048]{1,0:T(8,128)(2,1)S(1)}, bf16[128,2048]{1,0:T(8,128)(2,1)S(1)}, u32[]{:S(2)}, u32[]{:S(2)}) %collective-permute-start.12) | collective-permute-done | bytes 524320 | tf_op jit(solution)/shard_map/ppermute | solution.py:181
  25.4 0.5 collective-permute-start.16
  25.9 2.4 %collective-permute-start.2 = (s32[2,128]{1,0:T(2,128)}, s32[2,128]{1,0:T(2,128)S(1)}, u32[]{:S(2)}, u32[]{:S(2)}) collective-permute-start(s32[2,128]{1,0:T(2,128)} %bitcast.10), channel_id=1, source_target_pairs={{0,2},{1,5},{2,0},{3,7},{4,6},{5,1},{6,4},{7,3},{8,10},{9,13},{10,... | collective-permute-start | bytes 3080 | tf_op jit(solution)/shard_map/ppermute | solution.py:181
  28.3 1.8 %collective-permute-done.2.refs_2_ = s32[2,128]{1,0:T(2,128)S(1)} collective-permute-done((s32[2,128]{1,0:T(2,128)}, s32[2,128]{1,0:T(2,128)S(1)}, u32[]{:S(2)}, u32[]{:S(2)}) %collective-permute-start.2) | collective-permute-done | bytes 1056 | tf_op jit(solution)/shard_map/ppermute | solution.py:181
  30.1 1.0 %collective-permute-start.8 = (s32[2,128]{1,0:T(2,128)}, s32[2,128]{1,0:T(2,128)S(1)}, u32[]{:S(2)}, u32[]{:S(2)}) collective-permute-start(s32[2,128]{1,0:T(2,128)} %bitcast.11), channel_id=1, source_target_pairs={{0,4},{1,3},{2,6},{3,1},{4,0},{5,7},{6,2},{7,5},{8,12},{9,11},{10,... | collective-permute-start | bytes 3080 | tf_op jit(solution)/shard_map/ppermute | solution.py:181
  31.1 2.7 %collective-permute-done.8.refs_2_ = s32[2,128]{1,0:T(2,128)S(1)} collective-permute-done((s32[2,128]{1,0:T(2,128)}, s32[2,128]{1,0:T(2,128)S(1)}, u32[]{:S(2)}, u32[]{:S(2)}) %collective-permute-start.8) | collective-permute-done | bytes 1056 | tf_op jit(solution)/shard_map/ppermute | solution.py:181
  33.9 0.0 collective-permute-start.3
  33.9 2.9 %load_weights.1 = (bf16[2048,512]{1,0:T(8,128)(2,1)S(1)}, bf16[2048,512]{1,0:T(8,128)(2,1)S(1)}, bf16[512,2048]{1,0:T(8,128)(2,1)S(1)}) custom-call(bf16[1,2048,512]{2,1,0:T(8,128)(2,1)} %refs_0_.2, bf16[1,2048,512]{2,1,0:T(8,128)(2,1)} %refs_1_.1, bf16[1,512,2048]{2,1,0:T(8,128)(2,1)} %refs_2_.1), custom_call_target="tpu_custom_call" | custom-call | tf_op jit(solution)/shard_map/load_weights/pallas_call | solution.py:110
  36.8 0.0 collective-permute-done.3.refs_3_
  36.8 2.2 %collective-permute-start.14 = (s32[2,128]{1,0:T(2,128)S(1)}, s32[2,128]{1,0:T(2,128)S(1)}, u32[]{:S(2)}, u32[]{:S(2)}) collective-permute-start(s32[2,128]{1,0:T(2,128)S(1)} %bitcast.12), channel_id=1, source_target_pairs={{0,6},{1,7},{2,4},{3,5},{4,2},{5,3},{6,0},{7,1},{8,14},{9,15},{10,... | collective-permute-start | bytes 3080 | tf_op jit(solution)/shard_map/ppermute | solution.py:181
  39.0 0.2 collective-permute-start.9
  39.2 1.8 %expert_rows.4 = (bf16[64,2048]{1,0:T(8,128)(2,1)S(1)}, bf16[64,2048]{1,0:T(8,128)(2,1)S(1)}, f32[8,128]{1,0:T(8,128)S(1)}) custom-call(f32[1,2048]{1,0:T(1,128)S(1)} %bitcast.5, bf16[2048,512]{1,0:T(8,128)(2,1)S(1)} %get-tuple-element.17.wg_ref, bf16[2048,512]{1,0:T(8,128)(2,1)S(1)} %get-tuple-element.18.wu_ref, ...), custom_call_target="tpu_custom_call" | custom-call | flops 805306368 | bytes 6291456 | tf_op jit(solution)/shard_map/expert_rows/pallas_call | solution.py:78
  41.0 0.3 collective-permute-done.14.refs_2_
  41.3 0.1 collective-permute-start.17
  41.4 0.5 collective-permute-start.15
  41.8 1.8 %expert_rows.5 = (bf16[64,2048]{1,0:T(8,128)(2,1)S(1)}, bf16[64,2048]{1,0:T(8,128)(2,1)S(1)}, f32[8,128]{1,0:T(8,128)S(1)}) custom-call(f32[1,2048]{1,0:T(1,128)S(1)} %bitcast.6, bf16[2048,512]{1,0:T(8,128)(2,1)S(1)} %get-tuple-element.17.wg_ref, bf16[2048,512]{1,0:T(8,128)(2,1)S(1)} %get-tuple-element.18.wu_ref, ...), custom_call_target="tpu_custom_call" | custom-call | flops 805306368 | bytes 6291456 | tf_op jit(solution)/shard_map/expert_rows/pallas_call | solution.py:78
  43.7 1.1 %collective-permute-start.10 = (bf16[64,2048]{1,0:T(8,128)(2,1)S(1)}, bf16[64,2048]{1,0:T(8,128)(2,1)S(1)}, u32[]{:S(2)}, u32[]{:S(2)}) collective-permute-start(bf16[64,2048]{1,0:T(8,128)(2,1)S(1)} %get-tuple-element.23), channel_id=1, source_target_pairs={{0,4},{1,3},{2,6},{3,1},{4,0},{5,7},{6,2},{7,5},{8,12},{9,11},{10,... | collective-permute-start | bytes 786440 | tf_op jit(solution)/shard_map/ppermute | solution.py:181
  44.8 0.6 collective-permute-start.11
  45.4 0.0 collective-permute-done.13.refs_1_
  45.4 1.8 %expert_rows.6 = (bf16[64,2048]{1,0:T(8,128)(2,1)S(1)}, bf16[64,2048]{1,0:T(8,128)(2,1)S(1)}, f32[8,128]{1,0:T(8,128)S(1)}) custom-call(f32[1,2048]{1,0:T(1,128)S(1)} %bitcast.7, bf16[2048,512]{1,0:T(8,128)(2,1)S(1)} %get-tuple-element.17.wg_ref, bf16[2048,512]{1,0:T(8,128)(2,1)S(1)} %get-tuple-element.18.wu_ref, ...), custom_call_target="tpu_custom_call" | custom-call | flops 805306368 | bytes 6291456 | tf_op jit(solution)/shard_map/expert_rows/pallas_call | solution.py:78
  47.2 0.0 copy-start.1
  47.2 0.0 copy-start.2
  47.3 0.0 copy-start.3
  47.3 1.8 %expert_rows.7 = (bf16[64,2048]{1,0:T(8,128)(2,1)S(1)}, bf16[64,2048]{1,0:T(8,128)(2,1)S(1)}, f32[8,128]{1,0:T(8,128)S(1)}) custom-call(f32[1,2048]{1,0:T(1,128)S(1)} %bitcast.8, bf16[2048,512]{1,0:T(8,128)(2,1)S(1)} %get-tuple-element.17.wg_ref, bf16[2048,512]{1,0:T(8,128)(2,1)S(1)} %get-tuple-element.18.wu_ref, ...), custom_call_target="tpu_custom_call" | custom-call | flops 805306368 | bytes 6291456 | tf_op jit(solution)/shard_map/expert_rows/pallas_call | solution.py:78
  49.1 1.8 %collective-permute-start.21 = (f32[1,128]{1,0:T(1,128)S(1)}, f32[1,128]{1,0:T(1,128)S(1)}, u32[]{:S(2)}, u32[]{:S(2)}) collective-permute-start(f32[1,128]{1,0:T(1,128)S(1)} %slice.6), channel_id=1, source_target_pairs={{0,8},{8,0},{16,24},{24,16},{1,9},{9,1},{17,25},{25,17},{2,10},{10... | collective-permute-start | bytes 1544 | tf_op jit(solution)/shard_map/ppermute | solution.py:238
  50.9 1.8 %collective-permute-done.21 = f32[1,128]{1,0:T(1,128)S(1)} collective-permute-done((f32[1,128]{1,0:T(1,128)S(1)}, f32[1,128]{1,0:T(1,128)S(1)}, u32[]{:S(2)}, u32[]{:S(2)}) %collective-permute-start.21) | collective-permute-done | bytes 544 | tf_op jit(solution)/shard_map/ppermute | solution.py:238
  52.7 2.8 %collective-permute-start.22 = (f32[1,128]{1,0:T(1,128)S(1)}, f32[1,128]{1,0:T(1,128)S(1)}, u32[]{:S(2)}, u32[]{:S(2)}) collective-permute-start(f32[1,128]{1,0:T(1,128)S(1)} %slice_add_fusion), channel_id=1, source_target_pairs={{0,16},{8,24},{16,0},{24,8},{1,17},{9,25},{17,1},{25,9},{2,18},{10... | collective-permute-start | bytes 1544 | tf_op jit(solution)/shard_map/ppermute | solution.py:238
  55.5 1.5 %collective-permute-start.4 = (bf16[64,2048]{1,0:T(8,128)(2,1)S(1)}, bf16[64,2048]{1,0:T(8,128)(2,1)S(1)}, u32[]{:S(2)}, u32[]{:S(2)}) collective-permute-start(bf16[64,2048]{1,0:T(8,128)(2,1)S(1)} %get-tuple-element.20), channel_id=1, source_target_pairs={{0,2},{1,5},{2,0},{3,7},{4,6},{5,1},{6,4},{7,3},{8,10},{9,13},{10,... | collective-permute-start | bytes 786440 | tf_op jit(solution)/shard_map/ppermute | solution.py:181
  57.0 0.0 collective-permute-start.5
  57.0 0.0 collective-permute-done.10.refs_2_
  57.0 0.6 collective-permute-start.18
  57.7 1.6 %collective-permute-start.19 = (bf16[64,2048]{1,0:T(8,128)(2,1)S(1)}, bf16[64,2048]{1,0:T(8,128)(2,1)S(1)}, u32[]{:S(2)}, u32[]{:S(2)}) collective-permute-start(bf16[64,2048]{1,0:T(8,128)(2,1)S(1)} %get-tuple-element.29), channel_id=1, source_target_pairs={{0,6},{1,7},{2,4},{3,5},{4,2},{5,3},{6,0},{7,1},{8,14},{9,15},{10,... | collective-permute-start | bytes 786440 | tf_op jit(solution)/shard_map/ppermute | solution.py:181
  59.3 0.0 collective-permute-done.22
  59.3 0.7 collective-permute-start.20
  60.0 1.0 %shared_rows.1.base_ref = f32[128,2048]{1,0:T(8,128)S(1)} custom-call(bf16[128,2048]{1,0:T(8,128)(2,1)S(1)} %copy-done, f32[1,2048]{1,0:T(1,128)S(1)} %bitcast.9, bf16[2048,256]{1,0:T(8,128)(2,1)S(1)} %copy-done.1, bf16[2048,256]{1,0:T(8,128)(2,1)S(1)} %copy-done.2, bf16[256,2048]{1,0:T(8,128)(2,1)S(1)} %copy-done.3), custom_call_target="tpu_custom_call" | custom-call | tf_op jit(solution)/shard_map/shared_rows/pallas_call | solution.py:218
  61.0 0.5 multiply_bitcast_fusion
  61.6 2.2 %collective-permute-done.4.refs_0_ = bf16[64,2048]{1,0:T(8,128)(2,1)S(1)} collective-permute-done((bf16[64,2048]{1,0:T(8,128)(2,1)S(1)}, bf16[64,2048]{1,0:T(8,128)(2,1)S(1)}, u32[]{:S(2)}, u32[]{:S(2)}) %collective-permute-start.4) | collective-permute-done | bytes 262176 | tf_op jit(solution)/shard_map/ppermute | solution.py:181
  63.8 1.8 %collective-permute-done.5.refs_1_ = bf16[64,2048]{1,0:T(8,128)(2,1)S(1)} collective-permute-done((bf16[64,2048]{1,0:T(8,128)(2,1)S(1)}, bf16[64,2048]{1,0:T(8,128)(2,1)S(1)}, u32[]{:S(2)}, u32[]{:S(2)}) %collective-permute-start.5) | collective-permute-done | bytes 262176 | tf_op jit(solution)/shard_map/ppermute | solution.py:181
  65.6 0.0 collective-permute-done.18.refs_5_
  65.6 1.0 %combine_rows.2.base_ref = f32[128,2048]{1,0:T(8,128)S(1)} custom-call(s32[2,128]{1,0:T(2,128)S(1)} %bitcast.15, f32[2,128]{1,0:T(2,128)S(1)} %bitcast.17, f32[128,2048]{1,0:T(8,128)S(1)} %shared_rows.1.base_ref, bf16[64,2048]{1,0:T(8,128)(2,1)S(1)} %collective-permute-done.4.refs_0_, bf16[64,2048]{1,0:T(8,128)(2,1)S(1)} %collective-permute-done.5.refs_1_, ...), custom_call_target="tpu_custom_call" | custom-call | tf_op jit(solution)/shard_map/combine_rows/pallas_call | solution.py:149
  66.6 3.3 %collective-permute-done.19.refs_0_ = bf16[64,2048]{1,0:T(8,128)(2,1)S(1)} collective-permute-done((bf16[64,2048]{1,0:T(8,128)(2,1)S(1)}, bf16[64,2048]{1,0:T(8,128)(2,1)S(1)}, u32[]{:S(2)}, u32[]{:S(2)}) %collective-permute-start.19) | collective-permute-done | bytes 262176 | tf_op jit(solution)/shard_map/ppermute | solution.py:181
  69.9 6.4 %collective-permute-done.20.refs_1_ = bf16[64,2048]{1,0:T(8,128)(2,1)S(1)} collective-permute-done((bf16[64,2048]{1,0:T(8,128)(2,1)S(1)}, bf16[64,2048]{1,0:T(8,128)(2,1)S(1)}, u32[]{:S(2)}, u32[]{:S(2)}) %collective-permute-start.20) | collective-permute-done | bytes 262176 | tf_op jit(solution)/shard_map/ppermute | solution.py:181
  76.3 1.5 %combine_rows.3 = bf16[128,2048]{1,0:T(8,128)(2,1)} custom-call(s32[2,128]{1,0:T(2,128)S(1)} %bitcast.16, f32[2,128]{1,0:T(2,128)S(1)} %bitcast.18, f32[128,2048]{1,0:T(8,128)S(1)} %combine_rows.2.base_ref, bf16[64,2048]{1,0:T(8,128)(2,1)S(1)} %collective-permute-done.19.refs_0_, bf16[64,2048]{1,0:T(8,128)(2,1)S(1)} %collective-permute-done.20.refs_1_), custom_call_target="tpu_custom_call" | custom-call | tf_op jit(solution)/shard_map/combine_rows/pallas_call | solution.py:149
  (25 shorter events, 0.1 us)
Async XLA Ops:
  0.6 15.6 %collective-permute-start = (bf16[128,2048]{1,0:T(8,128)(2,1)}, bf16[128,2048]{1,0:T(8,128)(2,1)S(1)}, u32[]{:S(2)}, u32[]{:S(2)}) collective-permute-start(bf16[128,2048]{1,0:T(8,128)(2,1)} %refs_0_.3), channel_id=1, source_target_pairs={{0,2},{1,5},{2,0},{3,7},{4,6},{5,1},{6,4},{7,3},{8,10},{9,13},{10,... | collective-permute-start | bytes 1572872 | tf_op jit(solution)/shard_map/ppermute | solution.py:181
  3.7 14.0 %collective-permute-start.6 = (bf16[128,2048]{1,0:T(8,128)(2,1)}, bf16[128,2048]{1,0:T(8,128)(2,1)S(1)}, u32[]{:S(2)}, u32[]{:S(2)}) collective-permute-start(bf16[128,2048]{1,0:T(8,128)(2,1)} %refs_0_.3), channel_id=1, source_target_pairs={{0,4},{1,3},{2,6},{3,1},{4,0},{5,7},{6,2},{7,5},{8,12},{9,11},{10,... | collective-permute-start | bytes 1572872 | tf_op jit(solution)/shard_map/ppermute | solution.py:181
  16.2 9.2 %collective-permute-start.12 = (bf16[128,2048]{1,0:T(8,128)(2,1)S(1)}, bf16[128,2048]{1,0:T(8,128)(2,1)S(1)}, u32[]{:S(2)}, u32[]{:S(2)}) collective-permute-start(bf16[128,2048]{1,0:T(8,128)(2,1)S(1)} %collective-permute-done.refs_0_), channel_id=1, source_target_pairs={{0,4},{1,3},{2,6},{3,1},{4,0},{5,7},{6,2},{7,5},{8,12},{9,11},{10,... | collective-permute-start | bytes 1572872 | tf_op jit(solution)/shard_map/ppermute | solution.py:181
  17.6 21.3 %collective-permute-start.1 = (bf16[128,2048]{1,0:T(8,128)(2,1)S(1)}, bf16[128,2048]{1,0:T(8,128)(2,1)S(1)}, u32[]{:S(2)}, u32[]{:S(2)}) collective-permute-start(bf16[128,2048]{1,0:T(8,128)(2,1)S(1)} %collective-permute-done.refs_0_), channel_id=1, source_target_pairs={{0,1},{1,0},{2,3},{3,2},{4,5},{5,4},{6,7},{7,6},{8,9},{9,8},{10,11... | collective-permute-start | bytes 1572872 | tf_op jit(solution)/shard_map/ppermute | solution.py:181
  17.7 24.2 %collective-permute-start.7 = (bf16[128,2048]{1,0:T(8,128)(2,1)S(1)}, bf16[128,2048]{1,0:T(8,128)(2,1)S(1)}, u32[]{:S(2)}, u32[]{:S(2)}) collective-permute-start(bf16[128,2048]{1,0:T(8,128)(2,1)S(1)} %collective-permute-done.6.refs_0_), channel_id=1, source_target_pairs={{0,1},{1,0},{2,3},{3,2},{4,5},{5,4},{6,7},{7,6},{8,9},{9,8},{10,11... | collective-permute-start | bytes 1572872 | tf_op jit(solution)/shard_map/ppermute | solution.py:181
  25.4 20.0 %collective-permute-start.13 = (bf16[128,2048]{1,0:T(8,128)(2,1)S(1)}, bf16[128,2048]{1,0:T(8,128)(2,1)S(1)}, u32[]{:S(2)}, u32[]{:S(2)}) collective-permute-start(bf16[128,2048]{1,0:T(8,128)(2,1)S(1)} %collective-permute-done.12.refs_0_), channel_id=1, source_target_pairs={{0,1},{1,0},{2,3},{3,2},{4,5},{5,4},{6,7},{7,6},{8,9},{9,8},{10,11... | collective-permute-start | bytes 1572872 | tf_op jit(solution)/shard_map/ppermute | solution.py:181
  25.4 21.8 %collective-permute-start.16 = (bf16[128,2048]{1,0:T(8,128)(2,1)}, bf16[128,2048]{1,0:T(8,128)(2,1)S(1)}, u32[]{:S(2)}, u32[]{:S(2)}) collective-permute-start(bf16[128,2048]{1,0:T(8,128)(2,1)} %refs_0_.3), channel_id=1, source_target_pairs={{0,1},{1,0},{2,3},{3,2},{4,5},{5,4},{6,7},{7,6},{8,9},{9,8},{10,11... | collective-permute-start | bytes 1572872 | tf_op jit(solution)/shard_map/ppermute | solution.py:181
  25.9 10.9 %copy-start.5 = (s32[128,2]{0,1:T(2,128)S(1)}, s32[128,2]{0,1:T(2,128)}, u32[]{:S(2)}) copy-start(s32[128,2]{0,1:T(2,128)} %param.12) | copy-start | bytes 3076
  25.9 13.3 %copy-start.4 = (f32[2048]{0:T(1024)S(1)}, f32[2048]{0:T(1024)}, u32[]{:S(2)}) copy-start(f32[2048]{0:T(1024)} %param.11) | copy-start | bytes 24580
  25.9 4.2 %collective-permute-start.2 = (s32[2,128]{1,0:T(2,128)}, s32[2,128]{1,0:T(2,128)S(1)}, u32[]{:S(2)}, u32[]{:S(2)}) collective-permute-start(s32[2,128]{1,0:T(2,128)} %bitcast.10), channel_id=1, source_target_pairs={{0,2},{1,5},{2,0},{3,7},{4,6},{5,1},{6,4},{7,3},{8,10},{9,13},{10,... | collective-permute-start | bytes 3080 | tf_op jit(solution)/shard_map/ppermute | solution.py:181
  30.1 3.8 %collective-permute-start.8 = (s32[2,128]{1,0:T(2,128)}, s32[2,128]{1,0:T(2,128)S(1)}, u32[]{:S(2)}, u32[]{:S(2)}) collective-permute-start(s32[2,128]{1,0:T(2,128)} %bitcast.11), channel_id=1, source_target_pairs={{0,4},{1,3},{2,6},{3,1},{4,0},{5,7},{6,2},{7,5},{8,12},{9,11},{10,... | collective-permute-start | bytes 3080 | tf_op jit(solution)/shard_map/ppermute | solution.py:181
  33.9 2.9 %collective-permute-start.3 = (s32[2,128]{1,0:T(2,128)S(1)}, s32[2,128]{1,0:T(2,128)S(1)}, u32[]{:S(2)}, u32[]{:S(2)}) collective-permute-start(s32[2,128]{1,0:T(2,128)S(1)} %collective-permute-done.2.refs_2_), channel_id=1, source_target_pairs={{0,1},{1,0},{2,3},{3,2},{4,5},{5,4},{6,7},{7,6},{8,9},{9,8},{10,11... | collective-permute-start | bytes 3080 | tf_op jit(solution)/shard_map/ppermute | solution.py:181
  36.8 4.5 %collective-permute-start.14 = (s32[2,128]{1,0:T(2,128)S(1)}, s32[2,128]{1,0:T(2,128)S(1)}, u32[]{:S(2)}, u32[]{:S(2)}) collective-permute-start(s32[2,128]{1,0:T(2,128)S(1)} %bitcast.12), channel_id=1, source_target_pairs={{0,6},{1,7},{2,4},{3,5},{4,2},{5,3},{6,0},{7,1},{8,14},{9,15},{10,... | collective-permute-start | bytes 3080 | tf_op jit(solution)/shard_map/ppermute | solution.py:181
  39.0 2.4 %collective-permute-start.9 = (s32[2,128]{1,0:T(2,128)S(1)}, s32[2,128]{1,0:T(2,128)S(1)}, u32[]{:S(2)}, u32[]{:S(2)}) collective-permute-start(s32[2,128]{1,0:T(2,128)S(1)} %collective-permute-done.8.refs_2_), channel_id=1, source_target_pairs={{0,1},{1,0},{2,3},{3,2},{4,5},{5,4},{6,7},{7,6},{8,9},{9,8},{10,11... | collective-permute-start | bytes 3080 | tf_op jit(solution)/shard_map/ppermute | solution.py:181
  41.3 5.9 %collective-permute-start.17 = (s32[2,128]{1,0:T(2,128)S(1)}, s32[2,128]{1,0:T(2,128)S(1)}, u32[]{:S(2)}, u32[]{:S(2)}) collective-permute-start(s32[2,128]{1,0:T(2,128)S(1)} %bitcast.13), channel_id=1, source_target_pairs={{0,1},{1,0},{2,3},{3,2},{4,5},{5,4},{6,7},{7,6},{8,9},{9,8},{10,11... | collective-permute-start | bytes 3080 | tf_op jit(solution)/shard_map/ppermute | solution.py:181
  41.4 3.4 %collective-permute-start.15 = (s32[2,128]{1,0:T(2,128)S(1)}, s32[2,128]{1,0:T(2,128)S(1)}, u32[]{:S(2)}, u32[]{:S(2)}) collective-permute-start(s32[2,128]{1,0:T(2,128)S(1)} %collective-permute-done.14.refs_2_), channel_id=1, source_target_pairs={{0,1},{1,0},{2,3},{3,2},{4,5},{5,4},{6,7},{7,6},{8,9},{9,8},{10,11... | collective-permute-start | bytes 3080 | tf_op jit(solution)/shard_map/ppermute | solution.py:181
  43.7 13.3 %collective-permute-start.10 = (bf16[64,2048]{1,0:T(8,128)(2,1)S(1)}, bf16[64,2048]{1,0:T(8,128)(2,1)S(1)}, u32[]{:S(2)}, u32[]{:S(2)}) collective-permute-start(bf16[64,2048]{1,0:T(8,128)(2,1)S(1)} %get-tuple-element.23), channel_id=1, source_target_pairs={{0,4},{1,3},{2,6},{3,1},{4,0},{5,7},{6,2},{7,5},{8,12},{9,11},{10,... | collective-permute-start | bytes 786440 | tf_op jit(solution)/shard_map/ppermute | solution.py:181
  44.8 12.9 %collective-permute-start.11 = (bf16[64,2048]{1,0:T(8,128)(2,1)S(1)}, bf16[64,2048]{1,0:T(8,128)(2,1)S(1)}, u32[]{:S(2)}, u32[]{:S(2)}) collective-permute-start(bf16[64,2048]{1,0:T(8,128)(2,1)S(1)} %get-tuple-element.24), channel_id=1, source_target_pairs={{0,3},{1,4},{2,1},{3,6},{4,7},{5,0},{6,5},{7,2},{8,11},{9,12},{10,... | collective-permute-start | bytes 786440 | tf_op jit(solution)/shard_map/ppermute | solution.py:181
  45.4 1.8 %copy-start = (bf16[128,2048]{1,0:T(8,128)(2,1)S(1)}, bf16[128,2048]{1,0:T(8,128)(2,1)}, u32[]{:S(2)}) copy-start(bf16[128,2048]{1,0:T(8,128)(2,1)} %refs_0_.3) | copy-start | bytes 1572868
  47.2 12.8 %copy-start.1 = (bf16[2048,256]{1,0:T(8,128)(2,1)S(1)}, bf16[2048,256]{1,0:T(8,128)(2,1)}, u32[]{:S(2)}) copy-start(bf16[2048,256]{1,0:T(8,128)(2,1)} %wg_ref.1) | copy-start | bytes 3145732
  47.2 12.8 %copy-start.2 = (bf16[2048,256]{1,0:T(8,128)(2,1)S(1)}, bf16[2048,256]{1,0:T(8,128)(2,1)}, u32[]{:S(2)}) copy-start(bf16[2048,256]{1,0:T(8,128)(2,1)} %wu_ref.1) | copy-start | bytes 3145732
  47.3 12.7 %copy-start.3 = (bf16[256,2048]{1,0:T(8,128)(2,1)S(1)}, bf16[256,2048]{1,0:T(8,128)(2,1)}, u32[]{:S(2)}) copy-start(bf16[256,2048]{1,0:T(8,128)(2,1)} %wd_ref.1) | copy-start | bytes 3145732
  49.1 3.6 %collective-permute-start.21 = (f32[1,128]{1,0:T(1,128)S(1)}, f32[1,128]{1,0:T(1,128)S(1)}, u32[]{:S(2)}, u32[]{:S(2)}) collective-permute-start(f32[1,128]{1,0:T(1,128)S(1)} %slice.6), channel_id=1, source_target_pairs={{0,8},{8,0},{16,24},{24,16},{1,9},{9,1},{17,25},{25,17},{2,10},{10... | collective-permute-start | bytes 1544 | tf_op jit(solution)/shard_map/ppermute | solution.py:238
  52.7 6.6 %collective-permute-start.22 = (f32[1,128]{1,0:T(1,128)S(1)}, f32[1,128]{1,0:T(1,128)S(1)}, u32[]{:S(2)}, u32[]{:S(2)}) collective-permute-start(f32[1,128]{1,0:T(1,128)S(1)} %slice_add_fusion), channel_id=1, source_target_pairs={{0,16},{8,24},{16,0},{24,8},{1,17},{9,25},{17,1},{25,9},{2,18},{10... | collective-permute-start | bytes 1544 | tf_op jit(solution)/shard_map/ppermute | solution.py:238
  55.5 8.3 %collective-permute-start.4 = (bf16[64,2048]{1,0:T(8,128)(2,1)S(1)}, bf16[64,2048]{1,0:T(8,128)(2,1)S(1)}, u32[]{:S(2)}, u32[]{:S(2)}) collective-permute-start(bf16[64,2048]{1,0:T(8,128)(2,1)S(1)} %get-tuple-element.20), channel_id=1, source_target_pairs={{0,2},{1,5},{2,0},{3,7},{4,6},{5,1},{6,4},{7,3},{8,10},{9,13},{10,... | collective-permute-start | bytes 786440 | tf_op jit(solution)/shard_map/ppermute | solution.py:181
  57.0 8.6 %collective-permute-start.5 = (bf16[64,2048]{1,0:T(8,128)(2,1)S(1)}, bf16[64,2048]{1,0:T(8,128)(2,1)S(1)}, u32[]{:S(2)}, u32[]{:S(2)}) collective-permute-start(bf16[64,2048]{1,0:T(8,128)(2,1)S(1)} %get-tuple-element.21), channel_id=1, source_target_pairs={{0,5},{1,2},{2,7},{3,0},{4,1},{5,6},{6,3},{7,4},{8,13},{9,10},{10,... | collective-permute-start | bytes 786440 | tf_op jit(solution)/shard_map/ppermute | solution.py:181
  57.0 8.6 %collective-permute-start.18 = (bf16[64,2048]{1,0:T(8,128)(2,1)S(1)}, bf16[64,2048]{1,0:T(8,128)(2,1)S(1)}, u32[]{:S(2)}, u32[]{:S(2)}) collective-permute-start(bf16[64,2048]{1,0:T(8,128)(2,1)S(1)} %get-tuple-element.28), channel_id=1, source_target_pairs={{0,1},{1,0},{2,3},{3,2},{4,5},{5,4},{6,7},{7,6},{8,9},{9,8},{10,11... | collective-permute-start | bytes 786440 | tf_op jit(solution)/shard_map/ppermute | solution.py:181
  57.7 12.2 %collective-permute-start.19 = (bf16[64,2048]{1,0:T(8,128)(2,1)S(1)}, bf16[64,2048]{1,0:T(8,128)(2,1)S(1)}, u32[]{:S(2)}, u32[]{:S(2)}) collective-permute-start(bf16[64,2048]{1,0:T(8,128)(2,1)S(1)} %get-tuple-element.29), channel_id=1, source_target_pairs={{0,6},{1,7},{2,4},{3,5},{4,2},{5,3},{6,0},{7,1},{8,14},{9,15},{10,... | collective-permute-start | bytes 786440 | tf_op jit(solution)/shard_map/ppermute | solution.py:181
  59.3 6.3 %copy-start.6 = (f32[128,2]{0,1:T(2,128)S(1)}, f32[128,2]{0,1:T(2,128)}, u32[]{:S(2)}) copy-start(f32[128,2]{0,1:T(2,128)} %param.13) | copy-start | bytes 3076
  59.3 16.9 %collective-permute-start.20 = (bf16[64,2048]{1,0:T(8,128)(2,1)S(1)}, bf16[64,2048]{1,0:T(8,128)(2,1)S(1)}, u32[]{:S(2)}, u32[]{:S(2)}) collective-permute-start(bf16[64,2048]{1,0:T(8,128)(2,1)S(1)} %get-tuple-element.30), channel_id=1, source_target_pairs={{0,7},{1,6},{2,5},{3,4},{4,3},{5,2},{6,1},{7,0},{8,15},{9,14},{10,... | collective-permute-start | bytes 786440 | tf_op jit(solution)/shard_map/ppermute | solution.py:181

commit v3 on v2

v3 whole, which is shorter than its diff:
```python
import functools

import jax
import jax.numpy as jnp
import numpy as np
from jax import lax
from jax.experimental import pallas as pl
from jax.experimental.pallas import tpu as pltpu
from jax.sharding import PartitionSpec as P

LANES = 128
VMEM = pl.BlockSpec(memory_space=pltpu.VMEM)
F32 = jnp.float32
BF16 = jnp.bfloat16


def dot(a, b, contract=((1,), (0,))):
    return lax.dot_general(a, b, (contract, ((), ())), preferred_element_type=F32)


def layer_normed(values, gain):
    center = jnp.mean(values, axis=-1, keepdims=True)
    moved = values - center
    spread = jnp.mean(moved * moved, axis=-1, keepdims=True)
    return (moved * lax.rsqrt(spread + 1e-05) * gain).astype(BF16)


def silu(v):
    return v / (1.0 + jnp.exp(-v))


def before_mask(rows):
    row = lax.broadcasted_iota(jnp.int32, (rows, rows), 0)
    col = lax.broadcasted_iota(jnp.int32, (rows, rows), 1)
    return jnp.where(row < col, 1.0, 0.0).astype(BF16)


def places(first, second, expert, slots, before):
    rows = first.shape[1]
    named = jnp.where((first == expert) | (second == expert), 1.0, 0.0)
    rank = dot(jnp.broadcast_to(named, (8, rows)).astype(BF16), before)[0:1]
    slot = lax.broadcasted_iota(jnp.int32, (slots, rows), 0).astype(F32)
    return jnp.where((rank == slot) & (named > 0.0), 1.0, 0.0)


def origin_id(masks):
    me = lax.axis_index("tp")
    return jnp.where(me % 2 == 0, me ^ masks[0], me ^ masks[1])


def expert_kernel(count, slots, halves, gain_ref, wg_ref, wu_ref, wd_ref, *refs):
    blocks, metas = refs[:count], refs[count : 2 * count]
    outs, normed = refs[2 * count : 3 * count], refs[3 * count]
    rows = blocks[0].shape[0]
    me = lax.axis_index("tp")
    before = before_mask(rows)
    for i, block in enumerate(blocks):
        at = 2 * halves[i]
        pick = places(metas[i][at : at + 1, :], metas[i][at + 1 : at + 2, :], me, slots, before)
        normed[i * slots : (i + 1) * slots, :] = layer_normed(
            dot(pick.astype(BF16), block[...]), gain_ref[...]
        )
    gate = dot(normed[...], wg_ref[...])
    up = dot(normed[...], wu_ref[...])
    hidden = (silu(gate) * up).astype(BF16)
    result = dot(hidden, wd_ref[...]).astype(BF16)
    for i, out in enumerate(outs):
        out[...] = result[i * slots : (i + 1) * slots]


def expert_call(gain, weights, blocks, metas, halves, slots):
    count = len(blocks)
    width, units = weights[0].shape
    return pl.pallas_call(
        functools.partial(expert_kernel, count, slots, halves),
        out_shape=[jax.ShapeDtypeStruct((slots, width), BF16)] * count,
        in_specs=[VMEM] * (4 + 2 * count),
        out_specs=[VMEM] * count,
        scratch_shapes=[pltpu.VMEM((count * slots, width), BF16)],
        compiler_params=pltpu.CompilerParams(vmem_limit_bytes=24 * 2**20),
        cost_estimate=pl.CostEstimate(
            flops=6 * count * slots * width * units, bytes_accessed=6 * width * units, transcendentals=0
        ),
        name="expert_rows",
    )(gain, *weights, *blocks, *metas)


def pair_kernel(mine_ref, other_ref, out_ref):
    top = mine_ref.shape[0]
    out_ref[0:top, :] = mine_ref[...]
    out_ref[top:, :] = other_ref[...]


def pair_call(mine, other):
    return pl.pallas_call(
        pair_kernel,
        out_shape=jax.ShapeDtypeStruct((2 * mine.shape[0], mine.shape[1]), mine.dtype),
        in_specs=[VMEM] * 2,
        out_specs=VMEM,
        compiler_params=pltpu.CompilerParams(vmem_limit_bytes=4 * 2**20),
        name="pair_routes",
    )(mine, other)


def tally_kernel(*refs):
    metas, out_ref = refs[:-1], refs[-1]
    rows = metas[0].shape[1]
    kinds = lax.broadcasted_iota(jnp.int32, (LANES, rows), 0)
    seen = jnp.zeros((LANES, rows), F32)
    for meta in metas:
        for i in range(meta.shape[0]):
            seen = seen + jnp.where(meta[i : i + 1, :] == kinds, 1.0, 0.0)
    out_ref[...] = dot(jnp.ones((8, rows), BF16), seen.astype(BF16), ((1,), (1,)))


def tally_call(metas):
    return pl.pallas_call(
        tally_kernel,
        out_shape=jax.ShapeDtypeStruct((8, LANES), F32),
        in_specs=[VMEM] * len(metas),
        out_specs=VMEM,
        compiler_params=pltpu.CompilerParams(vmem_limit_bytes=4 * 2**20),
        name="tally_routes",
    )(*metas)


def load_kernel(count, *refs):
    sources, targets, sems = refs[:count], refs[count : 2 * count], refs[2 * count]
    copies = []
    for i, (source, target) in enumerate(zip(sources, targets)):
        part = target.shape[0] // 4
        for j in range(4):
            piece = pl.ds(j * part, part)
            copies.append(
                pltpu.make_async_copy(source.at[0, piece], target.at[piece], sems.at[i, j])
            )
    for copy in copies:
        copy.start()
    for copy in copies:
        copy.wait()


def load_call(*weights):
    count = len(weights)
    return pl.pallas_call(
        functools.partial(load_kernel, count),
        out_shape=[jax.ShapeDtypeStruct(w.shape[1:], w.dtype) for w in weights],
        in_specs=[pl.BlockSpec(memory_space=pltpu.HBM)] * count,
        out_specs=[VMEM] * count,
        scratch_shapes=[pltpu.SemaphoreType.DMA((count, 4))],
        compiler_params=pltpu.CompilerParams(vmem_limit_bytes=16 * 2**20),
        name="load_weights",
    )(*[pltpu.with_memory_space_constraint(w, pltpu.HBM) for w in weights])


def shared_kernel(tokens_ref, gain_ref, wg_ref, wu_ref, wd_ref, out_ref):
    normed = layer_normed(tokens_ref[...].astype(F32), gain_ref[...])
    hidden = (silu(dot(normed, wg_ref[...])) * dot(normed, wu_ref[...])).astype(BF16)
    out_ref[...] = dot(hidden, wd_ref[...])


def picks_of(routes_ref, origins, slots, before):
    first, second = routes_ref[0:1, :], routes_ref[1:2, :]
    lefts, rights = [], []
    for masks in origins:
        expert = origin_id(masks)
        pick = places(first, second, expert, slots, before)
        left = jnp.where(first == expert, pick, 0.0)
        lefts.append(left)
        rights.append(pick - left)
    stack = [jnp.concatenate(part, axis=0).T for part in (lefts, rights)]
    return jnp.concatenate(stack, axis=0).astype(BF16)


def combine_kernel(early, late, routes_ref, gates_ref, base_ref, *refs):
    blocks, (out_ref, picks_ref, gates_out) = refs[:-3], refs[-3:]
    rows, slots = base_ref.shape[0], blocks[0].shape[0]
    before = before_mask(rows)
    gates = gates_ref[...].T
    gates_out[...] = gates
    picks_ref[...] = picks_of(routes_ref, late, slots, before)
    values = jnp.concatenate([block[...] for block in blocks], axis=0)
    chosen = dot(picks_of(routes_ref, early, slots, before), values)
    out_ref[...] = (
        base_ref[...] + gates[:, 0:1] * chosen[:rows] + gates[:, 1:2] * chosen[rows:]
    )


def finish_kernel(pieces, picks_ref, gates_ref, base_ref, *refs):
    blocks, (out_ref, mixed, sems) = refs[:-3], refs[-3:]
    rows, width = base_ref.shape
    part = width // pieces
    copies = []
    for j in range(pieces):
        cols = slice(j * part, (j + 1) * part)
        values = jnp.concatenate([block[:, cols] for block in blocks], axis=0)
        chosen = dot(picks_ref[...], values)
        total = base_ref[:, cols] + gates_ref[:, 0:1] * chosen[:rows]
        mixed[:, cols] = (total + gates_ref[:, 1:2] * chosen[rows:]).astype(mixed.dtype)
        copies.append(pltpu.make_async_copy(mixed.at[:, cols], out_ref.at[:, cols], sems.at[j]))
        copies[-1].start()
    for copy in copies:
        copy.wait()


def combine_call(early, late, routes, gates, base, blocks):
    rows, slots = base.shape[0], blocks[0].shape[0]
    return pl.pallas_call(
        functools.partial(combine_kernel, early, late),
        out_shape=[
            jax.ShapeDtypeStruct(base.shape, F32),
            jax.ShapeDtypeStruct((2 * rows, slots * len(late)), BF16),
            jax.ShapeDtypeStruct((rows, gates.shape[0]), F32),
        ],
        in_specs=[VMEM] * (3 + len(blocks)),
        out_specs=[VMEM] * 3,
        compiler_params=pltpu.CompilerParams(vmem_limit_bytes=24 * 2**20),
        name="combine_rows",
    )(routes, gates, base, *blocks)


def finish_call(picks, gates, base, blocks, pieces=4):
    return pl.pallas_call(
        functools.partial(finish_kernel, pieces),
        out_shape=jax.ShapeDtypeStruct(base.shape, BF16),
        in_specs=[VMEM] * (3 + len(blocks)),
        out_specs=pl.BlockSpec(memory_space=pltpu.HBM),
        scratch_shapes=[pltpu.VMEM(base.shape, BF16), pltpu.SemaphoreType.DMA((pieces,))],
        compiler_params=pltpu.CompilerParams(vmem_limit_bytes=24 * 2**20),
        name="finish_rows",
    )(picks, gates, base, *blocks)


def per_device(
    tokens,
    norm_gain,
    routes,
    gates,
    expert_gate,
    expert_up,
    expert_down,
    shared_gate,
    shared_up,
    shared_down,
):
    rows, width = tokens.shape
    top = routes.shape[1]
    groups, planes = lax.axis_size("tp"), lax.axis_size("ep")
    slots = 2 * rows * top // groups
    ids = np.arange(groups)
    partner = ids ^ 1
    gain = norm_gain.reshape(1, width)
    routes, gates = routes.T, gates.T

    def send(value, perm):
        return lax.ppermute(value, "tp", [(int(i), int(perm[i])) for i in ids])

    def masks_of(perm):
        return int(perm[0]), int(perm[1] ^ 1)

    masks = [1 << b for b in range(1, groups.bit_length() - 1)]
    hops = [
        np.where(ids % 2 == 0, ids ^ masks[i], ids ^ masks[-1 - i]) for i in range(len(masks))
    ]
    both = pair_call(routes, send(routes, partner))
    known, metas = [(tokens, ids)], [both]
    for hop in hops:
        for block, origin in list(known):
            known.append((send(block, hop), origin[hop]))
            metas.append(send(both, origin[hop]))
    weights = load_call(expert_gate, expert_up) + load_call(expert_down)
    total = tally_call(metas)[0:1]

    def meta_of(source):
        for meta, (_, origin) in zip(metas, known):
            if np.array_equal(origin, source):
                return meta, 0
            if np.array_equal(origin ^ 1, source):
                return meta, 1

    returned = []
    for number in (*range(1, len(known)), 0):
        block, origin = known[number]
        across = send(block, partner)
        sources = (origin, origin[partner])
        found = [meta_of(source) for source in sources]
        results = expert_call(
            gain, weights, [block, across], [m for m, _ in found], [h for _, h in found], slots
        )
        back = []
        for result, source in zip(results, sources):
            if np.array_equal(source, ids):
                back.append((result, ids))
            else:
                back.append((send(result, source), np.argsort(source)))
        returned.append(back)

    base = pl.pallas_call(
        shared_kernel,
        out_shape=jax.ShapeDtypeStruct((rows, width), F32),
        in_specs=[VMEM] * 5,
        out_specs=VMEM,
        compiler_params=pltpu.CompilerParams(vmem_limit_bytes=24 * 2**20),
        name="shared_rows",
    )(tokens, gain, shared_gate, shared_up, shared_down)

    late = returned.pop(-2)
    if len(returned) > 2:
        late = returned.pop(-2) + late
    early = [item for back in returned for item in back]
    base, picks, columns = combine_call(
        [masks_of(origin) for _, origin in early],
        [masks_of(origin) for _, origin in late],
        routes,
        gates,
        base,
        [block for block, _ in early],
    )
    mixed = finish_call(picks, columns, base, [block for block, _ in late])

    if planes & (planes - 1):
        total = lax.psum(total, "ep")
    else:
        for bit in range(planes.bit_length() - 1):
            other = lax.ppermute(total, "ep", [(i, i ^ (1 << bit)) for i in range(planes)])
            total = total + other
    load = total[0, :groups] * (groups / (rows * top * planes * groups))
    return mixed, load


def solution(mesh):
    placed = (
        P(("ep", "tp"), None),
        P(),
        P(("ep", "tp"), None),
        P(("ep", "tp"), None),
        P("tp", None, None),
        P("tp", None, None),
        P("tp", None, None),
        P(),
        P(),
        P(),
    )

    return jax.shard_map(
        per_device,
        mesh=mesh,
        in_specs=placed,
        out_specs=(P(("ep", "tp"), None), P()),
        check_vma=False,
    )
```

time: 77.9 us -> 74.7 us (0.959); the launches traced: 77.7 us -> 73.4 us
  waiting for transfers between devices: 38.7 us -> 34 us
  starting transfers between devices: 24.1 us -> 23.1 us
    ppermute x21 -> x18, waiting for transfers between devices: 36.8 us -> 34 us  [send(): return lax.ppermute(value, 'tp', [(int(i), int(perm[i])) for i in ids])]
    ppermute x2, waiting for transfers between devices: 1.81 us -> 0.01 us  [per_device(): lax.ppermute(total, 'ep', [(i, i ^ 1 << bit) for i in range(planes)])]
    pallas_call x7 -> x10, Pallas kernels: 12.6 us -> 13.2 us  [the longest x4 7.29 us: expert_call(): pl.pallas_call(functools.partial(expert_kernel, count, slots, halves), ou...]
    ppermute x21 -> x18, starting transfers between devices: 19.5 us -> 18.9 us  [send(): return lax.ppermute(value, 'tp', [(int(i), int(perm[i])) for i in ids])]
  transfers between devices with their start and end apart: 23 -> 20, of which waited for: 10 -> 8; matrix products, arithmetic and copies ran while one was open for 1% -> 1% of each run, Pallas kernels for 16% -> 18%
where the time goes in v3:
time: 74.7 us; the launch traced here: 73.4 us
  waiting for transfers between devices  34 us (46%)
  starting transfers between devices  23.1 us (31%)
  Pallas kernels  14.2 us (19%)
  between operations  0.81 us (1%)
    ppermute x18, waiting for transfers between devices, send(): return lax.ppermute(value, 'tp', [(int(i), int(perm[i])) for i in ids])  34 us
    ppermute x18, starting transfers between devices, send(): return lax.ppermute(value, 'tp', [(int(i), int(perm[i])) for i in ids])  18.9 us
    pallas_call x4, Pallas kernels, expert_call(): pl.pallas_call(functools.partial(expert_kernel, count, slots, halves), ou...  7.29 us
    ppermute x2, starting transfers between devices, per_device(): lax.ppermute(total, 'ep', [(i, i ^ 1 << bit) for i in range(planes)])  4.18 us
    pallas_call x2, Pallas kernels, load_call(): pl.pallas_call(functools.partial(load_kernel, count), out_shape=[jax.Shap...  3.82 us
  transfers between devices with their start and end apart: 20, of which 8 were waited for; matrix products, arithmetic and copies ran while one was open for 1% of the time, Pallas kernels for 18%

profile of v3, /device:TPU:0, one launch (start us, length us, event | category | flops | bytes accessed | tf_op | source)
XLA Modules:
  0.0 73.4 jit_solution(5287413229549176678)
XLA Ops:
  0.6 3.0 %collective-permute-start = (bf16[128,2048]{1,0:T(8,128)(2,1)}, bf16[128,2048]{1,0:T(8,128)(2,1)S(1)}, u32[]{:S(2)}, u32[]{:S(2)}) collective-permute-start(bf16[128,2048]{1,0:T(8,128)(2,1)} %refs_0_.5), channel_id=1, source_target_pairs={{0,2},{1,5},{2,0},{3,7},{4,6},{5,1},{6,4},{7,3},{8,10},{9,13},{10,... | collective-permute-start | bytes 1572872 | tf_op jit(solution)/shard_map/ppermute | solution.py:256
  3.7 1.5 %collective-permute-start.9 = (bf16[128,2048]{1,0:T(8,128)(2,1)}, bf16[128,2048]{1,0:T(8,128)(2,1)S(1)}, u32[]{:S(2)}, u32[]{:S(2)}) collective-permute-start(bf16[128,2048]{1,0:T(8,128)(2,1)} %refs_0_.5), channel_id=1, source_target_pairs={{0,4},{1,3},{2,6},{3,1},{4,0},{5,7},{6,2},{7,5},{8,12},{9,11},{10,... | collective-permute-start | bytes 1572872 | tf_op jit(solution)/shard_map/ppermute | solution.py:256
  5.2 11.0 %collective-permute-done.refs_0_ = bf16[128,2048]{1,0:T(8,128)(2,1)S(1)} collective-permute-done((bf16[128,2048]{1,0:T(8,128)(2,1)}, bf16[128,2048]{1,0:T(8,128)(2,1)S(1)}, u32[]{:S(2)}, u32[]{:S(2)}) %collective-permute-start) | collective-permute-done | bytes 524320 | tf_op jit(solution)/shard_map/ppermute | solution.py:256
  16.2 1.5 %collective-permute-start.13 = (bf16[128,2048]{1,0:T(8,128)(2,1)S(1)}, bf16[128,2048]{1,0:T(8,128)(2,1)S(1)}, u32[]{:S(2)}, u32[]{:S(2)}) collective-permute-start(bf16[128,2048]{1,0:T(8,128)(2,1)S(1)} %collective-permute-done.refs_0_), channel_id=1, source_target_pairs={{0,4},{1,3},{2,6},{3,1},{4,0},{5,7},{6,2},{7,5},{8,12},{9,11},{10,... | collective-permute-start | bytes 1572872 | tf_op jit(solution)/shard_map/ppermute | solution.py:256
  17.6 0.0 collective-permute-start.7
  17.6 0.5 collective-permute-start.1
  18.2 0.0 collective-permute-done.9.refs_0_
  18.2 0.0 collective-permute-start.10
  18.2 7.2 %collective-permute-done.13.refs_0_ = bf16[128,2048]{1,0:T(8,128)(2,1)S(1)} collective-permute-done((bf16[128,2048]{1,0:T(8,128)(2,1)S(1)}, bf16[128,2048]{1,0:T(8,128)(2,1)S(1)}, u32[]{:S(2)}, u32[]{:S(2)}) %collective-permute-start.13) | collective-permute-done | bytes 524320 | tf_op jit(solution)/shard_map/ppermute | solution.py:256
  25.4 0.0 collective-permute-start.14
  25.4 0.5 collective-permute-start.2
  25.9 1.4 %collective-permute-done.2.other_ref = s32[2,128]{1,0:T(2,128)S(1)} collective-permute-done((s32[2,128]{1,0:T(2,128)}, s32[2,128]{1,0:T(2,128)S(1)}, u32[]{:S(2)}, u32[]{:S(2)}) %collective-permute-start.2) | collective-permute-done | bytes 1056 | tf_op jit(solution)/shard_map/ppermute | solution.py:256
  27.3 0.7 copy-done.5
  28.0 2.4 %collective-permute-start.3 = (s32[4,128]{1,0:T(4,128)S(1)}, s32[4,128]{1,0:T(4,128)S(1)}, u32[]{:S(2)}, u32[]{:S(2)}) collective-permute-start(s32[4,128]{1,0:T(4,128)S(1)} %pair_routes.1.refs_2_.refs_3_.refs_0_), channel_id=1, source_target_pairs={{0,2},{1,5},{2,0},{3,7},{4,6},{5,1},{6,4},{7,3},{8,10},{9,13},{10,... | collective-permute-start | bytes 6152 | tf_op jit(solution)/shard_map/ppermute | solution.py:256
  30.3 1.6 %collective-permute-done.3.refs_2_.refs_3_.refs_1_ = s32[4,128]{1,0:T(4,128)S(1)} collective-permute-done((s32[4,128]{1,0:T(4,128)S(1)}, s32[4,128]{1,0:T(4,128)S(1)}, u32[]{:S(2)}, u32[]{:S(2)}) %collective-permute-start.3) | collective-permute-done | bytes 2080 | tf_op jit(solution)/shard_map/ppermute | solution.py:256
  31.9 1.1 %collective-permute-start.4 = (s32[4,128]{1,0:T(4,128)S(1)}, s32[4,128]{1,0:T(4,128)S(1)}, u32[]{:S(2)}, u32[]{:S(2)}) collective-permute-start(s32[4,128]{1,0:T(4,128)S(1)} %pair_routes.1.refs_2_.refs_3_.refs_0_), channel_id=1, source_target_pairs={{0,4},{1,3},{2,6},{3,1},{4,0},{5,7},{6,2},{7,5},{8,12},{9,11},{10,... | collective-permute-start | bytes 6152 | tf_op jit(solution)/shard_map/ppermute | solution.py:256
  33.0 2.5 %collective-permute-done.4.refs_3_.refs_2_ = s32[4,128]{1,0:T(4,128)S(1)} collective-permute-done((s32[4,128]{1,0:T(4,128)S(1)}, s32[4,128]{1,0:T(4,128)S(1)}, u32[]{:S(2)}, u32[]{:S(2)}) %collective-permute-start.4) | collective-permute-done | bytes 2080 | tf_op jit(solution)/shard_map/ppermute | solution.py:256
  35.5 2.2 %collective-permute-start.15 = (s32[4,128]{1,0:T(4,128)S(1)}, s32[4,128]{1,0:T(4,128)S(1)}, u32[]{:S(2)}, u32[]{:S(2)}) collective-permute-start(s32[4,128]{1,0:T(4,128)S(1)} %pair_routes.1.refs_2_.refs_3_.refs_0_), channel_id=1, source_target_pairs={{0,6},{1,7},{2,4},{3,5},{4,2},{5,3},{6,0},{7,1},{8,14},{9,15},{10,... | collective-permute-start | bytes 6152 | tf_op jit(solution)/shard_map/ppermute | solution.py:256
  37.7 1.5 %load_weights.3.wd_ref = bf16[512,2048]{1,0:T(8,128)(2,1)S(1)} custom-call(bf16[1,512,2048]{2,1,0:T(8,128)(2,1)} %refs_0_.4), custom_call_target="tpu_custom_call" | custom-call | tf_op jit(solution)/shard_map/load_weights/pallas_call | solution.py:145
  39.2 0.0 copy-start
  39.2 0.0 copy-start.4
  39.2 2.3 %load_weights.2 = (bf16[2048,512]{1,0:T(8,128)(2,1)S(1)}, bf16[2048,512]{1,0:T(8,128)(2,1)S(1)}) custom-call(bf16[1,2048,512]{2,1,0:T(8,128)(2,1)} %refs_0_.3, bf16[1,2048,512]{2,1,0:T(8,128)(2,1)} %refs_1_.1), custom_call_target="tpu_custom_call" | custom-call | tf_op jit(solution)/shard_map/load_weights/pallas_call | solution.py:145
  41.5 0.2 tally_routes.1
  41.8 1.6 %collective-permute-start.18 = (f32[1,128]{1,0:T(1,128)S(1)}, f32[1,128]{1,0:T(1,128)S(1)}, u32[]{:S(2)}, u32[]{:S(2)}) collective-permute-start(f32[1,128]{1,0:T(1,128)S(1)} %slice.6), channel_id=1, source_target_pairs={{0,8},{8,0},{16,24},{24,16},{1,9},{9,1},{17,25},{25,17},{2,10},{10... | collective-permute-start | bytes 1544 | tf_op jit(solution)/shard_map/ppermute | solution.py:325
  43.3 0.0 collective-permute-done.7.refs_1_
  43.4 1.8 %expert_rows.5 = (bf16[64,2048]{1,0:T(8,128)(2,1)S(1)}, bf16[64,2048]{1,0:T(8,128)(2,1)S(1)}) custom-call(f32[1,2048]{1,0:T(1,128)S(1)} %bitcast.5, bf16[2048,512]{1,0:T(8,128)(2,1)S(1)} %get-tuple-element.15.wg_ref, bf16[2048,512]{1,0:T(8,128)(2,1)S(1)} %get-tuple-element.16.wu_ref, bf16[512,2048]{1,0:T(8,128)(2,1)S(1)} %load_weights.3.wd_ref, ...), custom_call_target="tpu_custom_call" | custom-call | flops 805306368 | bytes 6291456 | tf_op jit(solution)/shard_map/expert_rows/pallas_call | solution.py:74
  45.2 0.1 collective-permute-start.8
  45.3 1.8 %expert_rows.4 = (bf16[64,2048]{1,0:T(8,128)(2,1)S(1)}, bf16[64,2048]{1,0:T(8,128)(2,1)S(1)}) custom-call(f32[1,2048]{1,0:T(1,128)S(1)} %bitcast.6, bf16[2048,512]{1,0:T(8,128)(2,1)S(1)} %get-tuple-element.15.wg_ref, bf16[2048,512]{1,0:T(8,128)(2,1)S(1)} %get-tuple-element.16.wu_ref, bf16[512,2048]{1,0:T(8,128)(2,1)S(1)} %load_weights.3.wd_ref, ...), custom_call_target="tpu_custom_call" | custom-call | flops 805306368 | bytes 6291456 | tf_op jit(solution)/shard_map/expert_rows/pallas_call | solution.py:74
  47.1 0.6 collective-permute-start.5
  47.7 0.0 collective-permute-done.18
  47.7 2.6 %collective-permute-start.19 = (f32[1,128]{1,0:T(1,128)S(1)}, f32[1,128]{1,0:T(1,128)S(1)}, u32[]{:S(2)}, u32[]{:S(2)}) collective-permute-start(f32[1,128]{1,0:T(1,128)S(1)} %slice_add_fusion), channel_id=1, source_target_pairs={{0,16},{8,24},{16,0},{24,8},{1,17},{9,25},{17,1},{25,9},{2,18},{10... | collective-permute-start | bytes 1544 | tf_op jit(solution)/shard_map/ppermute | solution.py:325
  50.3 1.0 %collective-permute-start.6 = (bf16[64,2048]{1,0:T(8,128)(2,1)S(1)}, bf16[64,2048]{1,0:T(8,128)(2,1)S(1)}, u32[]{:S(2)}, u32[]{:S(2)}) collective-permute-start(bf16[64,2048]{1,0:T(8,128)(2,1)S(1)} %get-tuple-element.18), channel_id=1, source_target_pairs={{0,5},{1,2},{2,7},{3,0},{4,1},{5,6},{6,3},{7,4},{8,13},{9,10},{10,... | collective-permute-start | bytes 786440 | tf_op jit(solution)/shard_map/ppermute | solution.py:256
  51.3 1.8 %expert_rows.6 = (bf16[64,2048]{1,0:T(8,128)(2,1)S(1)}, bf16[64,2048]{1,0:T(8,128)(2,1)S(1)}) custom-call(f32[1,2048]{1,0:T(1,128)S(1)} %bitcast.7, bf16[2048,512]{1,0:T(8,128)(2,1)S(1)} %get-tuple-element.15.wg_ref, bf16[2048,512]{1,0:T(8,128)(2,1)S(1)} %get-tuple-element.16.wu_ref, bf16[512,2048]{1,0:T(8,128)(2,1)S(1)} %load_weights.3.wd_ref, ...), custom_call_target="tpu_custom_call" | custom-call | flops 805306368 | bytes 6291456 | tf_op jit(solution)/shard_map/expert_rows/pallas_call | solution.py:74
  53.2 0.0 copy-start.1
  53.2 0.0 copy-start.2
  53.2 0.0 copy-start.3
  53.2 1.4 %collective-permute-start.11 = (bf16[64,2048]{1,0:T(8,128)(2,1)S(1)}, bf16[64,2048]{1,0:T(8,128)(2,1)S(1)}, u32[]{:S(2)}, u32[]{:S(2)}) collective-permute-start(bf16[64,2048]{1,0:T(8,128)(2,1)S(1)} %get-tuple-element.24), channel_id=1, source_target_pairs={{0,4},{1,3},{2,6},{3,1},{4,0},{5,7},{6,2},{7,5},{8,12},{9,11},{10,... | collective-permute-start | bytes 786440 | tf_op jit(solution)/shard_map/ppermute | solution.py:256
  54.6 1.8 %expert_rows.7 = (bf16[64,2048]{1,0:T(8,128)(2,1)S(1)}, bf16[64,2048]{1,0:T(8,128)(2,1)S(1)}) custom-call(f32[1,2048]{1,0:T(1,128)S(1)} %bitcast.8, bf16[2048,512]{1,0:T(8,128)(2,1)S(1)} %get-tuple-element.15.wg_ref, bf16[2048,512]{1,0:T(8,128)(2,1)S(1)} %get-tuple-element.16.wu_ref, bf16[512,2048]{1,0:T(8,128)(2,1)S(1)} %load_weights.3.wd_ref, ...), custom_call_target="tpu_custom_call" | custom-call | flops 805306368 | bytes 6291456 | tf_op jit(solution)/shard_map/expert_rows/pallas_call | solution.py:74
  56.4 0.7 collective-permute-start.12
  57.1 1.3 %collective-permute-start.16 = (bf16[64,2048]{1,0:T(8,128)(2,1)S(1)}, bf16[64,2048]{1,0:T(8,128)(2,1)S(1)}, u32[]{:S(2)}, u32[]{:S(2)}) collective-permute-start(bf16[64,2048]{1,0:T(8,128)(2,1)S(1)} %get-tuple-element.26), channel_id=1, source_target_pairs={{0,6},{1,7},{2,4},{3,5},{4,2},{5,3},{6,0},{7,1},{8,14},{9,15},{10,... | collective-permute-start | bytes 786440 | tf_op jit(solution)/shard_map/ppermute | solution.py:256
  58.4 1.2 %collective-permute-start.17 = (bf16[64,2048]{1,0:T(8,128)(2,1)S(1)}, bf16[64,2048]{1,0:T(8,128)(2,1)S(1)}, u32[]{:S(2)}, u32[]{:S(2)}) collective-permute-start(bf16[64,2048]{1,0:T(8,128)(2,1)S(1)} %get-tuple-element.27), channel_id=1, source_target_pairs={{0,7},{1,6},{2,5},{3,4},{4,3},{5,2},{6,1},{7,0},{8,15},{9,14},{10,... | collective-permute-start | bytes 786440 | tf_op jit(solution)/shard_map/ppermute | solution.py:256
  59.6 1.0 %shared_rows.1.base_ref = f32[128,2048]{1,0:T(8,128)S(1)} custom-call(bf16[128,2048]{1,0:T(8,128)(2,1)S(1)} %copy-done, f32[1,2048]{1,0:T(1,128)S(1)} %bitcast.9, bf16[2048,256]{1,0:T(8,128)(2,1)S(1)} %copy-done.1, bf16[2048,256]{1,0:T(8,128)(2,1)S(1)} %copy-done.2, bf16[256,2048]{1,0:T(8,128)(2,1)S(1)} %copy-done.3), custom_call_target="tpu_custom_call" | custom-call | tf_op jit(solution)/shard_map/shared_rows/pallas_call | solution.py:298
  60.6 0.5 multiply_bitcast_fusion
  61.1 0.7 combine_rows.1
  61.9 2.5 %collective-permute-done.12.refs_1_ = bf16[64,2048]{1,0:T(8,128)(2,1)S(1)} collective-permute-done((bf16[64,2048]{1,0:T(8,128)(2,1)S(1)}, bf16[64,2048]{1,0:T(8,128)(2,1)S(1)}, u32[]{:S(2)}, u32[]{:S(2)}) %collective-permute-start.12) | collective-permute-done | bytes 262176 | tf_op jit(solution)/shard_map/ppermute | solution.py:256
  64.4 6.0 %collective-permute-done.16.refs_2_ = bf16[64,2048]{1,0:T(8,128)(2,1)S(1)} collective-permute-done((bf16[64,2048]{1,0:T(8,128)(2,1)S(1)}, bf16[64,2048]{1,0:T(8,128)(2,1)S(1)}, u32[]{:S(2)}, u32[]{:S(2)}) %collective-permute-start.16) | collective-permute-done | bytes 262176 | tf_op jit(solution)/shard_map/ppermute | solution.py:256
  70.4 1.8 %collective-permute-done.17.refs_3_ = bf16[64,2048]{1,0:T(8,128)(2,1)S(1)} collective-permute-done((bf16[64,2048]{1,0:T(8,128)(2,1)S(1)}, bf16[64,2048]{1,0:T(8,128)(2,1)S(1)}, u32[]{:S(2)}, u32[]{:S(2)}) %collective-permute-start.17) | collective-permute-done | bytes 262176 | tf_op jit(solution)/shard_map/ppermute | solution.py:256
  72.2 1.2 %finish_rows.1 = bf16[128,2048]{1,0:T(8,128)(2,1)} custom-call(bf16[256,256]{1,0:T(8,128)(2,1)S(1)} %get-tuple-element.21.picks_ref, f32[128,2]{1,0:T(8,128)S(1)} %get-tuple-element.22.gates_ref, f32[128,2048]{1,0:T(8,128)S(1)} %get-tuple-element.23.base_ref, bf16[64,2048]{1,0:T(8,128)(2,1)S(1)} %collective-permute-done.11.refs_0_, ...), custom_call_target="tpu_custom_call" | custom-call | tf_op jit(solution)/shard_map/finish_rows/pallas_call | solution.py:223
  (23 shorter events, 0.1 us)
Async XLA Ops:
  0.6 15.6 %collective-permute-start = (bf16[128,2048]{1,0:T(8,128)(2,1)}, bf16[128,2048]{1,0:T(8,128)(2,1)S(1)}, u32[]{:S(2)}, u32[]{:S(2)}) collective-permute-start(bf16[128,2048]{1,0:T(8,128)(2,1)} %refs_0_.5), channel_id=1, source_target_pairs={{0,2},{1,5},{2,0},{3,7},{4,6},{5,1},{6,4},{7,3},{8,10},{9,13},{10,... | collective-permute-start | bytes 1572872 | tf_op jit(solution)/shard_map/ppermute | solution.py:256
  3.7 14.5 %collective-permute-start.9 = (bf16[128,2048]{1,0:T(8,128)(2,1)}, bf16[128,2048]{1,0:T(8,128)(2,1)S(1)}, u32[]{:S(2)}, u32[]{:S(2)}) collective-permute-start(bf16[128,2048]{1,0:T(8,128)(2,1)} %refs_0_.5), channel_id=1, source_target_pairs={{0,4},{1,3},{2,6},{3,1},{4,0},{5,7},{6,2},{7,5},{8,12},{9,11},{10,... | collective-permute-start | bytes 1572872 | tf_op jit(solution)/shard_map/ppermute | solution.py:256
  16.2 9.2 %collective-permute-start.13 = (bf16[128,2048]{1,0:T(8,128)(2,1)S(1)}, bf16[128,2048]{1,0:T(8,128)(2,1)S(1)}, u32[]{:S(2)}, u32[]{:S(2)}) collective-permute-start(bf16[128,2048]{1,0:T(8,128)(2,1)S(1)} %collective-permute-done.refs_0_), channel_id=1, source_target_pairs={{0,4},{1,3},{2,6},{3,1},{4,0},{5,7},{6,2},{7,5},{8,12},{9,11},{10,... | collective-permute-start | bytes 1572872 | tf_op jit(solution)/shard_map/ppermute | solution.py:256
  17.6 25.7 %collective-permute-start.7 = (bf16[128,2048]{1,0:T(8,128)(2,1)}, bf16[128,2048]{1,0:T(8,128)(2,1)S(1)}, u32[]{:S(2)}, u32[]{:S(2)}) collective-permute-start(bf16[128,2048]{1,0:T(8,128)(2,1)} %refs_0_.5), channel_id=1, source_target_pairs={{0,1},{1,0},{2,3},{3,2},{4,5},{5,4},{6,7},{7,6},{8,9},{9,8},{10,11... | collective-permute-start | bytes 1572872 | tf_op jit(solution)/shard_map/ppermute | solution.py:256
  17.6 27.6 %collective-permute-start.1 = (bf16[128,2048]{1,0:T(8,128)(2,1)S(1)}, bf16[128,2048]{1,0:T(8,128)(2,1)S(1)}, u32[]{:S(2)}, u32[]{:S(2)}) collective-permute-start(bf16[128,2048]{1,0:T(8,128)(2,1)S(1)} %collective-permute-done.refs_0_), channel_id=1, source_target_pairs={{0,1},{1,0},{2,3},{3,2},{4,5},{5,4},{6,7},{7,6},{8,9},{9,8},{10,11... | collective-permute-start | bytes 1572872 | tf_op jit(solution)/shard_map/ppermute | solution.py:256
  18.2 32.2 %collective-permute-start.10 = (bf16[128,2048]{1,0:T(8,128)(2,1)S(1)}, bf16[128,2048]{1,0:T(8,128)(2,1)S(1)}, u32[]{:S(2)}, u32[]{:S(2)}) collective-permute-start(bf16[128,2048]{1,0:T(8,128)(2,1)S(1)} %collective-permute-done.9.refs_0_), channel_id=1, source_target_pairs={{0,1},{1,0},{2,3},{3,2},{4,5},{5,4},{6,7},{7,6},{8,9},{9,8},{10,11... | collective-permute-start | bytes 1572872 | tf_op jit(solution)/shard_map/ppermute | solution.py:256
  25.4 27.8 %collective-permute-start.14 = (bf16[128,2048]{1,0:T(8,128)(2,1)S(1)}, bf16[128,2048]{1,0:T(8,128)(2,1)S(1)}, u32[]{:S(2)}, u32[]{:S(2)}) collective-permute-start(bf16[128,2048]{1,0:T(8,128)(2,1)S(1)} %collective-permute-done.13.refs_0_), channel_id=1, source_target_pairs={{0,1},{1,0},{2,3},{3,2},{4,5},{5,4},{6,7},{7,6},{8,9},{9,8},{10,11... | collective-permute-start | bytes 1572872 | tf_op jit(solution)/shard_map/ppermute | solution.py:256
  25.4 1.9 %collective-permute-start.2 = (s32[2,128]{1,0:T(2,128)}, s32[2,128]{1,0:T(2,128)S(1)}, u32[]{:S(2)}, u32[]{:S(2)}) collective-permute-start(s32[2,128]{1,0:T(2,128)} %bitcast.10), channel_id=1, source_target_pairs={{0,1},{1,0},{2,3},{3,2},{4,5},{5,4},{6,7},{7,6},{8,9},{9,8},{10,11... | collective-permute-start | bytes 3080 | tf_op jit(solution)/shard_map/ppermute | solution.py:256
  27.3 0.7 copy-start.5
  28.0 3.9 %collective-permute-start.3 = (s32[4,128]{1,0:T(4,128)S(1)}, s32[4,128]{1,0:T(4,128)S(1)}, u32[]{:S(2)}, u32[]{:S(2)}) collective-permute-start(s32[4,128]{1,0:T(4,128)S(1)} %pair_routes.1.refs_2_.refs_3_.refs_0_), channel_id=1, source_target_pairs={{0,2},{1,5},{2,0},{3,7},{4,6},{5,1},{6,4},{7,3},{8,10},{9,13},{10,... | collective-permute-start | bytes 6152 | tf_op jit(solution)/shard_map/ppermute | solution.py:256
  31.9 3.6 %collective-permute-start.4 = (s32[4,128]{1,0:T(4,128)S(1)}, s32[4,128]{1,0:T(4,128)S(1)}, u32[]{:S(2)}, u32[]{:S(2)}) collective-permute-start(s32[4,128]{1,0:T(4,128)S(1)} %pair_routes.1.refs_2_.refs_3_.refs_0_), channel_id=1, source_target_pairs={{0,4},{1,3},{2,6},{3,1},{4,0},{5,7},{6,2},{7,5},{8,12},{9,11},{10,... | collective-permute-start | bytes 6152 | tf_op jit(solution)/shard_map/ppermute | solution.py:256
  35.5 6.0 %collective-permute-start.15 = (s32[4,128]{1,0:T(4,128)S(1)}, s32[4,128]{1,0:T(4,128)S(1)}, u32[]{:S(2)}, u32[]{:S(2)}) collective-permute-start(s32[4,128]{1,0:T(4,128)S(1)} %pair_routes.1.refs_2_.refs_3_.refs_0_), channel_id=1, source_target_pairs={{0,6},{1,7},{2,4},{3,5},{4,2},{5,3},{6,0},{7,1},{8,14},{9,15},{10,... | collective-permute-start | bytes 6152 | tf_op jit(solution)/shard_map/ppermute | solution.py:256
  39.2 4.1 %copy-start = (bf16[128,2048]{1,0:T(8,128)(2,1)S(1)}, bf16[128,2048]{1,0:T(8,128)(2,1)}, u32[]{:S(2)}) copy-start(bf16[128,2048]{1,0:T(8,128)(2,1)} %refs_0_.5) | copy-start | bytes 1572868
  39.2 4.1 %copy-start.4 = (f32[2048]{0:T(1024)S(1)}, f32[2048]{0:T(1024)}, u32[]{:S(2)}) copy-start(f32[2048]{0:T(1024)} %param.11) | copy-start | bytes 24580
  41.8 5.9 %collective-permute-start.18 = (f32[1,128]{1,0:T(1,128)S(1)}, f32[1,128]{1,0:T(1,128)S(1)}, u32[]{:S(2)}, u32[]{:S(2)}) collective-permute-start(f32[1,128]{1,0:T(1,128)S(1)} %slice.6), channel_id=1, source_target_pairs={{0,8},{8,0},{16,24},{24,16},{1,9},{9,1},{17,25},{25,17},{2,10},{10... | collective-permute-start | bytes 1544 | tf_op jit(solution)/shard_map/ppermute | solution.py:325
  45.2 11.9 %collective-permute-start.8 = (bf16[64,2048]{1,0:T(8,128)(2,1)S(1)}, bf16[64,2048]{1,0:T(8,128)(2,1)S(1)}, u32[]{:S(2)}, u32[]{:S(2)}) collective-permute-start(bf16[64,2048]{1,0:T(8,128)(2,1)S(1)} %get-tuple-element.20), channel_id=1, source_target_pairs={{0,1},{1,0},{2,3},{3,2},{4,5},{5,4},{6,7},{7,6},{8,9},{9,8},{10,11... | collective-permute-start | bytes 786440 | tf_op jit(solution)/shard_map/ppermute | solution.py:256
  47.1 11.3 %collective-permute-start.5 = (bf16[64,2048]{1,0:T(8,128)(2,1)S(1)}, bf16[64,2048]{1,0:T(8,128)(2,1)S(1)}, u32[]{:S(2)}, u32[]{:S(2)}) collective-permute-start(bf16[64,2048]{1,0:T(8,128)(2,1)S(1)} %get-tuple-element.17), channel_id=1, source_target_pairs={{0,2},{1,5},{2,0},{3,7},{4,6},{5,1},{6,4},{7,3},{8,10},{9,13},{10,... | collective-permute-start | bytes 786440 | tf_op jit(solution)/shard_map/ppermute | solution.py:256
  47.7 8.7 %collective-permute-start.19 = (f32[1,128]{1,0:T(1,128)S(1)}, f32[1,128]{1,0:T(1,128)S(1)}, u32[]{:S(2)}, u32[]{:S(2)}) collective-permute-start(f32[1,128]{1,0:T(1,128)S(1)} %slice_add_fusion), channel_id=1, source_target_pairs={{0,16},{8,24},{16,0},{24,8},{1,17},{9,25},{17,1},{25,9},{2,18},{10... | collective-permute-start | bytes 1544 | tf_op jit(solution)/shard_map/ppermute | solution.py:325
  50.3 10.8 %collective-permute-start.6 = (bf16[64,2048]{1,0:T(8,128)(2,1)S(1)}, bf16[64,2048]{1,0:T(8,128)(2,1)S(1)}, u32[]{:S(2)}, u32[]{:S(2)}) collective-permute-start(bf16[64,2048]{1,0:T(8,128)(2,1)S(1)} %get-tuple-element.18), channel_id=1, source_target_pairs={{0,5},{1,2},{2,7},{3,0},{4,1},{5,6},{6,3},{7,4},{8,13},{9,10},{10,... | collective-permute-start | bytes 786440 | tf_op jit(solution)/shard_map/ppermute | solution.py:256
  53.2 6.4 %copy-start.1 = (bf16[2048,256]{1,0:T(8,128)(2,1)S(1)}, bf16[2048,256]{1,0:T(8,128)(2,1)}, u32[]{:S(2)}) copy-start(bf16[2048,256]{1,0:T(8,128)(2,1)} %wg_ref.1) | copy-start | bytes 3145732
  53.2 6.4 %copy-start.2 = (bf16[2048,256]{1,0:T(8,128)(2,1)S(1)}, bf16[2048,256]{1,0:T(8,128)(2,1)}, u32[]{:S(2)}) copy-start(bf16[2048,256]{1,0:T(8,128)(2,1)} %wu_ref.1) | copy-start | bytes 3145732
  53.2 6.4 %copy-start.3 = (bf16[256,2048]{1,0:T(8,128)(2,1)S(1)}, bf16[256,2048]{1,0:T(8,128)(2,1)}, u32[]{:S(2)}) copy-start(bf16[256,2048]{1,0:T(8,128)(2,1)} %wd_ref.1) | copy-start | bytes 3145732
  53.2 8.6 %collective-permute-start.11 = (bf16[64,2048]{1,0:T(8,128)(2,1)S(1)}, bf16[64,2048]{1,0:T(8,128)(2,1)S(1)}, u32[]{:S(2)}, u32[]{:S(2)}) collective-permute-start(bf16[64,2048]{1,0:T(8,128)(2,1)S(1)} %get-tuple-element.24), channel_id=1, source_target_pairs={{0,4},{1,3},{2,6},{3,1},{4,0},{5,7},{6,2},{7,5},{8,12},{9,11},{10,... | collective-permute-start | bytes 786440 | tf_op jit(solution)/shard_map/ppermute | solution.py:256
  56.4 8.0 %collective-permute-start.12 = (bf16[64,2048]{1,0:T(8,128)(2,1)S(1)}, bf16[64,2048]{1,0:T(8,128)(2,1)S(1)}, u32[]{:S(2)}, u32[]{:S(2)}) collective-permute-start(bf16[64,2048]{1,0:T(8,128)(2,1)S(1)} %get-tuple-element.25), channel_id=1, source_target_pairs={{0,3},{1,4},{2,1},{3,6},{4,7},{5,0},{6,5},{7,2},{8,11},{9,12},{10,... | collective-permute-start | bytes 786440 | tf_op jit(solution)/shard_map/ppermute | solution.py:256
  57.1 13.3 %collective-permute-start.16 = (bf16[64,2048]{1,0:T(8,128)(2,1)S(1)}, bf16[64,2048]{1,0:T(8,128)(2,1)S(1)}, u32[]{:S(2)}, u32[]{:S(2)}) collective-permute-start(bf16[64,2048]{1,0:T(8,128)(2,1)S(1)} %get-tuple-element.26), channel_id=1, source_target_pairs={{0,6},{1,7},{2,4},{3,5},{4,2},{5,3},{6,0},{7,1},{8,14},{9,15},{10,... | collective-permute-start | bytes 786440 | tf_op jit(solution)/shard_map/ppermute | solution.py:256
  58.4 2.7 %copy-start.6 = (s32[128,2]{0,1:T(2,128)S(1)}, s32[128,2]{0,1:T(2,128)}, u32[]{:S(2)}) copy-start(s32[128,2]{0,1:T(2,128)} %param.12) | copy-start | bytes 3076
  58.4 2.7 %copy-start.7 = (f32[128,2]{0,1:T(2,128)S(1)}, f32[128,2]{0,1:T(2,128)}, u32[]{:S(2)}) copy-start(f32[128,2]{0,1:T(2,128)} %param.13) | copy-start | bytes 3076
  58.4 13.8 %collective-permute-start.17 = (bf16[64,2048]{1,0:T(8,128)(2,1)S(1)}, bf16[64,2048]{1,0:T(8,128)(2,1)S(1)}, u32[]{:S(2)}, u32[]{:S(2)}) collective-permute-start(bf16[64,2048]{1,0:T(8,128)(2,1)S(1)} %get-tuple-element.27), channel_id=1, source_target_pairs={{0,7},{1,6},{2,5},{3,4},{4,3},{5,2},{6,1},{7,0},{8,15},{9,14},{10,... | collective-permute-start | bytes 786440 | tf_op jit(solution)/shard_map/ppermute | solution.py:256

commit v4 on v3

--- a/solution.py
+++ b/solution.py
@@ -128,8 +128,8 @@
     sources, targets, sems = refs[:count], refs[count : 2 * count], refs[2 * count]
     copies = []
     for i, (source, target) in enumerate(zip(sources, targets)):
-        part = target.shape[0] // 4
-        for j in range(4):
+        part = target.shape[0] // 8
+        for j in range(8):
             piece = pl.ds(j * part, part)
             copies.append(
                 pltpu.make_async_copy(source.at[0, piece], target.at[piece], sems.at[i, j])
@@ -147,7 +147,7 @@
         out_shape=[jax.ShapeDtypeStruct(w.shape[1:], w.dtype) for w in weights],
         in_specs=[pl.BlockSpec(memory_space=pltpu.HBM)] * count,
         out_specs=[VMEM] * count,
-        scratch_shapes=[pltpu.SemaphoreType.DMA((count, 4))],
+        scratch_shapes=[pltpu.SemaphoreType.DMA((count, 8))],
         compiler_params=pltpu.CompilerParams(vmem_limit_bytes=16 * 2**20),
         name="load_weights",
     )(*[pltpu.with_memory_space_constraint(w, pltpu.HBM) for w in weights])
@@ -173,12 +173,17 @@
 
 
 def combine_kernel(early, late, routes_ref, gates_ref, base_ref, *refs):
-    blocks, (out_ref, picks_ref, gates_out) = refs[:-3], refs[-3:]
+    blocks, (out_ref, picks_ref, gates_out, last_ref, gate_ref) = refs[:-5], refs[-5:]
     rows, slots = base_ref.shape[0], blocks[0].shape[0]
     before = before_mask(rows)
     gates = gates_ref[...].T
     gates_out[...] = gates
-    picks_ref[...] = picks_of(routes_ref, late, slots, before)
+    picks_ref[...] = picks_of(routes_ref, late[:-1], slots, before)
+    first, second = routes_ref[0:1, :], routes_ref[1:2, :]
+    expert = origin_id(late[-1])
+    last_ref[...] = places(first, second, expert, slots, before).T.astype(BF16)
+    scale = jnp.where(first == expert, gates_ref[0:1, :], gates_ref[1:2, :])
+    gate_ref[...] = jnp.broadcast_to(scale, (8, rows)).T[:, 0:1]
     values = jnp.concatenate([block[...] for block in blocks], axis=0)
     chosen = dot(picks_of(routes_ref, early, slots, before), values)
     out_ref[...] = (
@@ -186,49 +191,68 @@
     )
 
 
-def finish_kernel(pieces, picks_ref, gates_ref, base_ref, *refs):
-    blocks, (out_ref, mixed, sems) = refs[:-3], refs[-3:]
-    rows, width = base_ref.shape
-    part = width // pieces
+def combine_call(early, late, routes, gates, base, blocks):
+    rows, slots = base.shape[0], blocks[0].shape[0]
+    return pl.pallas_call(
+        functools.partial(combine_kernel, early, late),
+        out_shape=[
+            jax.ShapeDtypeStruct(base.shape, F32),
+            jax.ShapeDtypeStruct((2 * rows, slots * (len(late) - 1)), BF16),
+            jax.ShapeDtypeStruct((rows, gates.shape[0]), F32),
+            jax.ShapeDtypeStruct((rows, slots), BF16),
+            jax.ShapeDtypeStruct((rows, 1), F32),
+        ],
+        in_specs=[VMEM] * (3 + len(blocks)),
+        out_specs=[VMEM] * 5,
+        compiler_params=pltpu.CompilerParams(vmem_limit_bytes=24 * 2**20),
+        name="combine_rows",
+    )(routes, gates, base, *blocks)
+
+
+def middle_kernel(picks_ref, gates_ref, base_ref, *refs):
+    blocks, out_ref = refs[:-1], refs[-1]
+    rows = base_ref.shape[0]
+    values = jnp.concatenate([block[...] for block in blocks], axis=0)
+    chosen = dot(picks_ref[...], values)
+    total = base_ref[...] + gates_ref[:, 0:1] * chosen[:rows]
+    out_ref[...] = total + gates_ref[:, 1:2] * chosen[rows:]
+
+
+def middle_call(picks, gates, base, blocks):
+    return pl.pallas_call(
+        middle_kernel,
+        out_shape=jax.ShapeDtypeStruct(base.shape, F32),
+        in_specs=[VMEM] * (3 + len(blocks)),
+        out_specs=VMEM,
+        compiler_params=pltpu.CompilerParams(vmem_limit_bytes=24 * 2**20),
+        name="middle_rows",
+    )(picks, gates, base, *blocks)
+
+
+def finish_kernel(pieces, pick_ref, gate_ref, base_ref, block_ref, out_ref, mixed, sems):
+    part = base_ref.shape[1] // pieces
+    gate = gate_ref[...]
     copies = []
     for j in range(pieces):
         cols = slice(j * part, (j + 1) * part)
-        values = jnp.concatenate([block[:, cols] for block in blocks], axis=0)
-        chosen = dot(picks_ref[...], values)
-        total = base_ref[:, cols] + gates_ref[:, 0:1] * chosen[:rows]
-        mixed[:, cols] = (total + gates_ref[:, 1:2] * chosen[rows:]).astype(mixed.dtype)
+        total = base_ref[:, cols] + gate * dot(pick_ref[...], block_ref[:, cols])
+        mixed[:, cols] = total.astype(mixed.dtype)
         copies.append(pltpu.make_async_copy(mixed.at[:, cols], out_ref.at[:, cols], sems.at[j]))
         copies[-1].start()
     for copy in copies:
         copy.wait()
 
 
-def combine_call(early, late, routes, gates, base, blocks):
-    rows, slots = base.shape[0], blocks[0].shape[0]
-    return pl.pallas_call(
-        functools.partial(combine_kernel, early, late),
-        out_shape=[
-            jax.ShapeDtypeStruct(base.shape, F32),
-            jax.ShapeDtypeStruct((2 * rows, slots * len(late)), BF16),
-            jax.ShapeDtypeStruct((rows, gates.shape[0]), F32),
-        ],
-        in_specs=[VMEM] * (3 + len(blocks)),
-        out_specs=[VMEM] * 3,
-        compiler_params=pltpu.CompilerParams(vmem_limit_bytes=24 * 2**20),
-        name="combine_rows",
-    )(routes, gates, base, *blocks)
-
-
-def finish_call(picks, gates, base, blocks, pieces=4):
+def finish_call(pick, gate, base, block, pieces=4):
     return pl.pallas_call(
         functools.partial(finish_kernel, pieces),
         out_shape=jax.ShapeDtypeStruct(base.shape, BF16),
-        in_specs=[VMEM] * (3 + len(blocks)),
+        in_specs=[VMEM] * 4,
         out_specs=pl.BlockSpec(memory_space=pltpu.HBM),
         scratch_shapes=[pltpu.VMEM(base.shape, BF16), pltpu.SemaphoreType.DMA((pieces,))],
         compiler_params=pltpu.CompilerParams(vmem_limit_bytes=24 * 2**20),
         name="finish_rows",
-    )(picks, gates, base, *blocks)
+    )(pick, gate, base, block)
 
 
 def per_device(
@@ -260,7 +284,7 @@
 
     masks = [1 << b for b in range(1, groups.bit_length() - 1)]
     hops = [
-        np.where(ids % 2 == 0, ids ^ masks[i], ids ^ masks[-1 - i]) for i in range(len(masks))
+        np.where(ids % 2 == 1, ids ^ masks[i], ids ^ masks[-1 - i]) for i in range(len(masks))
     ]
     both = pair_call(routes, send(routes, partner))
     known, metas = [(tokens, ids)], [both]
@@ -308,7 +332,7 @@
     if len(returned) > 2:
         late = returned.pop(-2) + late
     early = [item for back in returned for item in back]
-    base, picks, columns = combine_call(
+    base, picks, columns, pick, gate = combine_call(
         [masks_of(origin) for _, origin in early],
         [masks_of(origin) for _, origin in late],
         routes,
@@ -316,7 +340,8 @@
         base,
         [block for block, _ in early],
     )
-    mixed = finish_call(picks, columns, base, [block for block, _ in late])
+    base = middle_call(picks, columns, base, [block for block, _ in late[:-1]])
+    mixed = finish_call(pick, gate, base, late[-1][0])
 
     if planes & (planes - 1):
         total = lax.psum(total, "ep")

time: 74.7 us -> 75.1 us (level); the launches traced: 73.4 us -> 74.9 us
  waiting for transfers between devices: 34 us -> 35.3 us
    ppermute x18, waiting for transfers between devices: 34 us -> 35.3 us  [send(): return lax.ppermute(value, 'tp', [(int(i), int(perm[i])) for i in ids])]
where the time goes in v4:
time: 75.1 us; the launch traced here: 74.9 us
  waiting for transfers between devices  35.3 us (47%)
  starting transfers between devices  22.9 us (30%)
  Pallas kernels  14.6 us (19%)
  between operations  0.82 us (1%)
    ppermute x18, waiting for transfers between devices, send(): return lax.ppermute(value, 'tp', [(int(i), int(perm[i])) for i in ids])  35.3 us
    ppermute x18, starting transfers between devices, send(): return lax.ppermute(value, 'tp', [(int(i), int(perm[i])) for i in ids])  18.7 us
    pallas_call x4, Pallas kernels, expert_call(): pl.pallas_call(functools.partial(expert_kernel, count, slots, halves), ou...  7.3 us
    ppermute x2, starting transfers between devices, per_device(): lax.ppermute(total, 'ep', [(i, i ^ 1 << bit) for i in range(planes)])  4.17 us
    pallas_call x2, Pallas kernels, load_call(): pl.pallas_call(functools.partial(load_kernel, count), out_shape=[jax.Shap...  3.9 us
  transfers between devices with their start and end apart: 20, of which 8 were waited for; matrix products, arithmetic and copies ran while one was open for 1% of the time, Pallas kernels for 18%

profile of v4, /device:TPU:0, one launch (start us, length us, event | category | flops | bytes accessed | tf_op | source)
XLA Modules:
  0.0 74.9 jit_solution(16236641201594578972)
XLA Ops:
  0.6 3.1 %collective-permute-start = (bf16[128,2048]{1,0:T(8,128)(2,1)}, bf16[128,2048]{1,0:T(8,128)(2,1)S(1)}, u32[]{:S(2)}, u32[]{:S(2)}) collective-permute-start(bf16[128,2048]{1,0:T(8,128)(2,1)} %refs_0_.5), channel_id=1, source_target_pairs={{0,4},{1,3},{2,6},{3,1},{4,0},{5,7},{6,2},{7,5},{8,12},{9,11},{10,... | collective-permute-start | bytes 1572872 | tf_op jit(solution)/shard_map/ppermute | solution.py:280
  3.7 1.5 %collective-permute-start.9 = (bf16[128,2048]{1,0:T(8,128)(2,1)}, bf16[128,2048]{1,0:T(8,128)(2,1)S(1)}, u32[]{:S(2)}, u32[]{:S(2)}) collective-permute-start(bf16[128,2048]{1,0:T(8,128)(2,1)} %refs_0_.5), channel_id=1, source_target_pairs={{0,2},{1,5},{2,0},{3,7},{4,6},{5,1},{6,4},{7,3},{8,10},{9,13},{10,... | collective-permute-start | bytes 1572872 | tf_op jit(solution)/shard_map/ppermute | solution.py:280
  5.2 11.1 %collective-permute-done.refs_0_ = bf16[128,2048]{1,0:T(8,128)(2,1)S(1)} collective-permute-done((bf16[128,2048]{1,0:T(8,128)(2,1)}, bf16[128,2048]{1,0:T(8,128)(2,1)S(1)}, u32[]{:S(2)}, u32[]{:S(2)}) %collective-permute-start) | collective-permute-done | bytes 524320 | tf_op jit(solution)/shard_map/ppermute | solution.py:280
  16.2 1.4 %collective-permute-start.13 = (bf16[128,2048]{1,0:T(8,128)(2,1)S(1)}, bf16[128,2048]{1,0:T(8,128)(2,1)S(1)}, u32[]{:S(2)}, u32[]{:S(2)}) collective-permute-start(bf16[128,2048]{1,0:T(8,128)(2,1)S(1)} %collective-permute-done.refs_0_), channel_id=1, source_target_pairs={{0,2},{1,5},{2,0},{3,7},{4,6},{5,1},{6,4},{7,3},{8,10},{9,13},{10,... | collective-permute-start | bytes 1572872 | tf_op jit(solution)/shard_map/ppermute | solution.py:280
  17.6 0.0 collective-permute-start.7
  17.6 0.5 collective-permute-start.1
  18.2 0.0 collective-permute-start.10
  18.2 7.3 %collective-permute-done.13.refs_0_ = bf16[128,2048]{1,0:T(8,128)(2,1)S(1)} collective-permute-done((bf16[128,2048]{1,0:T(8,128)(2,1)S(1)}, bf16[128,2048]{1,0:T(8,128)(2,1)S(1)}, u32[]{:S(2)}, u32[]{:S(2)}) %collective-permute-start.13) | collective-permute-done | bytes 524320 | tf_op jit(solution)/shard_map/ppermute | solution.py:280
  25.4 0.5 collective-permute-start.2
  25.9 1.4 %collective-permute-done.2.other_ref = s32[2,128]{1,0:T(2,128)S(1)} collective-permute-done((s32[2,128]{1,0:T(2,128)}, s32[2,128]{1,0:T(2,128)S(1)}, u32[]{:S(2)}, u32[]{:S(2)}) %collective-permute-start.2) | collective-permute-done | bytes 1056 | tf_op jit(solution)/shard_map/ppermute | solution.py:280
  27.3 0.7 copy-done.5
  28.0 2.4 %collective-permute-start.3 = (s32[4,128]{1,0:T(4,128)S(1)}, s32[4,128]{1,0:T(4,128)S(1)}, u32[]{:S(2)}, u32[]{:S(2)}) collective-permute-start(s32[4,128]{1,0:T(4,128)S(1)} %pair_routes.1.refs_2_.refs_3_.refs_0_), channel_id=1, source_target_pairs={{0,4},{1,3},{2,6},{3,1},{4,0},{5,7},{6,2},{7,5},{8,12},{9,11},{10,... | collective-permute-start | bytes 6152 | tf_op jit(solution)/shard_map/ppermute | solution.py:280
  30.4 1.6 %collective-permute-done.3.refs_2_.refs_3_.refs_1_ = s32[4,128]{1,0:T(4,128)S(1)} collective-permute-done((s32[4,128]{1,0:T(4,128)S(1)}, s32[4,128]{1,0:T(4,128)S(1)}, u32[]{:S(2)}, u32[]{:S(2)}) %collective-permute-start.3) | collective-permute-done | bytes 2080 | tf_op jit(solution)/shard_map/ppermute | solution.py:280
  32.0 1.0 %collective-permute-start.4 = (s32[4,128]{1,0:T(4,128)S(1)}, s32[4,128]{1,0:T(4,128)S(1)}, u32[]{:S(2)}, u32[]{:S(2)}) collective-permute-start(s32[4,128]{1,0:T(4,128)S(1)} %pair_routes.1.refs_2_.refs_3_.refs_0_), channel_id=1, source_target_pairs={{0,2},{1,5},{2,0},{3,7},{4,6},{5,1},{6,4},{7,3},{8,10},{9,13},{10,... | collective-permute-start | bytes 6152 | tf_op jit(solution)/shard_map/ppermute | solution.py:280
  33.0 2.5 %collective-permute-done.4.refs_3_.refs_2_ = s32[4,128]{1,0:T(4,128)S(1)} collective-permute-done((s32[4,128]{1,0:T(4,128)S(1)}, s32[4,128]{1,0:T(4,128)S(1)}, u32[]{:S(2)}, u32[]{:S(2)}) %collective-permute-start.4) | collective-permute-done | bytes 2080 | tf_op jit(solution)/shard_map/ppermute | solution.py:280
  35.5 2.1 %collective-permute-start.15 = (s32[4,128]{1,0:T(4,128)S(1)}, s32[4,128]{1,0:T(4,128)S(1)}, u32[]{:S(2)}, u32[]{:S(2)}) collective-permute-start(s32[4,128]{1,0:T(4,128)S(1)} %pair_routes.1.refs_2_.refs_3_.refs_0_), channel_id=1, source_target_pairs={{0,6},{1,7},{2,4},{3,5},{4,2},{5,3},{6,0},{7,1},{8,14},{9,15},{10,... | collective-permute-start | bytes 6152 | tf_op jit(solution)/shard_map/ppermute | solution.py:280
  37.7 1.6 %load_weights.3.wd_ref = bf16[512,2048]{1,0:T(8,128)(2,1)S(1)} custom-call(bf16[1,512,2048]{2,1,0:T(8,128)(2,1)} %refs_0_.4), custom_call_target="tpu_custom_call" | custom-call | tf_op jit(solution)/shard_map/load_weights/pallas_call | solution.py:145
  39.3 0.0 copy-start
  39.3 0.0 copy-start.4
  39.3 2.3 %load_weights.2 = (bf16[2048,512]{1,0:T(8,128)(2,1)S(1)}, bf16[2048,512]{1,0:T(8,128)(2,1)S(1)}) custom-call(bf16[1,2048,512]{2,1,0:T(8,128)(2,1)} %refs_0_.3, bf16[1,2048,512]{2,1,0:T(8,128)(2,1)} %refs_1_.1), custom_call_target="tpu_custom_call" | custom-call | tf_op jit(solution)/shard_map/load_weights/pallas_call | solution.py:145
  41.6 0.0 collective-permute-done.15.refs_2_.refs_3_
  41.6 0.2 tally_routes.1
  41.9 1.6 %collective-permute-start.18 = (f32[1,128]{1,0:T(1,128)S(1)}, f32[1,128]{1,0:T(1,128)S(1)}, u32[]{:S(2)}, u32[]{:S(2)}) collective-permute-start(f32[1,128]{1,0:T(1,128)S(1)} %slice.6), channel_id=1, source_target_pairs={{0,8},{8,0},{16,24},{24,16},{1,9},{9,1},{17,25},{25,17},{2,10},{10... | collective-permute-start | bytes 1544 | tf_op jit(solution)/shard_map/ppermute | solution.py:350
  43.5 0.0 collective-permute-done.7.refs_1_
  43.5 1.8 %expert_rows.5 = (bf16[64,2048]{1,0:T(8,128)(2,1)S(1)}, bf16[64,2048]{1,0:T(8,128)(2,1)S(1)}) custom-call(f32[1,2048]{1,0:T(1,128)S(1)} %bitcast.5, bf16[2048,512]{1,0:T(8,128)(2,1)S(1)} %get-tuple-element.17.wg_ref, bf16[2048,512]{1,0:T(8,128)(2,1)S(1)} %get-tuple-element.18.wu_ref, bf16[512,2048]{1,0:T(8,128)(2,1)S(1)} %load_weights.3.wd_ref, ...), custom_call_target="tpu_custom_call" | custom-call | flops 805306368 | bytes 6291456 | tf_op jit(solution)/shard_map/expert_rows/pallas_call | solution.py:74
  45.3 0.1 collective-permute-start.8
  45.4 1.8 %expert_rows.4 = (bf16[64,2048]{1,0:T(8,128)(2,1)S(1)}, bf16[64,2048]{1,0:T(8,128)(2,1)S(1)}) custom-call(f32[1,2048]{1,0:T(1,128)S(1)} %bitcast.6, bf16[2048,512]{1,0:T(8,128)(2,1)S(1)} %get-tuple-element.17.wg_ref, bf16[2048,512]{1,0:T(8,128)(2,1)S(1)} %get-tuple-element.18.wu_ref, bf16[512,2048]{1,0:T(8,128)(2,1)S(1)} %load_weights.3.wd_ref, ...), custom_call_target="tpu_custom_call" | custom-call | flops 805306368 | bytes 6291456 | tf_op jit(solution)/shard_map/expert_rows/pallas_call | solution.py:74
  47.2 0.6 collective-permute-start.5
  47.8 2.6 %collective-permute-start.19 = (f32[1,128]{1,0:T(1,128)S(1)}, f32[1,128]{1,0:T(1,128)S(1)}, u32[]{:S(2)}, u32[]{:S(2)}) collective-permute-start(f32[1,128]{1,0:T(1,128)S(1)} %slice_add_fusion), channel_id=1, source_target_pairs={{0,16},{8,24},{16,0},{24,8},{1,17},{9,25},{17,1},{25,9},{2,18},{10... | collective-permute-start | bytes 1544 | tf_op jit(solution)/shard_map/ppermute | solution.py:350
  50.4 1.1 %collective-permute-start.6 = (bf16[64,2048]{1,0:T(8,128)(2,1)S(1)}, bf16[64,2048]{1,0:T(8,128)(2,1)S(1)}, u32[]{:S(2)}, u32[]{:S(2)}) collective-permute-start(bf16[64,2048]{1,0:T(8,128)(2,1)S(1)} %get-tuple-element.20), channel_id=1, source_target_pairs={{0,3},{1,4},{2,1},{3,6},{4,7},{5,0},{6,5},{7,2},{8,11},{9,12},{10,... | collective-permute-start | bytes 786440 | tf_op jit(solution)/shard_map/ppermute | solution.py:280
  51.4 1.8 %expert_rows.6 = (bf16[64,2048]{1,0:T(8,128)(2,1)S(1)}, bf16[64,2048]{1,0:T(8,128)(2,1)S(1)}) custom-call(f32[1,2048]{1,0:T(1,128)S(1)} %bitcast.7, bf16[2048,512]{1,0:T(8,128)(2,1)S(1)} %get-tuple-element.17.wg_ref, bf16[2048,512]{1,0:T(8,128)(2,1)S(1)} %get-tuple-element.18.wu_ref, bf16[512,2048]{1,0:T(8,128)(2,1)S(1)} %load_weights.3.wd_ref, ...), custom_call_target="tpu_custom_call" | custom-call | flops 805306368 | bytes 6291456 | tf_op jit(solution)/shard_map/expert_rows/pallas_call | solution.py:74
  53.3 0.0 collective-permute-done.14.refs_1_
  53.3 0.0 copy-start.1
  53.3 0.0 copy-start.2
  53.3 0.0 copy-start.3
  53.3 1.4 %collective-permute-start.11 = (bf16[64,2048]{1,0:T(8,128)(2,1)S(1)}, bf16[64,2048]{1,0:T(8,128)(2,1)S(1)}, u32[]{:S(2)}, u32[]{:S(2)}) collective-permute-start(bf16[64,2048]{1,0:T(8,128)(2,1)S(1)} %get-tuple-element.28), channel_id=1, source_target_pairs={{0,2},{1,5},{2,0},{3,7},{4,6},{5,1},{6,4},{7,3},{8,10},{9,13},{10,... | collective-permute-start | bytes 786440 | tf_op jit(solution)/shard_map/ppermute | solution.py:280
  54.7 1.8 %expert_rows.7 = (bf16[64,2048]{1,0:T(8,128)(2,1)S(1)}, bf16[64,2048]{1,0:T(8,128)(2,1)S(1)}) custom-call(f32[1,2048]{1,0:T(1,128)S(1)} %bitcast.8, bf16[2048,512]{1,0:T(8,128)(2,1)S(1)} %get-tuple-element.17.wg_ref, bf16[2048,512]{1,0:T(8,128)(2,1)S(1)} %get-tuple-element.18.wu_ref, bf16[512,2048]{1,0:T(8,128)(2,1)S(1)} %load_weights.3.wd_ref, ...), custom_call_target="tpu_custom_call" | custom-call | flops 805306368 | bytes 6291456 | tf_op jit(solution)/shard_map/expert_rows/pallas_call | solution.py:74
  56.6 0.7 collective-permute-start.12
  57.2 1.3 %collective-permute-start.16 = (bf16[64,2048]{1,0:T(8,128)(2,1)S(1)}, bf16[64,2048]{1,0:T(8,128)(2,1)S(1)}, u32[]{:S(2)}, u32[]{:S(2)}) collective-permute-start(bf16[64,2048]{1,0:T(8,128)(2,1)S(1)} %get-tuple-element.30), channel_id=1, source_target_pairs={{0,6},{1,7},{2,4},{3,5},{4,2},{5,3},{6,0},{7,1},{8,14},{9,15},{10,... | collective-permute-start | bytes 786440 | tf_op jit(solution)/shard_map/ppermute | solution.py:280
  58.5 1.2 %collective-permute-start.17 = (bf16[64,2048]{1,0:T(8,128)(2,1)S(1)}, bf16[64,2048]{1,0:T(8,128)(2,1)S(1)}, u32[]{:S(2)}, u32[]{:S(2)}) collective-permute-start(bf16[64,2048]{1,0:T(8,128)(2,1)S(1)} %get-tuple-element.31), channel_id=1, source_target_pairs={{0,7},{1,6},{2,5},{3,4},{4,3},{5,2},{6,1},{7,0},{8,15},{9,14},{10,... | collective-permute-start | bytes 786440 | tf_op jit(solution)/shard_map/ppermute | solution.py:280
  59.7 1.0 %shared_rows.1.base_ref = f32[128,2048]{1,0:T(8,128)S(1)} custom-call(bf16[128,2048]{1,0:T(8,128)(2,1)S(1)} %copy-done, f32[1,2048]{1,0:T(1,128)S(1)} %bitcast.9, bf16[2048,256]{1,0:T(8,128)(2,1)S(1)} %copy-done.1, bf16[2048,256]{1,0:T(8,128)(2,1)S(1)} %copy-done.2, bf16[256,2048]{1,0:T(8,128)(2,1)S(1)} %copy-done.3), custom_call_target="tpu_custom_call" | custom-call | tf_op jit(solution)/shard_map/shared_rows/pallas_call | solution.py:322
  60.7 0.5 multiply_bitcast_fusion
  61.3 0.8 %combine_rows.1 = (f32[128,2048]{1,0:T(8,128)S(1)}, bf16[256,192]{1,0:T(8,128)(2,1)S(1)}, f32[128,2]{1,0:T(8,128)S(1)}, bf16[128,64]{1,0:T(8,128)(2,1)S(1)}, f32[128,1]{1,0:T(8,128)S(1)}) custom-call(s32[2,128]{1,0:T(2,128)S(1)} %bitcast.12, f32[2,128]{1,0:T(2,128)S(1)} %bitcast.13, f32[128,2048]{1,0:T(8,128)S(1)} %shared_rows.1.base_ref, ...), custom_call_target="tpu_custom_call" | custom-call | tf_op jit(solution)/shard_map/combine_rows/pallas_call | solution.py:196
  62.0 2.7 %collective-permute-done.12.refs_1_ = bf16[64,2048]{1,0:T(8,128)(2,1)S(1)} collective-permute-done((bf16[64,2048]{1,0:T(8,128)(2,1)S(1)}, bf16[64,2048]{1,0:T(8,128)(2,1)S(1)}, u32[]{:S(2)}, u32[]{:S(2)}) %collective-permute-start.12) | collective-permute-done | bytes 262176 | tf_op jit(solution)/shard_map/ppermute | solution.py:280
  64.8 2.5 %collective-permute-done.16.refs_2_ = bf16[64,2048]{1,0:T(8,128)(2,1)S(1)} collective-permute-done((bf16[64,2048]{1,0:T(8,128)(2,1)S(1)}, bf16[64,2048]{1,0:T(8,128)(2,1)S(1)}, u32[]{:S(2)}, u32[]{:S(2)}) %collective-permute-start.16) | collective-permute-done | bytes 262176 | tf_op jit(solution)/shard_map/ppermute | solution.py:280
  67.3 0.4 middle_rows.1.base_ref
  67.7 6.2 %collective-permute-done.17.block_ref = bf16[64,2048]{1,0:T(8,128)(2,1)S(1)} collective-permute-done((bf16[64,2048]{1,0:T(8,128)(2,1)S(1)}, bf16[64,2048]{1,0:T(8,128)(2,1)S(1)}, u32[]{:S(2)}, u32[]{:S(2)}) %collective-permute-start.17) | collective-permute-done | bytes 262176 | tf_op jit(solution)/shard_map/ppermute | solution.py:280
  73.9 1.0 %finish_rows.1 = bf16[128,2048]{1,0:T(8,128)(2,1)} custom-call(bf16[128,64]{1,0:T(8,128)(2,1)S(1)} %get-tuple-element.23.pick_ref, f32[128,1]{1,0:T(8,128)S(1)} %get-tuple-element.24.gate_ref, f32[128,2048]{1,0:T(8,128)S(1)} %middle_rows.1.base_ref, bf16[64,2048]{1,0:T(8,128)(2,1)S(1)} %collective-permute-done.17.block_ref), custom_call_target="tpu_custom_call" | custom-call | tf_op jit(solution)/shard_map/finish_rows/pallas_call | solution.py:247
  (24 shorter events, 0.1 us)
Async XLA Ops:
  0.6 15.6 %collective-permute-start = (bf16[128,2048]{1,0:T(8,128)(2,1)}, bf16[128,2048]{1,0:T(8,128)(2,1)S(1)}, u32[]{:S(2)}, u32[]{:S(2)}) collective-permute-start(bf16[128,2048]{1,0:T(8,128)(2,1)} %refs_0_.5), channel_id=1, source_target_pairs={{0,4},{1,3},{2,6},{3,1},{4,0},{5,7},{6,2},{7,5},{8,12},{9,11},{10,... | collective-permute-start | bytes 1572872 | tf_op jit(solution)/shard_map/ppermute | solution.py:280
  3.7 14.5 %collective-permute-start.9 = (bf16[128,2048]{1,0:T(8,128)(2,1)}, bf16[128,2048]{1,0:T(8,128)(2,1)S(1)}, u32[]{:S(2)}, u32[]{:S(2)}) collective-permute-start(bf16[128,2048]{1,0:T(8,128)(2,1)} %refs_0_.5), channel_id=1, source_target_pairs={{0,2},{1,5},{2,0},{3,7},{4,6},{5,1},{6,4},{7,3},{8,10},{9,13},{10,... | collective-permute-start | bytes 1572872 | tf_op jit(solution)/shard_map/ppermute | solution.py:280
  16.2 9.2 %collective-permute-start.13 = (bf16[128,2048]{1,0:T(8,128)(2,1)S(1)}, bf16[128,2048]{1,0:T(8,128)(2,1)S(1)}, u32[]{:S(2)}, u32[]{:S(2)}) collective-permute-start(bf16[128,2048]{1,0:T(8,128)(2,1)S(1)} %collective-permute-done.refs_0_), channel_id=1, source_target_pairs={{0,2},{1,5},{2,0},{3,7},{4,6},{5,1},{6,4},{7,3},{8,10},{9,13},{10,... | collective-permute-start | bytes 1572872 | tf_op jit(solution)/shard_map/ppermute | solution.py:280
  17.6 25.8 %collective-permute-start.7 = (bf16[128,2048]{1,0:T(8,128)(2,1)}, bf16[128,2048]{1,0:T(8,128)(2,1)S(1)}, u32[]{:S(2)}, u32[]{:S(2)}) collective-permute-start(bf16[128,2048]{1,0:T(8,128)(2,1)} %refs_0_.5), channel_id=1, source_target_pairs={{0,1},{1,0},{2,3},{3,2},{4,5},{5,4},{6,7},{7,6},{8,9},{9,8},{10,11... | collective-permute-start | bytes 1572872 | tf_op jit(solution)/shard_map/ppermute | solution.py:280
  17.6 27.7 %collective-permute-start.1 = (bf16[128,2048]{1,0:T(8,128)(2,1)S(1)}, bf16[128,2048]{1,0:T(8,128)(2,1)S(1)}, u32[]{:S(2)}, u32[]{:S(2)}) collective-permute-start(bf16[128,2048]{1,0:T(8,128)(2,1)S(1)} %collective-permute-done.refs_0_), channel_id=1, source_target_pairs={{0,1},{1,0},{2,3},{3,2},{4,5},{5,4},{6,7},{7,6},{8,9},{9,8},{10,11... | collective-permute-start | bytes 1572872 | tf_op jit(solution)/shard_map/ppermute | solution.py:280
  18.2 32.2 %collective-permute-start.10 = (bf16[128,2048]{1,0:T(8,128)(2,1)S(1)}, bf16[128,2048]{1,0:T(8,128)(2,1)S(1)}, u32[]{:S(2)}, u32[]{:S(2)}) collective-permute-start(bf16[128,2048]{1,0:T(8,128)(2,1)S(1)} %collective-permute-done.9.refs_0_), channel_id=1, source_target_pairs={{0,1},{1,0},{2,3},{3,2},{4,5},{5,4},{6,7},{7,6},{8,9},{9,8},{10,11... | collective-permute-start | bytes 1572872 | tf_op jit(solution)/shard_map/ppermute | solution.py:280
  25.4 27.9 %collective-permute-start.14 = (bf16[128,2048]{1,0:T(8,128)(2,1)S(1)}, bf16[128,2048]{1,0:T(8,128)(2,1)S(1)}, u32[]{:S(2)}, u32[]{:S(2)}) collective-permute-start(bf16[128,2048]{1,0:T(8,128)(2,1)S(1)} %collective-permute-done.13.refs_0_), channel_id=1, source_target_pairs={{0,1},{1,0},{2,3},{3,2},{4,5},{5,4},{6,7},{7,6},{8,9},{9,8},{10,11... | collective-permute-start | bytes 1572872 | tf_op jit(solution)/shard_map/ppermute | solution.py:280
  25.4 1.9 %collective-permute-start.2 = (s32[2,128]{1,0:T(2,128)}, s32[2,128]{1,0:T(2,128)S(1)}, u32[]{:S(2)}, u32[]{:S(2)}) collective-permute-start(s32[2,128]{1,0:T(2,128)} %bitcast.10), channel_id=1, source_target_pairs={{0,1},{1,0},{2,3},{3,2},{4,5},{5,4},{6,7},{7,6},{8,9},{9,8},{10,11... | collective-permute-start | bytes 3080 | tf_op jit(solution)/shard_map/ppermute | solution.py:280
  27.3 0.7 copy-start.5
  28.0 3.9 %collective-permute-start.3 = (s32[4,128]{1,0:T(4,128)S(1)}, s32[4,128]{1,0:T(4,128)S(1)}, u32[]{:S(2)}, u32[]{:S(2)}) collective-permute-start(s32[4,128]{1,0:T(4,128)S(1)} %pair_routes.1.refs_2_.refs_3_.refs_0_), channel_id=1, source_target_pairs={{0,4},{1,3},{2,6},{3,1},{4,0},{5,7},{6,2},{7,5},{8,12},{9,11},{10,... | collective-permute-start | bytes 6152 | tf_op jit(solution)/shard_map/ppermute | solution.py:280
  32.0 3.6 %collective-permute-start.4 = (s32[4,128]{1,0:T(4,128)S(1)}, s32[4,128]{1,0:T(4,128)S(1)}, u32[]{:S(2)}, u32[]{:S(2)}) collective-permute-start(s32[4,128]{1,0:T(4,128)S(1)} %pair_routes.1.refs_2_.refs_3_.refs_0_), channel_id=1, source_target_pairs={{0,2},{1,5},{2,0},{3,7},{4,6},{5,1},{6,4},{7,3},{8,10},{9,13},{10,... | collective-permute-start | bytes 6152 | tf_op jit(solution)/shard_map/ppermute | solution.py:280
  35.5 6.1 %collective-permute-start.15 = (s32[4,128]{1,0:T(4,128)S(1)}, s32[4,128]{1,0:T(4,128)S(1)}, u32[]{:S(2)}, u32[]{:S(2)}) collective-permute-start(s32[4,128]{1,0:T(4,128)S(1)} %pair_routes.1.refs_2_.refs_3_.refs_0_), channel_id=1, source_target_pairs={{0,6},{1,7},{2,4},{3,5},{4,2},{5,3},{6,0},{7,1},{8,14},{9,15},{10,... | collective-permute-start | bytes 6152 | tf_op jit(solution)/shard_map/ppermute | solution.py:280
  39.3 4.2 %copy-start = (bf16[128,2048]{1,0:T(8,128)(2,1)S(1)}, bf16[128,2048]{1,0:T(8,128)(2,1)}, u32[]{:S(2)}) copy-start(bf16[128,2048]{1,0:T(8,128)(2,1)} %refs_0_.5) | copy-start | bytes 1572868
  39.3 4.2 %copy-start.4 = (f32[2048]{0:T(1024)S(1)}, f32[2048]{0:T(1024)}, u32[]{:S(2)}) copy-start(f32[2048]{0:T(1024)} %param.11) | copy-start | bytes 24580
  41.9 5.9 %collective-permute-start.18 = (f32[1,128]{1,0:T(1,128)S(1)}, f32[1,128]{1,0:T(1,128)S(1)}, u32[]{:S(2)}, u32[]{:S(2)}) collective-permute-start(f32[1,128]{1,0:T(1,128)S(1)} %slice.6), channel_id=1, source_target_pairs={{0,8},{8,0},{16,24},{24,16},{1,9},{9,1},{17,25},{25,17},{2,10},{10... | collective-permute-start | bytes 1544 | tf_op jit(solution)/shard_map/ppermute | solution.py:350
  45.3 11.9 %collective-permute-start.8 = (bf16[64,2048]{1,0:T(8,128)(2,1)S(1)}, bf16[64,2048]{1,0:T(8,128)(2,1)S(1)}, u32[]{:S(2)}, u32[]{:S(2)}) collective-permute-start(bf16[64,2048]{1,0:T(8,128)(2,1)S(1)} %get-tuple-element.22), channel_id=1, source_target_pairs={{0,1},{1,0},{2,3},{3,2},{4,5},{5,4},{6,7},{7,6},{8,9},{9,8},{10,11... | collective-permute-start | bytes 786440 | tf_op jit(solution)/shard_map/ppermute | solution.py:280
  47.2 11.3 %collective-permute-start.5 = (bf16[64,2048]{1,0:T(8,128)(2,1)S(1)}, bf16[64,2048]{1,0:T(8,128)(2,1)S(1)}, u32[]{:S(2)}, u32[]{:S(2)}) collective-permute-start(bf16[64,2048]{1,0:T(8,128)(2,1)S(1)} %get-tuple-element.19), channel_id=1, source_target_pairs={{0,4},{1,3},{2,6},{3,1},{4,0},{5,7},{6,2},{7,5},{8,12},{9,11},{10,... | collective-permute-start | bytes 786440 | tf_op jit(solution)/shard_map/ppermute | solution.py:280
  47.8 8.8 %collective-permute-start.19 = (f32[1,128]{1,0:T(1,128)S(1)}, f32[1,128]{1,0:T(1,128)S(1)}, u32[]{:S(2)}, u32[]{:S(2)}) collective-permute-start(f32[1,128]{1,0:T(1,128)S(1)} %slice_add_fusion), channel_id=1, source_target_pairs={{0,16},{8,24},{16,0},{24,8},{1,17},{9,25},{17,1},{25,9},{2,18},{10... | collective-permute-start | bytes 1544 | tf_op jit(solution)/shard_map/ppermute | solution.py:350
  50.4 10.9 %collective-permute-start.6 = (bf16[64,2048]{1,0:T(8,128)(2,1)S(1)}, bf16[64,2048]{1,0:T(8,128)(2,1)S(1)}, u32[]{:S(2)}, u32[]{:S(2)}) collective-permute-start(bf16[64,2048]{1,0:T(8,128)(2,1)S(1)} %get-tuple-element.20), channel_id=1, source_target_pairs={{0,3},{1,4},{2,1},{3,6},{4,7},{5,0},{6,5},{7,2},{8,11},{9,12},{10,... | collective-permute-start | bytes 786440 | tf_op jit(solution)/shard_map/ppermute | solution.py:280
  53.3 6.4 %copy-start.1 = (bf16[2048,256]{1,0:T(8,128)(2,1)S(1)}, bf16[2048,256]{1,0:T(8,128)(2,1)}, u32[]{:S(2)}) copy-start(bf16[2048,256]{1,0:T(8,128)(2,1)} %wg_ref.1) | copy-start | bytes 3145732
  53.3 6.4 %copy-start.2 = (bf16[2048,256]{1,0:T(8,128)(2,1)S(1)}, bf16[2048,256]{1,0:T(8,128)(2,1)}, u32[]{:S(2)}) copy-start(bf16[2048,256]{1,0:T(8,128)(2,1)} %wu_ref.1) | copy-start | bytes 3145732
  53.3 6.4 %copy-start.3 = (bf16[256,2048]{1,0:T(8,128)(2,1)S(1)}, bf16[256,2048]{1,0:T(8,128)(2,1)}, u32[]{:S(2)}) copy-start(bf16[256,2048]{1,0:T(8,128)(2,1)} %wd_ref.1) | copy-start | bytes 3145732
  53.3 8.7 %collective-permute-start.11 = (bf16[64,2048]{1,0:T(8,128)(2,1)S(1)}, bf16[64,2048]{1,0:T(8,128)(2,1)S(1)}, u32[]{:S(2)}, u32[]{:S(2)}) collective-permute-start(bf16[64,2048]{1,0:T(8,128)(2,1)S(1)} %get-tuple-element.28), channel_id=1, source_target_pairs={{0,2},{1,5},{2,0},{3,7},{4,6},{5,1},{6,4},{7,3},{8,10},{9,13},{10,... | collective-permute-start | bytes 786440 | tf_op jit(solution)/shard_map/ppermute | solution.py:280
  56.6 8.2 %collective-permute-start.12 = (bf16[64,2048]{1,0:T(8,128)(2,1)S(1)}, bf16[64,2048]{1,0:T(8,128)(2,1)S(1)}, u32[]{:S(2)}, u32[]{:S(2)}) collective-permute-start(bf16[64,2048]{1,0:T(8,128)(2,1)S(1)} %get-tuple-element.29), channel_id=1, source_target_pairs={{0,5},{1,2},{2,7},{3,0},{4,1},{5,6},{6,3},{7,4},{8,13},{9,10},{10,... | collective-permute-start | bytes 786440 | tf_op jit(solution)/shard_map/ppermute | solution.py:280
  57.2 10.1 %collective-permute-start.16 = (bf16[64,2048]{1,0:T(8,128)(2,1)S(1)}, bf16[64,2048]{1,0:T(8,128)(2,1)S(1)}, u32[]{:S(2)}, u32[]{:S(2)}) collective-permute-start(bf16[64,2048]{1,0:T(8,128)(2,1)S(1)} %get-tuple-element.30), channel_id=1, source_target_pairs={{0,6},{1,7},{2,4},{3,5},{4,2},{5,3},{6,0},{7,1},{8,14},{9,15},{10,... | collective-permute-start | bytes 786440 | tf_op jit(solution)/shard_map/ppermute | solution.py:280
  58.5 2.7 %copy-start.6 = (s32[128,2]{0,1:T(2,128)S(1)}, s32[128,2]{0,1:T(2,128)}, u32[]{:S(2)}) copy-start(s32[128,2]{0,1:T(2,128)} %param.12) | copy-start | bytes 3076
  58.5 2.7 %copy-start.7 = (f32[128,2]{0,1:T(2,128)S(1)}, f32[128,2]{0,1:T(2,128)}, u32[]{:S(2)}) copy-start(f32[128,2]{0,1:T(2,128)} %param.13) | copy-start | bytes 3076
  58.5 15.4 %collective-permute-start.17 = (bf16[64,2048]{1,0:T(8,128)(2,1)S(1)}, bf16[64,2048]{1,0:T(8,128)(2,1)S(1)}, u32[]{:S(2)}, u32[]{:S(2)}) collective-permute-start(bf16[64,2048]{1,0:T(8,128)(2,1)S(1)} %get-tuple-element.31), channel_id=1, source_target_pairs={{0,7},{1,6},{2,5},{3,4},{4,3},{5,2},{6,1},{7,0},{8,15},{9,14},{10,... | collective-permute-start | bytes 786440 | tf_op jit(solution)/shard_map/ppermute | solution.py:280
